TPU v7x, 256 devices: a 4x2x16 block of a 4x16x16 slice. The times are simulated.
256 devices in a mesh: grp: 2 (over y), sp: 16 (over z), tp: 8 (over x, core).
Axes of the slice: x: 4, y: 2, z: 16, core: 2. Of those that a mesh axis runs over, the one named last changes fastest.
The devices are a block of a 4x16x16 slice.
Arguments:
- residual: bfloat16 [16384, 2048], P(('grp', 'sp')), parts along dimension 0, may hold values from -6 to 6
- values: bfloat16 [16384, 4096], P(('grp', 'sp'), 'tp'), parts along dimension 0, may hold values from -6 to 6
- out_gate: bfloat16 [16384, 4096], P(('grp', 'sp'), 'tp'), parts along dimension 0, may hold values from -6 to 6
- writes: bfloat16 [16384, 1024], P(('grp', 'sp'), 'tp'), parts along dimension 0, may hold values from -6 to 6
- reads: bfloat16 [16384, 1024], P(('grp', 'sp'), 'tp'), parts along dimension 0, may hold values from -6 to 6
- step_raw: bfloat16 [64, 16384], P('tp', ('grp', 'sp')), parts along dimension 1, may hold values from -4.5 to 4.5
- decay_rate: float32 [64], P('tp'), may hold values from 0 to 0.1
- decay_jump: float32 [64, 16384], P('tp', ('grp', 'sp')), parts along dimension 1, may hold values from -0.7 to 0
- documents: int32 [16384], P(('grp', 'sp')), parts along dimension 0, may hold values from 0 to 7, never falling along the last dimension, each value on 1 to 1536 neighbouring positions
- taps_values: bfloat16 [4, 4096], P(None, 'tp'), may hold values from -3 to 3
- taps_write: bfloat16 [4, 1024], P(None, 'tp'), may hold values from -3 to 3
- taps_read: bfloat16 [4, 1024], P(None, 'tp'), may hold values from -3 to 3
- mixer_gain: bfloat16 [4096], P('tp'), may hold values from 0.099609375 to 1.8984375
- mixer_out: bfloat16 [4096, 2048], P('tp'), may hold values from -0.09375 to 0.09375
- channel_gain: bfloat16 [2048], replicated, may hold values from 0.099609375 to 1.8984375
- gate_weight: bfloat16 [2048, 5632], P('sp', 'tp'), may hold values from -0.125 to 0.125
- up_weight: bfloat16 [2048, 5632], P('sp', 'tp'), may hold values from -0.125 to 0.125
- down_rows: bfloat16 [2048, 5632], P('sp', 'tp'), may hold values from -0.078125 to 0.078125
Outputs:
- layer_out: bfloat16 [16384, 2048], P(('grp', 'sp'), 'tp'), parts along dimension 0
There are 2 independent parts, one for each index of `grp`. A program takes and returns all parts, laid end to end along the dimension named above; an argument that names none is the same for every part. Nothing has to cross between parts.
Inputs may be any that keep to these rules, and one draw needn't show every extreme that they name: `documents`: document numbers never fall along the sequence; a document starts where the number changes, and is one to 1536 positions long.
All inputs are finite; a program needn't handle non-finite values.
Results may differ from a plain program's by a relative error of at most 0.017.
Values may be sent and summed in bfloat16 or wider, within the bound.
No kernel may reach another device: no remote copies, remote signals or barrier semaphores. Data moves between devices by JAX's collectives and lax.ppermute only.
A program may use at most 64 MiB of HBM per device.

v0:
```python
import jax
import jax.numpy as jnp
from jax import lax
from jax.sharding import PartitionSpec as P

HEADS = 64
GROUPS = 8
BLOCK = 128


norm_eps = 1e-06


def from_behind(value, axis, by):
    peers = lax.axis_size(axis)
    pairs = [(i, i + by) for i in range(peers) if 0 <= i + by < peers]
    return lax.ppermute(value, axis, pairs)


def all_in_one(value, axis):
    leaves = jax.tree.leaves(value)
    turns = sorted(range(len(leaves)), key=lambda k: -leaves[k].size)
    width = (1, *leaves[turns[0]].shape)[-1]
    lines = [
        jnp.pad(leaves[k].reshape(-1), (0, -leaves[k].size % width)).reshape(-1, width)
        for k in turns
    ]
    both, at, found = (lax.all_gather(jnp.concatenate(lines), axis), 0, {})
    for k, line in zip(turns, lines):
        section = both[:, at : at + len(line)].reshape(len(both), -1)
        found[k] = section[:, : leaves[k].size].reshape(-1, *leaves[k].shape)
        at += len(line)
    numbers = iter(range(len(leaves)))
    return jax.tree.map(lambda _: found[next(numbers)], value)


def prefix(value, axis, combine, identity):
    peers, index = (lax.axis_size(axis), lax.axis_index(axis))
    everything = all_in_one(
        jax.tree.map(
            lambda part, kind: part.astype(kind),
            value,
            (jnp.bfloat16, jnp.bfloat16, jnp.bfloat16, jnp.bfloat16),
        ),
        axis,
    )
    start = jax.tree.map(
        lambda part, zero: jnp.broadcast_to(jnp.asarray(zero, part.dtype), part.shape),
        value,
        identity,
    )

    def step(k, before):
        reached = k < index
        new = combine(
            before, jax.tree.map(lambda part, own: part[k].astype(own.dtype), everything, value)
        )
        return jax.tree.map(lambda a, b: jnp.where(reached, a, b), new, before)

    return lax.fori_loop(0, peers, step, start)


def cut_along(value, dim, peers):
    shape = value.shape
    blocks = value.reshape(*shape[:dim], peers, shape[dim] // peers, *shape[dim + 1 :])
    return jnp.moveaxis(blocks, dim, 0)


def sum_at_owner(value, axis, dim):
    peers = lax.axis_size(axis)
    blocks = lax.all_to_all(cut_along(value, dim, peers), axis, 0, 0, tiled=True)
    return jnp.sum(blocks.astype(jnp.float32), axis=0)


def laid_out(blocks, dim):
    blocks = jnp.moveaxis(blocks, 0, dim)
    shape = blocks.shape
    return blocks.reshape(*shape[:dim], shape[dim] * shape[dim + 1], *shape[dim + 2 :])


def sent_to_all(value, axis):
    peers = lax.axis_size(axis)
    return lax.all_to_all(
        jnp.broadcast_to(value[None], (peers, *value.shape)), axis, 0, 0, tiled=True
    )


def gather_directly(value, axis, dim):
    return laid_out(sent_to_all(value, axis), dim)


def in_one_piece(arrays, axis, dim, along):
    both = jnp.concatenate(arrays, axis=along)
    result, at, gathered = (lax.all_gather(both, axis, axis=dim, tiled=True), 0, [])
    for a in arrays:
        gathered.append(lax.slice_in_dim(result, at, at + a.shape[along], axis=along))
        at += a.shape[along]
    return tuple(gathered)


def short_filter(rows, row_docs, taps):
    width = taps.shape[0]
    count = rows.shape[0] - width + 1
    own_docs = row_docs[width - 1 :]
    total = jnp.zeros((count, rows.shape[1]), jnp.float32)
    for offset in range(width):
        alive = (row_docs[offset : offset + count] == own_docs).astype(jnp.float32)
        total = (
            total
            + rows[offset : offset + count].astype(jnp.float32)
            * taps[offset].astype(jnp.float32)[None, :]
            * alive[:, None]
        )
    return jax.nn.silu(total).astype(jnp.bfloat16)


def block_pieces(values, writes, reads, step_size, log_decay, segment, heads_per, block):
    span = values.shape[0]
    block_count = span // block
    heads = step_size.shape[0]
    groups = heads // heads_per
    head_size = values.shape[1] // heads
    state_size = writes.shape[1] // groups
    value_blocks = values.reshape(block_count, block, groups, heads_per, head_size)
    write_blocks = writes.reshape(block_count, block, groups, state_size)
    read_blocks = reads.reshape(block_count, block, groups, state_size)
    block_docs = segment.reshape(block_count, block)
    step_blocks = step_size.reshape(groups, heads_per, block_count, block)
    running = jnp.cumsum(log_decay.reshape(groups, heads_per, block_count, block), axis=3)
    target = lax.broadcasted_iota(jnp.int32, (block, block), 0)
    source = lax.broadcasted_iota(jnp.int32, (block, block), 1)
    allowed = (target >= source)[None] & (block_docs[:, :, None] == block_docs[:, None, :])
    scores = jnp.einsum(
        "kign,kjgn->gkij", read_blocks, write_blocks, preferred_element_type=jnp.float32
    )
    spread = running[..., :, None] - running[..., None, :]
    decay = jnp.exp(jnp.where(allowed[None, None], spread, -jnp.inf))
    weights = (decay * scores[:, None] * step_blocks[..., None, :]).astype(jnp.bfloat16)
    inner = jnp.einsum(
        "gekij,kjgep->kigep", weights, value_blocks, preferred_element_type=jnp.float32
    )
    last_total = running[..., -1]
    same_end = (block_docs == block_docs[:, -1:]).astype(jnp.float32)
    end_factor = jnp.exp(last_total[..., None] - running) * step_blocks * same_end[None, None]
    scaled = (
        value_blocks.astype(jnp.float32) * jnp.transpose(end_factor, (2, 3, 0, 1))[..., None]
    ).astype(jnp.bfloat16)
    states = jnp.einsum(
        "kjgep,kjgn->kgepn", scaled, write_blocks, preferred_element_type=jnp.float32
    )
    return (inner, states, last_total, running, block_docs)


def block_passing(last_total, block_docs, prior_docs):
    return jnp.exp(last_total) * (block_docs[:, -1] == prior_docs).astype(jnp.float32)[None, None]


def carry_states(states, passing, start):

    def advance(held, entry):
        factor, fresh = entry
        return (factor[..., None, None] * held + fresh, held)

    final, entering = lax.scan(advance, start, (jnp.moveaxis(passing, 2, 0), states))
    return (entering, final)


def read_states(reads, entering, running, block_docs, prior_docs):
    block_count, block = block_docs.shape
    groups = entering.shape[1]
    read_blocks = reads.astype(jnp.float32).reshape(block_count, block, groups, -1)
    alive = (block_docs == prior_docs[:, None]).astype(jnp.float32)
    reach = jnp.exp(running) * alive[None, None]
    taken = jnp.einsum("kign,kgepn->kigep", read_blocks, entering)
    return taken * jnp.transpose(reach, (2, 3, 0, 1))[..., None]


def join_states(earlier, later):
    early_decay, early_state, early_first, early_last = earlier
    late_decay, late_state, late_first, late_last = later
    link = ((late_first == early_last) | (early_last < 0.0) | (late_first < 0.0)).astype(
        jnp.float32
    )
    carried = late_decay * link
    return (
        early_decay * carried,
        late_state + carried[..., None, None] * early_state,
        jnp.where(early_first < 0.0, late_first, early_first),
        jnp.where(late_last < 0.0, early_last, late_last),
    )


def down_product(hidden, rows):
    return lax.dot_general(
        hidden, rows, (((1,), (1,)), ((), ())), preferred_element_type=jnp.float32
    )


def on_device(
    residual,
    values,
    out_gate,
    writes,
    reads,
    step_raw,
    decay_rate,
    decay_jump,
    documents,
    taps_values,
    taps_write,
    taps_read,
    mixer_gain,
    mixer_out,
    channel_gain,
    gate_weight,
    up_weight,
    down_rows,
):
    tokens = values.shape[0]
    edge = taps_values.shape[0] - 1
    segment = documents.astype(jnp.float32)
    before = from_behind(
        (
            values[tokens - edge :],
            writes[tokens - edge :],
            reads[tokens - edge :],
            segment[tokens - edge :].astype(jnp.bfloat16),
        ),
        "sp",
        1,
    )
    row_docs = jnp.concatenate([before[3].astype(jnp.float32), segment])
    short_values = short_filter(jnp.concatenate([before[0], values]), row_docs, taps_values)
    short_writes = short_filter(jnp.concatenate([before[1], writes]), row_docs, taps_write)
    short_reads = short_filter(jnp.concatenate([before[2], reads]), row_docs, taps_read)
    step_size = jax.nn.softplus(step_raw.astype(jnp.float32))
    log_decay = decay_jump - decay_rate[:, None] * step_size
    heads_per = HEADS // GROUPS
    inner, states, last_total, running, block_docs = block_pieces(
        short_values, short_writes, short_reads, step_size, log_decay, segment, heads_per, BLOCK
    )
    groups = states.shape[1]
    local_prior = jnp.concatenate([jnp.full((1,), -1.0, jnp.float32), block_docs[:-1, -1]])
    zero_state = jnp.zeros(states.shape[1:], jnp.float32)
    entering, final = carry_states(
        states, block_passing(last_total, block_docs, local_prior), zero_state
    )
    whole_decay = jnp.exp(jnp.sum(last_total, axis=2)) * (segment[0] == segment[-1]).astype(
        jnp.float32
    )
    identity = (
        jnp.ones_like(whole_decay),
        zero_state,
        jnp.full((1,), -1.0, jnp.float32),
        jnp.full((1,), -1.0, jnp.float32),
    )
    scanned = prefix((whole_decay, final, segment[:1], segment[-1:]), "sp", join_states, identity)
    held = scanned[1]
    prior_docs = jnp.concatenate([scanned[3], block_docs[:-1, -1]])
    passing_in = block_passing(last_total, block_docs, prior_docs)
    gains = jnp.cumprod(passing_in, axis=2)
    gains = jnp.concatenate([jnp.ones_like(gains[..., :1]), gains[..., :-1]], axis=2)
    entering = entering + jnp.moveaxis(gains, 2, 0)[..., None, None] * held[None]
    mixed = inner + read_states(short_reads, entering, running, block_docs, prior_docs)
    gated = mixed.reshape(tokens, -1) * jax.nn.silu(out_gate.astype(jnp.float32))
    grouped = gated.reshape(tokens, groups, -1)
    grouped = grouped * lax.rsqrt(jnp.mean(grouped * grouped, axis=2, keepdims=True) + norm_eps)
    mixer_in = (grouped.reshape(tokens, -1) * mixer_gain.astype(jnp.float32)[None, :]).astype(
        jnp.bfloat16
    )
    partial_value = jnp.dot(mixer_in, mixer_out, preferred_element_type=jnp.float32)
    share = residual.shape[1] // lax.axis_size("tp")
    mix_share = sum_at_owner(partial_value.astype(jnp.bfloat16), "tp", 1)
    own_residual = lax.dynamic_slice_in_dim(residual, lax.axis_index("tp") * share, share, 1)
    own_after = (own_residual.astype(jnp.float32) + mix_share).astype(jnp.bfloat16)
    after = gather_directly(own_after, "tp", 1)
    after_wide = after.astype(jnp.float32)
    normal = after_wide * lax.rsqrt(
        jnp.mean(after_wide * after_wide, axis=1, keepdims=True) + norm_eps
    )
    normal = (normal * channel_gain.astype(jnp.float32)[None, :]).astype(jnp.bfloat16)
    late_weights = in_one_piece((gate_weight, up_weight, down_rows), "sp", 0, 1)
    gate = jnp.dot(normal, late_weights[0], preferred_element_type=jnp.float32)
    up = jnp.dot(normal, late_weights[1], preferred_element_type=jnp.float32)
    hidden = (jax.nn.silu(gate) * up).astype(jnp.bfloat16)
    down = down_product(hidden, late_weights[2])
    down_share = sum_at_owner(down.astype(jnp.bfloat16), "tp", 1)
    return (own_after.astype(jnp.float32) + down_share).astype(jnp.bfloat16)


def solution(mesh):
    return jax.shard_map(
        on_device,
        mesh=mesh,
        in_specs=(
            P(("grp", "sp"), None),
            P(("grp", "sp"), "tp"),
            P(("grp", "sp"), "tp"),
            P(("grp", "sp"), "tp"),
            P(("grp", "sp"), "tp"),
            P("tp", ("grp", "sp")),
            P("tp"),
            P("tp", ("grp", "sp")),
            P(("grp", "sp")),
            P(None, "tp"),
            P(None, "tp"),
            P(None, "tp"),
            P("tp"),
            P("tp", None),
            P(),
            P("sp", "tp"),
            P("sp", "tp"),
            P("sp", "tp"),
        ),
        out_specs=P(("grp", "sp"), "tp"),
        check_vma=False,
    )
```

profile of v0, /device:TPU:33, one launch (start us, length us, event | category | flops | bytes accessed | tf_op | source)
XLA Modules:
  0.0 341.1 jit_solution(3831854967552443935)
XLA Ops:
  7.5 5.2 %collective-permute-start.1 = (bf16[3]{0:T(256)(128)(2,1)S(1)}, bf16[3]{0:T(256)(128)(2,1)S(1)}, u32[]{:S(2)}, u32[]{:S(2)}) collective-permute-start(bf16[3]{0:T(256)(128)(2,1)S(1)} %slice.147), channel_id=1, source_target_pairs={{0,8},{8,16},{16,24},{24,32},{32,40},{40,48},{48,56},{56,64},{64,7... | collective-permute-start | bytes 26 | tf_op jit(solution)/shard_map/ppermute | solution.py:17
  13.6 4.4 %collective-permute-start = (bf16[3,512]{0,1:T(8,128)(2,1)S(1)}, bf16[3,512]{0,1:T(8,128)(2,1)S(1)}, u32[]{:S(2)}, u32[]{:S(2)}) collective-permute-start(bf16[3,512]{0,1:T(8,128)(2,1)S(1)} %copy.61), channel_id=1, source_target_pairs={{0,8},{8,16},{16,24},{24,32},{32,40},{40,48},{48,56},{56,64},{64,7... | collective-permute-start | bytes 9224 | tf_op jit(solution)/shard_map/ppermute | solution.py:17
  18.7 4.4 %collective-permute-start.3 = (bf16[3,128]{1,0:T(4,128)(2,1)S(1)}, bf16[3,128]{1,0:T(4,128)(2,1)S(1)}, u32[]{:S(2)}, u32[]{:S(2)}) collective-permute-start(bf16[3,128]{1,0:T(4,128)(2,1)S(1)} %slice.164), channel_id=1, source_target_pairs={{0,8},{8,16},{16,24},{24,32},{32,40},{40,48},{48,56},{56,64},{64,7... | collective-permute-start | bytes 2312 | tf_op jit(solution)/shard_map/ppermute | solution.py:17
  23.2 1.3 copy.62
  28.0 1.4 slice_convert_fusion.3
  29.5 1.3 fusion.55
  30.8 1.1 reduce_window_sum.11
  37.8 1.5 multiply_convert_fusion.6
  40.1 2.3 multiply_convert_fusion.4
  43.8 5.8 %while.29 = (s32[]{:T(128)}, f32[1,8,64,128]{3,2,1,0:T(8,128)S(1)}, f32[4,1,8,64,128]{4,3,2,1,0:T(8,128)}, f32[4,1,8]{2,1,0:T(1,128)}, f32[4,1,8,64,128]{4,3,2,1,0:T(8,128)S(1)}, /*index=5*/s32[]{:T(128)}, s32[]{:T(128)}) while((s32[]{:T(128)}, f32[1,8,64,128]{3,2,1,0:T(8,128)S(1)}, f32[4,1,8,64,128]{4,3,2,1,0:T(8,128)}, ...), condition=%wide.region_2.3_spmd.clone, body=%wide.region_1.2_spmd.clone.sunk | while | flops 262147 | bytes 1311424 | solution.py:164
  50.5 1.9 pad_maximum_fusion
  52.5 5.6 %collective-permute-start.2 = (bf16[3,128]{1,0:T(4,128)(2,1)S(1)}, bf16[3,128]{1,0:T(4,128)(2,1)S(1)}, u32[]{:S(2)}, u32[]{:S(2)}) collective-permute-start(bf16[3,128]{1,0:T(4,128)(2,1)S(1)} %slice.156), channel_id=1, source_target_pairs={{0,8},{8,16},{16,24},{24,32},{32,40},{40,48},{48,56},{56,64},{64,7... | collective-permute-start | bytes 2312 | tf_op jit(solution)/shard_map/ppermute | solution.py:17
  59.0 1.3 copy.78
  62.2 61.6 %all-gather.7.cloned.1.call-done = bf16[16,515,128]{2,1,0:T(8,128)(2,1)} async-done(((bf16[1,515,128]{2,1,0:T(8,128)(2,1)}), bf16[16,515,128]{2,1,0:T(8,128)(2,1)}) %all-gather.7.cloned.1.call-update) | async-done | bytes 2109456 | tf_op jit(solution)/shard_map/all_gather | solution.py:28
  124.8 3.2 slice.201
  127.9 64.7 %while.30 = (s32[]{:T(128)}, f32[1,8,64,128]{3,2,1,0:T(8,128)S(1)}, f32[1]{0:T(128)}, s32[]{:T(128)}, bf16[16,1,8,64,128]{4,3,2,1,0:T(8,128)(2,1)}, /*index=5*/b...) while((s32[]{:T(128)}, f32[1,8,64,128]{3,2,1,0:T(8,128)S(1)}, ...), condition=%wide.region_5.6_spmd.clone, body=%wide.region_4.5_spmd.clone.sunk | while | flops 327709 | bytes 655658 | solution.py:60
  129.8 1.0 fusion.77
  133.9 1.0 fusion.77
  137.9 1.0 fusion.77
  146.0 1.0 fusion.77
  154.1 1.0 fusion.77
  158.1 1.0 fusion.77
  166.2 1.0 fusion.77
  170.3 1.0 fusion.77
  174.3 1.0 fusion.77
  178.4 1.0 fusion.77
  186.5 1.0 fusion.77
  190.5 1.0 fusion.77
  192.7 1.3 compare_convert_fusion.1
  194.0 1.3 bitcast_multiply_fusion.2
  195.3 1.3 reduce_window.9
  198.1 1.6 fusion.20
  199.7 1.5 fusion.19
  202.4 1.4 convolution_convert_fusion.1
  203.8 1.5 copy.111
  205.3 14.4 %all-to-all-start = ((bf16[8,512,256]{2,1,0:T(8,128)(2,1)}), bf16[8,512,256]{2,1,0:T(8,128)(2,1)}, u32[]{:S(2)}, u32[]{:S(2)}) async-start(bf16[8,512,256]{2,1,0:T(8,128)(2,1)} %bitcast.210), calls=%async_computation | async-start | bytes 4194304 | tf_op jit(solution)/shard_map/all_to_all | solution.py:71
  219.7 26.3 %all-to-all-done = bf16[8,512,256]{2,1,0:T(8,128)(2,1)} async-done(((bf16[8,512,256]{2,1,0:T(8,128)(2,1)}), bf16[8,512,256]{2,1,0:T(8,128)(2,1)}, u32[]{:S(2)}, u32[]{:S(2)}) %all-to-all-start) | async-done | bytes 2097184 | tf_op jit(solution)/shard_map/all_to_all | solution.py:71
  246.0 2.0 convert_reduce_fusion.1
  248.0 1.0 add_convert_fusion.1
  249.1 1.6 broadcast_in_dim.25
  250.7 5.3 %all-to-all-start.1 = ((bf16[8,512,256]{1,2,0:T(8,128)(2,1)}), bf16[8,512,256]{1,2,0:T(8,128)(2,1)}, u32[]{:S(2)}, u32[]{:S(2)}) async-start(bf16[8,512,256]{1,2,0:T(8,128)(2,1)} %broadcast_in_dim.25), calls=%async_computation.1 | async-start | bytes 4194304 | tf_op jit(solution)/shard_map/all_to_all | solution.py:83
  256.0 26.4 %all-to-all-done.1 = bf16[8,512,256]{1,2,0:T(8,128)(2,1)} async-done(((bf16[8,512,256]{1,2,0:T(8,128)(2,1)}), bf16[8,512,256]{1,2,0:T(8,128)(2,1)}, u32[]{:S(2)}, u32[]{:S(2)}) %all-to-all-start.1) | async-done | bytes 2097184 | tf_op jit(solution)/shard_map/all_to_all | solution.py:83
  282.4 2.1 multiply_reduce_fusion
  284.5 3.5 %fusion.7 = bf16[512,2048]{0,1:T(8,128)(2,1)} fusion(f32[2048]{0:T(1024)S(1)} %convert_element_type.331, f32[512]{0:T(512)S(1)} %add_rsqrt_fusion, bf16[8,512,256]{1,2,0:T(8,128)(2,1)} %all-to-all-done.1), kind=kLoop, calls=%fused_computation.15 | loop fusion | flops 4194304 | bytes 4204544 | tf_op jit(solution)/shard_map/convert_element_type | solution.py:281
  288.0 5.2 %fusion.11 = f32[512,704]{0,1:T(8,128)} fusion(bf16[512,2048]{0,1:T(8,128)(2,1)} %fusion.7, bf16[2048,2112]{0,1:T(8,128)(2,1)} %all-gather.5.cloned.1.call-done), kind=kOutput, calls=%fused_computation.24 | convolution fusion | flops 1476395008 | bytes 6422528 | tf_op jit(solution)/shard_map/dot_general | solution.py:283
  293.2 8.5 %convolution_convert_fusion = bf16[512,2048]{1,0:T(8,128)(2,1)} fusion(bf16[2048,2112]{0,1:T(8,128)(2,1)} %all-gather.5.cloned.1.call-done, bf16[512,2048]{0,1:T(8,128)(2,1)} %fusion.7, f32[512,704]{0,1:T(8,128)} %fusion.11), kind=kOutput, calls=%fused_computation.19 | convolution fusion | flops 2956001280 | bytes 11403264 | tf_op jit(solution)/shard_map/dot_general | solution.py:194
  301.8 1.7 copy.110
  303.5 29.6 %all_to_all.15 = bf16[8,512,256]{2,1,0:T(8,128)(2,1)S(1)} all-to-all(bf16[8,512,256]{2,1,0:T(8,128)(2,1)S(1)} %bitcast.211), channel_id=1, replica_groups=mesh['grp'=2,'sp'=16,'tp'=8] {'tp'}, dimensions={0} | all-to-all | bytes 4194304 | tf_op jit(solution)/shard_map/all_to_all | solution.py:71
  (169 shorter events, 39.1 us)
Async XLA Ops:
  6.5 195.8 %copy-start = (bf16[512,2048]{1,0:T(8,128)(2,1)S(1)}, bf16[512,2048]{1,0:T(8,128)(2,1)}, u32[]{:S(2)}) copy-start(bf16[512,2048]{1,0:T(8,128)(2,1)} %param.35) | copy-start | bytes 6291460
  6.6 117.2 %all-gather.7.cloned.1.call-start = ((), (), s32[]{:S(2)}) async-start(), calls=%async_computation.4 | async-start | bytes 2263040 | tf_op jit(solution)/shard_map/all_gather | solution.py:28
  7.4 17.4 %copy-start.9 = (f32[4,128]{1,0:T(4,128)}, f32[4,128]{1,0:T(4,128)S(1)}, u32[]{:S(2)}) copy-start(f32[4,128]{1,0:T(4,128)S(1)} %get-tuple-element.321) | copy-start | bytes 6148
  7.5 29.5 %collective-permute-start.1 = (bf16[3]{0:T(256)(128)(2,1)S(1)}, bf16[3]{0:T(256)(128)(2,1)S(1)}, u32[]{:S(2)}, u32[]{:S(2)}) collective-permute-start(bf16[3]{0:T(256)(128)(2,1)S(1)} %slice.147), channel_id=1, source_target_pairs={{0,8},{8,16},{16,24},{24,32},{32,40},{40,48},{48,56},{56,64},{64,7... | collective-permute-start | bytes 26 | tf_op jit(solution)/shard_map/ppermute | solution.py:17
  13.6 25.8 %collective-permute-start = (bf16[3,512]{0,1:T(8,128)(2,1)S(1)}, bf16[3,512]{0,1:T(8,128)(2,1)S(1)}, u32[]{:S(2)}, u32[]{:S(2)}) collective-permute-start(bf16[3,512]{0,1:T(8,128)(2,1)S(1)} %copy.61), channel_id=1, source_target_pairs={{0,8},{8,16},{16,24},{24,32},{32,40},{40,48},{48,56},{56,64},{64,7... | collective-permute-start | bytes 9224 | tf_op jit(solution)/shard_map/ppermute | solution.py:17
  18.7 19.1 %collective-permute-start.3 = (bf16[3,128]{1,0:T(4,128)(2,1)S(1)}, bf16[3,128]{1,0:T(4,128)(2,1)S(1)}, u32[]{:S(2)}, u32[]{:S(2)}) collective-permute-start(bf16[3,128]{1,0:T(4,128)(2,1)S(1)} %slice.164), channel_id=1, source_target_pairs={{0,8},{8,16},{16,24},{24,32},{32,40},{40,48},{48,56},{56,64},{64,7... | collective-permute-start | bytes 2312 | tf_op jit(solution)/shard_map/ppermute | solution.py:17
  24.6 14.8 %copy-start.21 = (f32[4]{0:T(128)}, f32[4]{0:T(128)S(1)}, u32[]{:S(2)}) copy-start(f32[4]{0:T(128)S(1)} %slice_reduce_fusion.3) | copy-start | bytes 52
  24.8 14.6 %copy-start.22 = (f32[3]{0:T(128)}, f32[3]{0:T(128)S(1)}, u32[]{:S(2)}) copy-start(f32[3]{0:T(128)S(1)} %slice_reduce_fusion.2) | copy-start | bytes 40
  32.1 7.3 %copy-start.19 = (f32[8,4]{0,1:T(4,128)}, f32[8,4]{0,1:T(4,128)S(1)}, u32[]{:S(2)}) copy-start(f32[8,4]{0,1:T(4,128)S(1)} %get-tuple-element.276) | copy-start | bytes 388
  37.8 2.2 copy-start.11
  37.8 2.2 copy-start.13
  37.8 2.2 copy-start.15
  37.8 2.2 copy-start.17
  39.3 4.4 %copy-start.3 = (bf16[512,128]{1,0:T(8,128)(2,1)}, bf16[512,128]{1,0:T(8,128)(2,1)S(1)}, u32[]{:S(2)}) copy-start(bf16[512,128]{1,0:T(8,128)(2,1)S(1)} %multiply_convert_fusion.6) | copy-start | bytes 393220
  39.4 0.7 copy-start.7
  42.5 1.0 copy-start.1
  43.8 5.9 %copy-start.25 = (bf16[1,128]{1,0:T(2,128)(2,1)S(1)}, bf16[1,128]{1,0:T(2,128)(2,1)}, u32[]{:S(2)}) copy-start(bf16[1,128]{1,0:T(2,128)(2,1)} %get-tuple-element.333) | copy-start | bytes 772
  43.8 5.9 %copy-start.26 = (bf16[1,128]{1,0:T(2,128)(2,1)S(1)}, bf16[1,128]{1,0:T(2,128)(2,1)}, u32[]{:S(2)}) copy-start(bf16[1,128]{1,0:T(2,128)(2,1)} %get-tuple-element.334) | copy-start | bytes 772
  43.8 5.9 %copy-start.29 = (bf16[1,128]{1,0:T(2,128)(2,1)S(1)}, bf16[1,128]{1,0:T(2,128)(2,1)}, u32[]{:S(2)}) copy-start(bf16[1,128]{1,0:T(2,128)(2,1)} %pad_bitcast_fusion.3) | copy-start | bytes 772
  49.6 2.9 copy-start.6
  49.6 8.6 %copy-start.10 = (f32[4,128]{1,0:T(4,128)S(1)}, f32[4,128]{1,0:T(4,128)}, u32[]{:S(2)}) copy-start(f32[4,128]{1,0:T(4,128)} %copy-done.9) | copy-start | bytes 6148
  49.6 9.4 %copy-start.24 = (bf16[4,128]{1,0:T(4,128)(2,1)S(1)}, bf16[4,128]{1,0:T(4,128)(2,1)}, u32[]{:S(2)}) copy-start(bf16[4,128]{1,0:T(4,128)(2,1)} %param.33) | copy-start | bytes 3076
  49.6 10.7 %copy-start.28 = (bf16[512]{0:T(512)(128)(2,1)S(1)}, bf16[512]{0:T(512)(128)(2,1)}, u32[]{:S(2)}) copy-start(bf16[512]{0:T(512)(128)(2,1)} %param.34) | copy-start | bytes 3076
  49.6 11.2 %copy-start.12 = (f32[512]{0:T(512)S(1)}, f32[512]{0:T(512)}, u32[]{:S(2)}) copy-start(f32[512]{0:T(512)} %copy-done.11) | copy-start | bytes 6148
  49.6 11.2 %copy-start.14 = (f32[512]{0:T(512)S(1)}, f32[512]{0:T(512)}, u32[]{:S(2)}) copy-start(f32[512]{0:T(512)} %copy-done.13) | copy-start | bytes 6148
  49.6 11.2 %copy-start.16 = (f32[512]{0:T(512)S(1)}, f32[512]{0:T(512)}, u32[]{:S(2)}) copy-start(f32[512]{0:T(512)} %copy-done.15) | copy-start | bytes 6148
  49.6 11.2 %copy-start.18 = (f32[512]{0:T(512)S(1)}, f32[512]{0:T(512)}, u32[]{:S(2)}) copy-start(f32[512]{0:T(512)} %copy-done.17) | copy-start | bytes 6148
  49.6 11.6 %copy-start.4 = (bf16[512,128]{1,0:T(8,128)(2,1)S(1)}, bf16[512,128]{1,0:T(8,128)(2,1)}, u32[]{:S(2)}) copy-start(bf16[512,128]{1,0:T(8,128)(2,1)} %copy-done.3) | copy-start | bytes 393220
  50.4 237.6 %all-gather.5.cloned.1.call-start = ((), (), s32[]{:S(2)}) async-start(), calls=%async_computation.3 | async-start | bytes 9191424 | tf_op jit(solution)/shard_map/all_gather | solution.py:94
  52.5 8.3 %collective-permute-start.2 = (bf16[3,128]{1,0:T(4,128)(2,1)S(1)}, bf16[3,128]{1,0:T(4,128)(2,1)S(1)}, u32[]{:S(2)}, u32[]{:S(2)}) collective-permute-start(bf16[3,128]{1,0:T(4,128)(2,1)S(1)} %slice.156), channel_id=1, source_target_pairs={{0,8},{8,16},{16,24},{24,32},{32,40},{40,48},{48,56},{56,64},{64,7... | collective-permute-start | bytes 2312 | tf_op jit(solution)/shard_map/ppermute | solution.py:17
  192.6 7.1 %copy-start.2 = (bf16[4,128,8,64]{1,0,3,2:T(4,128)(2,1)S(1)}, bf16[4,128,8,64]{1,0,3,2:T(4,128)(2,1)}, u32[]{:S(2)}) copy-start(bf16[4,128,8,64]{1,0,3,2:T(4,128)(2,1)} %copy-done.1) | copy-start | bytes 1572868
  196.6 3.1 copy-start.5
  196.6 3.1 copy-start.8
  196.6 3.1 copy-start.20
  201.3 1.1 copy-start.27
  205.3 40.7 %all-to-all-start = ((bf16[8,512,256]{2,1,0:T(8,128)(2,1)}), bf16[8,512,256]{2,1,0:T(8,128)(2,1)}, u32[]{:S(2)}, u32[]{:S(2)}) async-start(bf16[8,512,256]{2,1,0:T(8,128)(2,1)} %bitcast.210), calls=%async_computation | async-start | bytes 4194304 | tf_op jit(solution)/shard_map/all_to_all | solution.py:71
  250.7 5.3 %copy-start.23 = (bf16[2048]{0:T(1024)(128)(2,1)S(1)}, bf16[2048]{0:T(1024)(128)(2,1)}, u32[]{:S(2)}) copy-start(bf16[2048]{0:T(1024)(128)(2,1)} %param.36) | copy-start | bytes 12292
  250.7 31.7 %all-to-all-start.1 = ((bf16[8,512,256]{1,2,0:T(8,128)(2,1)}), bf16[8,512,256]{1,2,0:T(8,128)(2,1)}, u32[]{:S(2)}, u32[]{:S(2)}) async-start(bf16[8,512,256]{1,2,0:T(8,128)(2,1)} %broadcast_in_dim.25), calls=%async_computation.1 | async-start | bytes 4194304 | tf_op jit(solution)/shard_map/all_to_all | solution.py:83
Sparse Core Ops, SparseCore 0:
  50.6 73.1 all-gather.6
  125.5 126.2 all-gather.4
where the time goes:
time: 343 us; the launch traced here: 341 us
  waiting for transfers between devices  114 us (33%)
  other arithmetic  52.4 us (15%)
  starting transfers between devices  39.5 us (12%)
  loops' own time  38.9 us (11%)
  local copies, waits for them, and re-layouts  30.2 us (9%)
  blocking collectives  29.6 us (9%)
  matrix products  19.5 us (6%)
  between operations  16.6 us (5%)
    all_gather x1, waiting for transfers between devices, all_in_one(): both, at, found = (lax.all_gather(jnp.concatenate(lines), axis), 0, {})  61.6 us
    another operation x1, loops' own time, prefix(): return lax.fori_loop(0, peers, step, start)  38.8 us
    all_to_all x1, blocking collectives, sum_at_owner(): lax.all_to_all(cut_along(value, dim, peers), axis, 0, 0, tiled=True)  29.6 us
    all_to_all x1, waiting for transfers between devices, sent_to_all(): lax.all_to_all(jnp.broadcast_to(value[None], (peers, *value.shape)), axis...  26.4 us
    all_to_all x1, waiting for transfers between devices, sum_at_owner(): lax.all_to_all(cut_along(value, dim, peers), axis, 0, 0, tiled=True)  26.3 us
    ppermute x4, starting transfers between devices, from_behind(): return lax.ppermute(value, axis, pairs)  19.7 us
    select_n x16, other arithmetic, step(): return jax.tree.map(lambda a, b: jnp.where(reached, a, b), new, before)  16.2 us
    all_to_all x1, starting transfers between devices, sum_at_owner(): lax.all_to_all(cut_along(value, dim, peers), axis, 0, 0, tiled=True)  14.4 us
  transfers between devices with their start and end apart: 8, of which 3 were waited for; matrix products, arithmetic and copies ran while one was open for 22% of the time, Pallas kernels for 0%

commit v1 on v0

--- a/solution.py
+++ b/solution.py
@@ -17,47 +17,17 @@
     return lax.ppermute(value, axis, pairs)
 
 
-def all_in_one(value, axis):
-    leaves = jax.tree.leaves(value)
-    turns = sorted(range(len(leaves)), key=lambda k: -leaves[k].size)
-    width = (1, *leaves[turns[0]].shape)[-1]
-    lines = [
-        jnp.pad(leaves[k].reshape(-1), (0, -leaves[k].size % width)).reshape(-1, width)
-        for k in turns
-    ]
-    both, at, found = (lax.all_gather(jnp.concatenate(lines), axis), 0, {})
-    for k, line in zip(turns, lines):
-        section = both[:, at : at + len(line)].reshape(len(both), -1)
-        found[k] = section[:, : leaves[k].size].reshape(-1, *leaves[k].shape)
-        at += len(line)
-    numbers = iter(range(len(leaves)))
-    return jax.tree.map(lambda _: found[next(numbers)], value)
-
-
-def prefix(value, axis, combine, identity):
-    peers, index = (lax.axis_size(axis), lax.axis_index(axis))
-    everything = all_in_one(
-        jax.tree.map(
-            lambda part, kind: part.astype(kind),
-            value,
-            (jnp.bfloat16, jnp.bfloat16, jnp.bfloat16, jnp.bfloat16),
-        ),
-        axis,
-    )
-    start = jax.tree.map(
-        lambda part, zero: jnp.broadcast_to(jnp.asarray(zero, part.dtype), part.shape),
-        value,
-        identity,
-    )
-
-    def step(k, before):
-        reached = k < index
-        new = combine(
-            before, jax.tree.map(lambda part, own: part[k].astype(own.dtype), everything, value)
-        )
-        return jax.tree.map(lambda a, b: jnp.where(reached, a, b), new, before)
-
-    return lax.fori_loop(0, peers, step, start)
+def state_behind(final, decay, axis):
+    shape = final.shape
+    rows = final.reshape(-1, shape[-1])
+    tail = jnp.broadcast_to(decay.reshape(-1, 1), (decay.size, shape[-1]))
+    packed = jnp.concatenate([rows, tail]).astype(jnp.bfloat16)
+    first = from_behind(packed, axis, 1).astype(jnp.float32)
+    near = first[: len(rows)].reshape(shape)
+    near_decay = first[len(rows) :, 0].reshape(decay.shape)
+    two = (final + decay[..., None, None] * near).astype(jnp.bfloat16)
+    far = from_behind(two, axis, 2).astype(jnp.float32)
+    return near + near_decay[..., None, None] * far
 
 
 def cut_along(value, dim, peers):
@@ -173,21 +143,6 @@
     reach = jnp.exp(running) * alive[None, None]
     taken = jnp.einsum("kign,kgepn->kigep", read_blocks, entering)
     return taken * jnp.transpose(reach, (2, 3, 0, 1))[..., None]
-
-
-def join_states(earlier, later):
-    early_decay, early_state, early_first, early_last = earlier
-    late_decay, late_state, late_first, late_last = later
-    link = ((late_first == early_last) | (early_last < 0.0) | (late_first < 0.0)).astype(
-        jnp.float32
-    )
-    carried = late_decay * link
-    return (
-        early_decay * carried,
-        late_state + carried[..., None, None] * early_state,
-        jnp.where(early_first < 0.0, late_first, early_first),
-        jnp.where(late_last < 0.0, early_last, late_last),
-    )
 
 
 def down_product(hidden, rows):
@@ -218,21 +173,28 @@
 ):
     tokens = values.shape[0]
     edge = taps_values.shape[0] - 1
+    late_weights = in_one_piece((gate_weight, up_weight, down_rows), "sp", 0, 1)
     segment = documents.astype(jnp.float32)
-    before = from_behind(
-        (
+    last_rows = jnp.concatenate(
+        [
             values[tokens - edge :],
             writes[tokens - edge :],
             reads[tokens - edge :],
-            segment[tokens - edge :].astype(jnp.bfloat16),
-        ),
-        "sp",
-        1,
-    )
-    row_docs = jnp.concatenate([before[3].astype(jnp.float32), segment])
-    short_values = short_filter(jnp.concatenate([before[0], values]), row_docs, taps_values)
-    short_writes = short_filter(jnp.concatenate([before[1], writes]), row_docs, taps_write)
-    short_reads = short_filter(jnp.concatenate([before[2], reads]), row_docs, taps_read)
+            jnp.broadcast_to(segment[tokens - edge :, None].astype(jnp.bfloat16), (edge, 128)),
+        ],
+        axis=1,
+    )
+    before = from_behind(last_rows, "sp", 1)
+    wide, narrow = values.shape[1], writes.shape[1]
+    before_values = before[:, :wide]
+    before_writes = before[:, wide : wide + narrow]
+    before_reads = before[:, wide + narrow : wide + 2 * narrow]
+    before_docs = before[:, wide + 2 * narrow].astype(jnp.float32)
+    before_docs = jnp.where(lax.axis_index("sp") == 0, -1.0, before_docs)
+    row_docs = jnp.concatenate([before_docs, segment])
+    short_values = short_filter(jnp.concatenate([before_values, values]), row_docs, taps_values)
+    short_writes = short_filter(jnp.concatenate([before_writes, writes]), row_docs, taps_write)
+    short_reads = short_filter(jnp.concatenate([before_reads, reads]), row_docs, taps_read)
     step_size = jax.nn.softplus(step_raw.astype(jnp.float32))
     log_decay = decay_jump - decay_rate[:, None] * step_size
     heads_per = HEADS // GROUPS
@@ -245,18 +207,12 @@
     entering, final = carry_states(
         states, block_passing(last_total, block_docs, local_prior), zero_state
     )
-    whole_decay = jnp.exp(jnp.sum(last_total, axis=2)) * (segment[0] == segment[-1]).astype(
+    behind_doc = before_docs[edge - 1 :]
+    whole_decay = jnp.exp(jnp.sum(last_total, axis=2)) * (behind_doc[0] == segment[-1]).astype(
         jnp.float32
     )
-    identity = (
-        jnp.ones_like(whole_decay),
-        zero_state,
-        jnp.full((1,), -1.0, jnp.float32),
-        jnp.full((1,), -1.0, jnp.float32),
-    )
-    scanned = prefix((whole_decay, final, segment[:1], segment[-1:]), "sp", join_states, identity)
-    held = scanned[1]
-    prior_docs = jnp.concatenate([scanned[3], block_docs[:-1, -1]])
+    held = state_behind(final, whole_decay, "sp")
+    prior_docs = jnp.concatenate([behind_doc, block_docs[:-1, -1]])
     passing_in = block_passing(last_total, block_docs, prior_docs)
     gains = jnp.cumprod(passing_in, axis=2)
     gains = jnp.concatenate([jnp.ones_like(gains[..., :1]), gains[..., :-1]], axis=2)
@@ -279,7 +235,6 @@
         jnp.mean(after_wide * after_wide, axis=1, keepdims=True) + norm_eps
     )
     normal = (normal * channel_gain.astype(jnp.float32)[None, :]).astype(jnp.bfloat16)
-    late_weights = in_one_piece((gate_weight, up_weight, down_rows), "sp", 0, 1)
     gate = jnp.dot(normal, late_weights[0], preferred_element_type=jnp.float32)
     up = jnp.dot(normal, late_weights[1], preferred_element_type=jnp.float32)
     hidden = (jax.nn.silu(gate) * up).astype(jnp.bfloat16)

time: 343 us -> 220 us (0.64)
  waiting for transfers between devices: 114 us -> 58 us
  loops' own time: 38.9 us -> 0.07 us
  other arithmetic: 52.4 us -> 35.5 us
  local copies, waits for them, and re-layouts: 30.2 us -> 19.5 us
  blocking collectives: 29.6 us -> 33.3 us
    all_gather x1 -> x0, waiting for transfers between devices: 61.6 us -> none  [all_in_one(): both, at, found = (lax.all_gather(jnp.concatenate(lines), axis), 0, {})]
    another operation x1 -> x0, loops' own time: 38.8 us -> none  [prefix(): return lax.fori_loop(0, peers, step, start)]
    select_n x16 -> x2, other arithmetic: 16.2 us -> 1.27 us  [on_device(): before_docs = jnp.where(lax.axis_index('sp') == 0, -1.0, before_docs)]
    dynamic_slice x16 -> x0, local copies, waits for them, and re-layouts: 9.43 us -> none  [step(): part[k].astype(own.dtype)]
    ppermute x4 -> x3, waiting for transfers between devices: 0.01 us -> 5.14 us  [from_behind(): return lax.ppermute(value, axis, pairs)]
    all_to_all x1, blocking collectives: 29.6 us -> 33.3 us  [sum_at_owner(): lax.all_to_all(cut_along(value, dim, peers), axis, 0, 0, tiled=True)]
    ppermute x4 -> x3, starting transfers between devices: 19.7 us -> 18.4 us  [from_behind(): return lax.ppermute(value, axis, pairs)]
  transfers between devices with their start and end apart: 8 -> 6, of which waited for: 3 -> 3; matrix products, arithmetic and copies ran while one was open for 22% -> 25% of each run, Pallas kernels for 0% -> 0%
where the time goes in v1:
time: 220 us; the launch traced here: 219 us
  waiting for transfers between devices  58 us (26%)
  starting transfers between devices  38.8 us (18%)
  other arithmetic  35.5 us (16%)
  blocking collectives  33.3 us (15%)
  local copies, waits for them, and re-layouts  19.5 us (9%)
  matrix products  18.2 us (8%)
  between operations  15.2 us (7%)
    all_to_all x1, blocking collectives, sum_at_owner(): lax.all_to_all(cut_along(value, dim, peers), axis, 0, 0, tiled=True)  33.3 us
    all_to_all x1, waiting for transfers between devices, sum_at_owner(): lax.all_to_all(cut_along(value, dim, peers), axis, 0, 0, tiled=True)  26.4 us
    all_to_all x1, waiting for transfers between devices, sent_to_all(): lax.all_to_all(jnp.broadcast_to(value[None], (peers, *value.shape)), axis...  26.4 us
    ppermute x3, starting transfers between devices, from_behind(): return lax.ppermute(value, axis, pairs)  18.4 us
    all_to_all x1, starting transfers between devices, sum_at_owner(): lax.all_to_all(cut_along(value, dim, peers), axis, 0, 0, tiled=True)  15 us
    dot_general x1, matrix products, down_product(): lax.dot_general(hidden, rows, (((1,), (1,)), ((), ())), preferred_element...  8.48 us
    all_to_all x1, starting transfers between devices, sent_to_all(): lax.all_to_all(jnp.broadcast_to(value[None], (peers, *value.shape)), axis...  5.36 us
    dot_general x1, matrix products, on_device(): gate = jnp.dot(normal, late_weights[0], preferred_element_type=jnp.float32)  5.24 us
  transfers between devices with their start and end apart: 6, of which 3 were waited for; matrix products, arithmetic and copies ran while one was open for 25% of the time, Pallas kernels for 0%

profile of v1, /device:TPU:33, one launch (start us, length us, event | category | flops | bytes accessed | tf_op | source)
XLA Modules:
  0.0 218.6 jit_solution(1482210887745309485)
XLA Ops:
  6.6 2.1 pad_maximum_fusion
  8.8 0.7 slice.143
  9.5 0.7 slice.144
  10.2 0.7 slice.142
  11.8 0.9 copy.63
  12.6 5.9 %collective-permute-start = (bf16[3,896]{0,1:T(8,128)(2,1)}, bf16[3,896]{0,1:T(8,128)(2,1)}, u32[]{:S(2)}, u32[]{:S(2)}) collective-permute-start(bf16[3,896]{0,1:T(8,128)(2,1)} %copy.63), channel_id=1, source_target_pairs={{0,8},{8,16},{16,24},{24,32},{32,40},{40,48},{48,56},{56,64},{64,7... | collective-permute-start | bytes 16136 | tf_op jit(solution)/shard_map/ppermute | solution.py:17
  18.6 1.3 fusion.50
  19.9 1.1 reduce_window_sum.11
  21.3 0.8 slice_reduce_fusion
  22.1 1.4 bitcast_convert_fusion.3
  23.5 1.4 bitcast_convert_fusion.7
  24.9 0.8 slice_convert_fusion.3
  25.7 0.8 compare_and_fusion
  28.1 2.0 copy.76
  32.6 1.3 compare_convert_fusion.1
  35.2 0.8 fusion.58
  37.3 0.9 slice.186
  39.0 1.3 multiply_convert_fusion.4
  40.5 1.6 multiply_convert_fusion.6
  42.1 0.9 multiply_convert_fusion.3
  44.1 6.0 %while.13 = (s32[]{:T(128)}, f32[1,8,64,128]{3,2,1,0:T(8,128)S(1)}, f32[4,1,8,64,128]{4,3,2,1,0:T(8,128)}, f32[4,1,8]{2,1,0:T(1,128)}, f32[4,1,8,64,128]{4,3,2,1,0:T(8,128)S(1)}, /*index=5*/s32[]{:T(128)}, s32[]{:T(128)}) while((s32[]{:T(128)}, f32[1,8,64,128]{3,2,1,0:T(8,128)S(1)}, f32[4,1,8,64,128]{4,3,2,1,0:T(8,128)}, ...), condition=%wide.region_2.3_spmd.clone, body=%wide.region_1.2_spmd.clone.sunk | while | flops 262147 | bytes 1310924 | solution.py:134
  44.7 0.7 bitcast_dynamic-update-slice_fusion.2
  46.2 0.7 bitcast_dynamic-update-slice_fusion.2
  47.7 0.7 bitcast_dynamic-update-slice_fusion.2
  49.3 0.7 bitcast_dynamic-update-slice_fusion.2
  50.9 3.7 %collective-permute-start.1 = (bf16[520,128]{0,1:T(8,128)(2,1)S(1)}, bf16[520,128]{0,1:T(8,128)(2,1)S(1)}, u32[]{:S(2)}, u32[]{:S(2)}) collective-permute-start(bf16[520,128]{0,1:T(8,128)(2,1)S(1)} %pad_maximum_fusion.2), channel_id=1, source_target_pairs={{0,8},{8,16},{16,24},{24,32},{32,40},{40,48},{48,56},{56,64},{64,7... | collective-permute-start | bytes 399368 | tf_op jit(solution)/shard_map/ppermute | solution.py:17
  54.7 1.5 multiply_convert_fusion.7
  56.2 0.9 fusion.59
  57.1 0.7 reduce_window.9
  58.1 8.7 %collective-permute-start.2 = (bf16[1,8,64,128]{3,2,1,0:T(8,128)(2,1)S(1)}, bf16[1,8,64,128]{3,2,1,0:T(8,128)(2,1)S(1)}, u32[]{:S(2)}, u32[]{:S(2)}) collective-permute-start(bf16[1,8,64,128]{3,2,1,0:T(8,128)(2,1)S(1)} %add_convert_fusion.2), channel_id=1, source_target_pairs={{0,16},{8,24},{16,32},{24,40},{32,48},{40,56},{48,64},{56,72},{64,... | collective-permute-start | bytes 393224 | tf_op jit(solution)/shard_map/ppermute | solution.py:17
  66.9 5.1 %collective-permute-done.2 = bf16[1,8,64,128]{3,2,1,0:T(8,128)(2,1)S(1)} collective-permute-done((bf16[1,8,64,128]{3,2,1,0:T(8,128)(2,1)S(1)}, bf16[1,8,64,128]{3,2,1,0:T(8,128)(2,1)S(1)}, u32[]{:S(2)}, u32[]{:S(2)}) %collective-permute-start.2) | collective-permute-done | bytes 131104 | tf_op jit(solution)/shard_map/ppermute | solution.py:17
  72.5 1.5 fusion.14
  75.5 1.4 convolution_convert_fusion.1
  76.9 1.5 copy.98
  78.4 15.0 %all-to-all-start = ((bf16[8,512,256]{2,1,0:T(8,128)(2,1)}), bf16[8,512,256]{2,1,0:T(8,128)(2,1)}, u32[]{:S(2)}, u32[]{:S(2)}) async-start(bf16[8,512,256]{2,1,0:T(8,128)(2,1)} %bitcast.155), calls=%async_computation | async-start | bytes 4194304 | tf_op jit(solution)/shard_map/all_to_all | solution.py:41
  93.4 26.4 %all-to-all-done = bf16[8,512,256]{2,1,0:T(8,128)(2,1)} async-done(((bf16[8,512,256]{2,1,0:T(8,128)(2,1)}), bf16[8,512,256]{2,1,0:T(8,128)(2,1)}, u32[]{:S(2)}, u32[]{:S(2)}) %all-to-all-start) | async-done | bytes 2097184 | tf_op jit(solution)/shard_map/all_to_all | solution.py:41
  119.8 1.9 convert_reduce_fusion.1
  121.7 1.0 add_convert_fusion.1
  122.9 1.6 broadcast_in_dim.32
  124.5 5.4 %all-to-all-start.1 = ((bf16[8,512,256]{1,2,0:T(8,128)(2,1)}), bf16[8,512,256]{1,2,0:T(8,128)(2,1)}, u32[]{:S(2)}, u32[]{:S(2)}) async-start(bf16[8,512,256]{1,2,0:T(8,128)(2,1)} %broadcast_in_dim.32), calls=%async_computation.1 | async-start | bytes 4194304 | tf_op jit(solution)/shard_map/all_to_all | solution.py:53
  129.8 26.4 %all-to-all-done.1 = bf16[8,512,256]{1,2,0:T(8,128)(2,1)} async-done(((bf16[8,512,256]{1,2,0:T(8,128)(2,1)}), bf16[8,512,256]{1,2,0:T(8,128)(2,1)}, u32[]{:S(2)}, u32[]{:S(2)}) %all-to-all-start.1) | async-done | bytes 2097184 | tf_op jit(solution)/shard_map/all_to_all | solution.py:53
  156.2 2.1 multiply_reduce_fusion
  158.3 3.5 %fusion.2 = bf16[512,2048]{0,1:T(8,128)(2,1)} fusion(f32[2048]{0:T(1024)S(1)} %convert_element_type.265, f32[512]{0:T(512)S(1)} %add_rsqrt_fusion, bf16[8,512,256]{1,2,0:T(8,128)(2,1)} %all-to-all-done.1), kind=kLoop, calls=%fused_computation.6 | loop fusion | flops 4194304 | bytes 4204544 | tf_op jit(solution)/shard_map/convert_element_type | solution.py:237
  161.8 5.2 %fusion.6 = f32[512,704]{0,1:T(8,128)} fusion(bf16[512,2048]{0,1:T(8,128)(2,1)} %fusion.2, bf16[2048,2112]{0,1:T(8,128)(2,1)} %all-gather.2.cloned.1.call-done), kind=kOutput, calls=%fused_computation.15 | convolution fusion | flops 1476395008 | bytes 6422528 | tf_op jit(solution)/shard_map/dot_general | solution.py:238
  167.1 8.5 %convolution_convert_fusion = bf16[512,2048]{1,0:T(8,128)(2,1)} fusion(bf16[2048,2112]{0,1:T(8,128)(2,1)} %all-gather.2.cloned.1.call-done, bf16[512,2048]{0,1:T(8,128)(2,1)} %fusion.2, f32[512,704]{0,1:T(8,128)} %fusion.6), kind=kOutput, calls=%fused_computation.10 | convolution fusion | flops 2956001280 | bytes 11403264 | tf_op jit(solution)/shard_map/dot_general | solution.py:149
  175.6 1.7 copy.97
  177.3 33.3 %all_to_all.15 = bf16[8,512,256]{2,1,0:T(8,128)(2,1)S(1)} all-to-all(bf16[8,512,256]{2,1,0:T(8,128)(2,1)S(1)} %bitcast.156), channel_id=1, replica_groups=mesh['grp'=2,'sp'=16,'tp'=8] {'tp'}, dimensions={0} | all-to-all | bytes 4194304 | tf_op jit(solution)/shard_map/all_to_all | solution.py:41
  210.9 0.8 add_convert_fusion
  (102 shorter events, 14.8 us)
Async XLA Ops:
  6.5 68.9 %copy-start = (bf16[512,2048]{1,0:T(8,128)(2,1)S(1)}, bf16[512,2048]{1,0:T(8,128)(2,1)}, u32[]{:S(2)}) copy-start(bf16[512,2048]{1,0:T(8,128)(2,1)} %param.33) | copy-start | bytes 6291460
  6.6 20.1 %copy-start.5 = (bf16[512,512]{1,0:T(8,128)(2,1)S(1)}, bf16[512,512]{1,0:T(8,128)(2,1)}, u32[]{:S(2)}) copy-start(bf16[512,512]{1,0:T(8,128)(2,1)} %param.21) | copy-start | bytes 1572868
  6.6 27.4 %copy-start.14 = (s32[512]{0:T(512)S(1)}, s32[512]{0:T(512)}, u32[]{:S(2)}) copy-start(s32[512]{0:T(512)} %param.28) | copy-start | bytes 6148
  6.6 27.5 %copy-start.13 = (bf16[8,512]{1,0:T(8,128)(2,1)S(1)}, bf16[8,512]{1,0:T(8,128)(2,1)}, u32[]{:S(2)}) copy-start(bf16[8,512]{1,0:T(8,128)(2,1)} %param.25) | copy-start | bytes 24580
  6.6 20.4 %copy-start.21 = (bf16[512]{0:T(512)(128)(2,1)S(1)}, bf16[512]{0:T(512)(128)(2,1)}, u32[]{:S(2)}) copy-start(bf16[512]{0:T(512)(128)(2,1)} %param.32) | copy-start | bytes 3076
  6.6 155.3 %all-gather.2.cloned.1.call-start = ((), (), s32[]{:S(2)}) async-start(), calls=%async_computation.3 | async-start | bytes 9191424 | tf_op jit(solution)/shard_map/all_gather | solution.py:64
  12.6 17.5 %collective-permute-start = (bf16[3,896]{0,1:T(8,128)(2,1)}, bf16[3,896]{0,1:T(8,128)(2,1)}, u32[]{:S(2)}, u32[]{:S(2)}) collective-permute-start(bf16[3,896]{0,1:T(8,128)(2,1)} %copy.63), channel_id=1, source_target_pairs={{0,8},{8,16},{16,24},{24,32},{32,40},{40,48},{48,56},{56,64},{64,7... | collective-permute-start | bytes 16136 | tf_op jit(solution)/shard_map/ppermute | solution.py:17
  39.0 1.5 copy-start.9
  39.0 1.5 copy-start.10
  39.0 1.5 copy-start.11
  39.0 1.5 copy-start.12
  40.4 2.6 %copy-start.2 = (bf16[4,128,8,64]{1,0,3,2:T(4,128)(2,1)}, bf16[4,128,8,64]{1,0,3,2:T(4,128)(2,1)S(1)}, u32[]{:S(2)}) copy-start(bf16[4,128,8,64]{1,0,3,2:T(4,128)(2,1)S(1)} %reshape.383) | copy-start | bytes 1572868
  40.4 2.9 %copy-start.16 = (f32[8,4]{0,1:T(4,128)S(1)}, f32[8,4]{0,1:T(4,128)}, u32[]{:S(2)}) copy-start(f32[8,4]{0,1:T(4,128)} %get-tuple-element.75) | copy-start | bytes 388
  40.5 2.9 %copy-start.18 = (f32[4]{0:T(128)S(1)}, f32[4]{0:T(128)}, u32[]{:S(2)}) copy-start(f32[4]{0:T(128)} %get-tuple-element.86) | copy-start | bytes 52
  40.5 2.9 %copy-start.19 = (f32[4]{0:T(128)S(1)}, f32[4]{0:T(128)}, u32[]{:S(2)}) copy-start(f32[4]{0:T(128)} %get-tuple-element.111) | copy-start | bytes 52
  50.1 22.0 %copy-start.7 = (f32[4,128,8]{1,2,0:T(8,128)S(1)}, f32[4,128,8]{1,2,0:T(8,128)}, u32[]{:S(2)}) copy-start(f32[4,128,8]{1,2,0:T(8,128)} %get-tuple-element.92) | copy-start | bytes 49156
  50.9 6.9 %collective-permute-start.1 = (bf16[520,128]{0,1:T(8,128)(2,1)S(1)}, bf16[520,128]{0,1:T(8,128)(2,1)S(1)}, u32[]{:S(2)}, u32[]{:S(2)}) collective-permute-start(bf16[520,128]{0,1:T(8,128)(2,1)S(1)} %pad_maximum_fusion.2), channel_id=1, source_target_pairs={{0,8},{8,16},{16,24},{24,32},{32,40},{40,48},{48,56},{56,64},{64,7... | collective-permute-start | bytes 399368 | tf_op jit(solution)/shard_map/ppermute | solution.py:17
  57.9 14.2 %copy-start.4 = (f32[4,1,8,64,128]{4,3,2,1,0:T(8,128)S(1)}, f32[4,1,8,64,128]{4,3,2,1,0:T(8,128)}, u32[]{:S(2)}) copy-start(f32[4,1,8,64,128]{4,3,2,1,0:T(8,128)} %get-tuple-element.33) | copy-start | bytes 3145732
  58.0 14.5 %copy-start.3 = (bf16[4,128,8,64]{1,0,3,2:T(4,128)(2,1)S(1)}, bf16[4,128,8,64]{1,0,3,2:T(4,128)(2,1)}, u32[]{:S(2)}) copy-start(bf16[4,128,8,64]{1,0,3,2:T(4,128)(2,1)} %copy-done.2) | copy-start | bytes 1572868
  58.0 14.5 %copy-start.6 = (f32[4,128,128]{2,1,0:T(8,128)S(1)}, f32[4,128,128]{2,1,0:T(8,128)}, u32[]{:S(2)}) copy-start(f32[4,128,128]{2,1,0:T(8,128)} %fusion.59) | copy-start | bytes 786436
  58.0 14.5 %copy-start.8 = (pred[4,128,128]{2,1,0:T(8,128)(4,1)S(1)}, pred[4,128,128]{2,1,0:T(8,128)(4,1)}, u32[]{:S(2)}) copy-start(pred[4,128,128]{2,1,0:T(8,128)(4,1)} %compare_and_fusion) | copy-start | bytes 196612
  58.0 14.5 %copy-start.15 = (f32[8,4,128]{2,0,1:T(8,128)S(1)}, f32[8,4,128]{2,0,1:T(8,128)}, u32[]{:S(2)}) copy-start(f32[8,4,128]{2,0,1:T(8,128)} %get-tuple-element.94) | copy-start | bytes 49156
  58.1 13.9 %collective-permute-start.2 = (bf16[1,8,64,128]{3,2,1,0:T(8,128)(2,1)S(1)}, bf16[1,8,64,128]{3,2,1,0:T(8,128)(2,1)S(1)}, u32[]{:S(2)}, u32[]{:S(2)}) collective-permute-start(bf16[1,8,64,128]{3,2,1,0:T(8,128)(2,1)S(1)} %add_convert_fusion.2), channel_id=1, source_target_pairs={{0,16},{8,24},{16,32},{24,40},{32,48},{40,56},{48,64},{56,72},{64,... | collective-permute-start | bytes 393224 | tf_op jit(solution)/shard_map/ppermute | solution.py:17
  74.0 1.1 copy-start.1
  74.0 1.4 copy-start.20
  78.4 41.4 %all-to-all-start = ((bf16[8,512,256]{2,1,0:T(8,128)(2,1)}), bf16[8,512,256]{2,1,0:T(8,128)(2,1)}, u32[]{:S(2)}, u32[]{:S(2)}) async-start(bf16[8,512,256]{2,1,0:T(8,128)(2,1)} %bitcast.155), calls=%async_computation | async-start | bytes 4194304 | tf_op jit(solution)/shard_map/all_to_all | solution.py:41
  124.5 5.4 %copy-start.17 = (bf16[2048]{0:T(1024)(128)(2,1)S(1)}, bf16[2048]{0:T(1024)(128)(2,1)}, u32[]{:S(2)}) copy-start(bf16[2048]{0:T(1024)(128)(2,1)} %param.34) | copy-start | bytes 12292
  124.5 31.8 %all-to-all-start.1 = ((bf16[8,512,256]{1,2,0:T(8,128)(2,1)}), bf16[8,512,256]{1,2,0:T(8,128)(2,1)}, u32[]{:S(2)}, u32[]{:S(2)}) async-start(bf16[8,512,256]{1,2,0:T(8,128)(2,1)} %broadcast_in_dim.32), calls=%async_computation.1 | async-start | bytes 4194304 | tf_op jit(solution)/shard_map/all_to_all | solution.py:53
Sparse Core Ops, SparseCore 0:
  9.1 143.5 all-gather.1

commit v2 on v1

v2 whole, which is shorter than its diff:
```python
import functools

import jax
import jax.numpy as jnp
from jax import lax
from jax.experimental import pallas as pl
from jax.experimental.pallas import tpu as pltpu
from jax.sharding import PartitionSpec as P

HEADS = 64
GROUPS = 8
BLOCK = 128
EDGE = 16
LANES = 128

norm_eps = 1e-06

F32 = jnp.float32
BF16 = jnp.bfloat16


def from_behind(value, axis, by):
    peers = lax.axis_size(axis)
    pairs = [(i, i + by) for i in range(peers) if 0 <= i + by < peers]
    return lax.ppermute(value, axis, pairs)


def silu(x):
    return x * jax.nn.sigmoid(x)


def shape(dims, kind):
    return jax.ShapeDtypeStruct(dims, kind)


def transposed(rows):
    return jnp.transpose(rows, (1, 0))


def doc_rows(docs_ref):
    return docs_ref[...].astype(F32)


def running_sum(x):
    lane = lax.broadcasted_iota(jnp.int32, x.shape, 1)
    shift = 1
    while shift < x.shape[1]:
        x = x + jnp.where(lane >= shift, pltpu.roll(x, shift, 1), 0.0)
        shift *= 2
    return x


def per_channel(columns, pair, rows):
    lane = lax.broadcasted_iota(jnp.int32, (rows, LANES), 1)
    return jnp.where(
        lane < LANES // 2,
        jnp.broadcast_to(columns[:, 2 * pair : 2 * pair + 1], (rows, LANES)),
        jnp.broadcast_to(columns[:, 2 * pair + 1 : 2 * pair + 2], (rows, LANES)),
    )


def place_docs(dext_ref, prior_ref, docs, blocks):
    dext_ref[0:EDGE] = prior_ref[...].astype(F32)
    padded = jnp.concatenate([docs, jnp.zeros((8 - blocks, BLOCK), F32)]) if blocks < 8 else docs
    columns = transposed(padded)
    for b in range(blocks):
        dext_ref[EDGE + b * BLOCK : EDGE + (b + 1) * BLOCK] = jnp.broadcast_to(
            columns[:, b : b + 1], (BLOCK, LANES)
        )


def short_filter(ext_ref, dext_ref, taps_ref, out_ref, blocks, width):
    taps = taps_ref[...].astype(F32)
    count = taps.shape[0]
    for b in range(blocks):
        first = EDGE + b * BLOCK
        own = dext_ref[first : first + BLOCK]
        masks = [
            dext_ref[first - count + 1 + k : first - count + 1 + k + BLOCK] == own
            for k in range(count - 1)
        ]
        for c in range(width // LANES):
            cols = slice(c * LANES, (c + 1) * LANES)
            total = None
            for k in range(count):
                start = first - count + 1 + k
                term = ext_ref[start : start + BLOCK, cols] * taps[k : k + 1, cols]
                if k < count - 1:
                    term = jnp.where(masks[k], term, 0.0)
                total = term if total is None else total + term
            out_ref[b * BLOCK : (b + 1) * BLOCK, cols] = silu(total).astype(BF16)


def pack_kernel(values_ref, writes_ref, reads_ref, docs_ref, out_ref):
    wide, narrow = values_ref.shape[1], writes_ref.shape[1]
    out_ref[:, 0:wide] = values_ref[...]
    out_ref[:, wide : wide + narrow] = writes_ref[...]
    out_ref[:, wide + narrow : wide + 2 * narrow] = reads_ref[...]
    blocks = docs_ref.shape[0]
    last = jnp.broadcast_to(doc_rows(docs_ref)[blocks - 1 :], (8, BLOCK))
    column = transposed(last)[BLOCK - EDGE :, 0:1]
    out_ref[:, wide + 2 * narrow :] = jnp.broadcast_to(column, (EDGE, LANES)).astype(BF16)


def pack_edge(values, writes, reads, docs):
    tokens, wide = values.shape
    narrow = writes.shape[1]
    at = tokens // EDGE - 1
    return pl.pallas_call(
        pack_kernel,
        grid=(1,),
        in_specs=[
            pl.BlockSpec((EDGE, wide), lambda i: (at, 0)),
            pl.BlockSpec((EDGE, narrow), lambda i: (at, 0)),
            pl.BlockSpec((EDGE, narrow), lambda i: (at, 0)),
            pl.BlockSpec(docs.shape, lambda i: (0, 0)),
        ],
        out_specs=pl.BlockSpec((EDGE, wide + 2 * narrow + LANES), lambda i: (0, 0)),
        out_shape=shape((EDGE, wide + 2 * narrow + LANES), BF16),
        name="pack_edge",
    )(values, writes, reads, docs)


def state_kernel(
    before_ref,
    values_ref,
    writes_ref,
    step_ref,
    rate_ref,
    jump_ref,
    docs_ref,
    taps_values_ref,
    taps_write_ref,
    sv_ref,
    sw_ref,
    run_ref,
    stepped_ref,
    enter_ref,
    send_ref,
    ext_ref,
    wext_ref,
    dext_ref,
):
    tokens, wide = values_ref.shape
    narrow = writes_ref.shape[1]
    blocks = tokens // BLOCK
    heads = step_ref.shape[0]
    docs = doc_rows(docs_ref)
    place_docs(dext_ref, before_ref.at[:, wide + 2 * narrow :], docs, blocks)
    ext_ref[0:EDGE] = before_ref[:, 0:wide].astype(F32)
    ext_ref[EDGE:] = values_ref[...].astype(F32)
    wext_ref[0:EDGE] = before_ref[:, wide : wide + narrow].astype(F32)
    wext_ref[EDGE:] = writes_ref[...].astype(F32)
    short_filter(wext_ref, dext_ref, taps_write_ref, sw_ref, blocks, narrow)
    short_filter(ext_ref, dext_ref, taps_values_ref, sv_ref, blocks, wide)

    raw = step_ref[...].astype(F32)
    step = jnp.maximum(raw, 0.0) + jnp.log1p(jnp.exp(-jnp.abs(raw)))
    stepped_ref[...] = step
    log_decay = jump_ref[...] - rate_ref[...] * step
    held = None
    total = jnp.zeros((heads, 1), F32)
    head_size = wide // heads
    for b in range(blocks):
        span = slice(b * BLOCK, (b + 1) * BLOCK)
        run = running_sum(log_decay[:, span])
        run_ref[:, span] = run
        last = run[:, BLOCK - 1 :]
        total = total + last
        row = docs[b : b + 1]
        end = row[:, BLOCK - 1 :]
        factor = jnp.where(row == end, jnp.exp(last - run) * step[:, span], 0.0)
        columns = transposed(factor)
        scaled = jnp.concatenate(
            [
                (
                    sv_ref[span, p * LANES : (p + 1) * LANES].astype(F32)
                    * per_channel(columns, p, BLOCK)
                ).astype(BF16)
                for p in range(wide // LANES)
            ],
            axis=1,
        )
        fresh = lax.dot_general(
            scaled, sw_ref[span], (((0,), (0,)), ((), ())), preferred_element_type=F32
        )
        if held is None:
            held = fresh
        else:
            enter_ref[b - 1] = held.astype(BF16)
            passing = jnp.where(docs[b - 1 : b, BLOCK - 1 :] == end, jnp.exp(last), 0.0)
            held = jnp.concatenate(
                [
                    held[h * head_size : (h + 1) * head_size] * passing[h : h + 1]
                    + fresh[h * head_size : (h + 1) * head_size]
                    for h in range(heads)
                ]
            )
    send_ref[0:wide] = held.astype(BF16)
    behind = before_ref[EDGE - 1 : EDGE, wide + 2 * narrow :].astype(F32)
    whole = jnp.where(
        behind == docs[blocks - 1 :, BLOCK - 1 :], jnp.broadcast_to(jnp.exp(total), (heads, LANES)), 0.0
    )
    send_ref[wide:] = jnp.concatenate([whole, jnp.zeros((16 - heads, LANES), F32)]).astype(BF16)


def local_states(before, values, writes, step_raw, rate, jump, docs, taps_values, taps_write):
    tokens, wide = values.shape
    narrow = writes.shape[1]
    heads = step_raw.shape[0]
    blocks = tokens // BLOCK
    return pl.pallas_call(
        state_kernel,
        out_shape=(
            shape((tokens, wide), BF16),
            shape((tokens, narrow), BF16),
            shape((heads, tokens), F32),
            shape((heads, tokens), F32),
            shape((blocks - 1, wide, narrow), BF16),
            shape((wide + 16, narrow), BF16),
        ),
        scratch_shapes=[
            pltpu.VMEM((EDGE + tokens, wide), F32),
            pltpu.VMEM((EDGE + tokens, narrow), F32),
            pltpu.VMEM((EDGE + tokens, LANES), F32),
        ],
        cost_estimate=pl.CostEstimate(flops=400_000_000, transcendentals=0, bytes_accessed=4_000_000),
        name="local_states",
    )(before, values, writes, step_raw, rate, jump, docs, taps_values, taps_write)


def decayed(near, decay, far, heads):
    size = near.shape[0] // heads
    return jnp.concatenate(
        [
            near[h * size : (h + 1) * size] + decay[h : h + 1] * far[h * size : (h + 1) * size]
            for h in range(heads)
        ]
    )


def join_kernel(heads, own_ref, near_ref, out_ref):
    wide = out_ref.shape[0]
    own = own_ref[0:wide].astype(F32)
    decay = own_ref[wide:].astype(F32)
    out_ref[...] = decayed(own, decay, near_ref[0:wide].astype(F32), heads).astype(BF16)


def join_states(own, near, heads):
    return pl.pallas_call(
        functools.partial(join_kernel, heads),
        out_shape=shape((own.shape[0] - 16, own.shape[1]), BF16),
        name="join_states",
    )(own, near)


def inner_kernel(
    before_ref,
    reads_ref,
    docs_ref,
    taps_ref,
    sv_ref,
    sw_ref,
    run_ref,
    step_ref,
    enter_ref,
    sr_ref,
    mixed_ref,
    reach_ref,
    ext_ref,
    dext_ref,
):
    tokens, narrow = reads_ref.shape
    wide = sv_ref.shape[1]
    blocks = tokens // BLOCK
    heads = step_ref.shape[0]
    docs = doc_rows(docs_ref)
    place_docs(dext_ref, before_ref.at[:, wide + 2 * narrow :], docs, blocks)
    ext_ref[0:EDGE] = before_ref[:, wide + narrow : wide + 2 * narrow].astype(F32)
    ext_ref[EDGE:] = reads_ref[...].astype(F32)
    short_filter(ext_ref, dext_ref, taps_ref, sr_ref, blocks, narrow)
    target = lax.broadcasted_iota(jnp.int32, (BLOCK, BLOCK), 0)
    source = lax.broadcasted_iota(jnp.int32, (BLOCK, BLOCK), 1)
    low = source < LANES // 2
    gain = None
    for b in range(blocks):
        span = slice(b * BLOCK, (b + 1) * BLOCK)
        row = docs[b : b + 1]
        column = dext_ref[EDGE + b * BLOCK : EDGE + (b + 1) * BLOCK]
        allowed = (target >= source) & (column == row)
        reads, writes = sr_ref[span], sw_ref[span]
        scores = lax.dot_general(
            reads, writes, (((1,), (1,)), ((), ())), preferred_element_type=F32
        )
        run, step = run_ref[:, span], step_ref[:, span]
        run_columns = transposed(run)
        if b == 0:
            prior = before_ref[EDGE - 1 : EDGE, wide + 2 * narrow :].astype(F32)
        else:
            prior = jnp.broadcast_to(docs[b - 1 : b, BLOCK - 1 :], (1, BLOCK))
        reach = jnp.where(row == prior, jnp.exp(run), 0.0)
        last = run[:, BLOCK - 1 :]
        passing = jnp.where(row[:, BLOCK - 1 :] == prior[:, 0:1], jnp.exp(last), 0.0)
        reach_ref[:, span] = reach if gain is None else reach * gain
        gain = passing if gain is None else gain * passing
        reach_columns = transposed(reach)
        if b > 0:
            taken = lax.dot_general(
                reads, enter_ref[b - 1], (((1,), (1,)), ((), ())), preferred_element_type=F32
            )
        for p in range(wide // LANES):
            cols = slice(p * LANES, (p + 1) * LANES)
            weights = []
            for h in (2 * p, 2 * p + 1):
                spread = run_columns[:, h : h + 1] - run[h : h + 1]
                decay = jnp.exp(jnp.where(allowed, spread, -1e30))
                weights.append((decay * scores * step[h : h + 1]).astype(BF16))
            here = sv_ref[span, cols]
            zero = jnp.zeros_like(here)
            both = jnp.concatenate([jnp.where(low, here, zero), jnp.where(low, zero, here)])
            mixed = jnp.dot(
                jnp.concatenate(weights, axis=1), both, preferred_element_type=F32
            )
            if b > 0:
                mixed = mixed + taken[:, cols] * per_channel(reach_columns, p, BLOCK)
            mixed_ref[span, cols] = mixed


def local_mix(before, reads, docs, taps, sv, sw, run, step, enter):
    tokens, narrow = reads.shape
    wide = sv.shape[1]
    heads = step.shape[0]
    return pl.pallas_call(
        inner_kernel,
        out_shape=(
            shape((tokens, narrow), BF16),
            shape((tokens, wide), F32),
            shape((heads, tokens), F32),
        ),
        scratch_shapes=[
            pltpu.VMEM((EDGE + tokens, narrow), F32),
            pltpu.VMEM((EDGE + tokens, LANES), F32),
        ],
        cost_estimate=pl.CostEstimate(flops=800_000_000, transcendentals=0, bytes_accessed=4_000_000),
        name="local_mix",
    )(before, reads, docs, taps, sv, sw, run, step, enter)


def project_kernel(
    core_ref,
    near_ref,
    far_ref,
    sr_ref,
    mixed_ref,
    reach_ref,
    gate_ref,
    gain_ref,
    weight_ref,
    mine_ref,
    other_ref,
    in_ref,
):
    tokens, wide = mixed_ref.shape
    heads = reach_ref.shape[0]
    share = mine_ref.shape[2]
    near = near_ref[0:wide].astype(F32)
    decay = near_ref[wide:].astype(F32)
    held = decayed(near, decay, far_ref[...].astype(F32), heads).astype(BF16)
    for b in range(tokens // BLOCK):
        span = slice(b * BLOCK, (b + 1) * BLOCK)
        taken = lax.dot_general(
            sr_ref[span], held, (((1,), (1,)), ((), ())), preferred_element_type=F32
        )
        columns = transposed(reach_ref[:, span])
        parts, square = [], None
        for p in range(wide // LANES):
            cols = slice(p * LANES, (p + 1) * LANES)
            mixed = mixed_ref[span, cols] + taken[:, cols] * per_channel(columns, p, BLOCK)
            part = mixed * silu(gate_ref[span, cols].astype(F32))
            parts.append(part)
            square = part * part if square is None else square + part * part
        mean = jnp.sum(square, axis=1, keepdims=True) / wide
        scale = lax.rsqrt(mean + norm_eps)
        for p, part in enumerate(parts):
            cols = slice(p * LANES, (p + 1) * LANES)
            in_ref[span, cols] = (part * scale * gain_ref[:, cols].astype(F32)).astype(BF16)
    core = core_ref[0]
    rows = in_ref[...]
    for flip, out_ref in ((1, other_ref), (0, mine_ref)):
        for k in range(out_ref.shape[0]):
            c = 2 * k + (core ^ flip)
            cols = pl.ds(pl.multiple_of(c * share, share), share)
            out_ref[k] = jnp.dot(rows, weight_ref[:, cols], preferred_element_type=F32).astype(BF16)


def vmem():
    return pl.BlockSpec(memory_space=pltpu.VMEM)


def smem():
    return pl.BlockSpec(memory_space=pltpu.SMEM)


def project(core, near, far, sr, mixed, reach, gate, gain, weight, owners):
    tokens, wide = mixed.shape
    share = weight.shape[1] // (2 * owners)
    return pl.pallas_call(
        project_kernel,
        in_specs=[smem()] + [vmem()] * 8,
        out_shape=(shape((owners, tokens, share), BF16),) * 2,
        scratch_shapes=[pltpu.VMEM((tokens, wide), BF16)],
        cost_estimate=pl.CostEstimate(
            flops=2 * tokens * wide * weight.shape[1], transcendentals=0, bytes_accessed=6_000_000
        ),
        name="project",
    )(core, near, far, sr, mixed, reach, gate, gain, weight)


def after_kernel(at_ref, parts_ref, residual_ref, own_ref, out_ref):
    total = residual_ref[...].astype(F32)
    for k in range(parts_ref.shape[0]):
        total = total + parts_ref[k].astype(F32)
    after = total.astype(BF16)
    own_ref[...] = after
    for k in range(out_ref.shape[0]):
        out_ref[k] = after


def after_mix(at, parts, residual):
    owners, tokens, share = parts.shape
    return pl.pallas_call(
        after_kernel,
        grid_spec=pltpu.PrefetchScalarGridSpec(
            num_scalar_prefetch=1,
            grid=(1,),
            in_specs=[
                pl.BlockSpec((owners, tokens, share), lambda i, at: (0, 0, 0)),
                pl.BlockSpec((tokens, share), lambda i, at: (0, at[0])),
            ],
            out_specs=[
                pl.BlockSpec((tokens, share), lambda i, at: (0, 0)),
                pl.BlockSpec((owners, tokens, share), lambda i, at: (0, 0, 0)),
            ],
        ),
        out_shape=(shape((tokens, share), BF16), shape((owners, tokens, share), BF16)),
        name="after_mix",
    )(at, parts, residual)


def mixer_kernel(at_ref, mine_ref, other_ref, gain_ref, weight_ref, *refs):
    out_refs = refs[:2]
    after, normal, late, downs, hidden_ref, out, after_sem, late_sem, down_sem, out_sem = refs[2:]
    _, owners, tokens, share = after.shape
    peers, _, depth = weight_ref.shape
    units = hidden_ref.shape[1]
    core = at_ref[0]

    loads = [
        pltpu.make_async_copy(ref, after.at[k], after_sem.at[k])
        for k, ref in enumerate((mine_ref, other_ref))
    ]
    heavy, rows = [], []
    for k in range(peers):
        cols = pl.ds(k * depth, depth)
        heavy.append(
            pltpu.make_async_copy(
                weight_ref.at[k, pl.ds(0, 2 * units)], late.at[:, cols], late_sem.at[k]
            )
        )
        rows.append(
            pltpu.make_async_copy(
                weight_ref.at[k, pl.ds(2 * units, units)], downs.at[:, cols], down_sem.at[k]
            )
        )
    for copy in (*loads, *heavy, *rows):
        copy.start()

    for copy in loads:
        copy.wait()
    square = None
    for flip in range(2):
        for k in range(owners):
            x = after[flip, k].astype(F32)
            square = x * x if square is None else square + x * x
    scale = lax.rsqrt(jnp.sum(square, axis=1, keepdims=True) / (2 * owners * share) + norm_eps)
    for flip in range(2):
        for k in range(owners):
            c = 2 * k + (core ^ flip)
            normal[:, pl.ds(pl.multiple_of(c * share, share), share)] = (
                after[flip, k].astype(F32) * scale * gain_ref[c].astype(F32)
            ).astype(BF16)
    for copy in heavy:
        copy.wait()
    across = (((1,), (1,)), ((), ()))
    gate = lax.dot_general(normal[...], late[0:units], across, preferred_element_type=F32)
    up = lax.dot_general(normal[...], late[units:], across, preferred_element_type=F32)
    hidden_ref[...] = (silu(gate) * up).astype(BF16)
    for copy in rows:
        copy.wait()
    stores = []
    for flip in (1, 0):
        for k in range(owners):
            c = 2 * k + (core ^ flip)
            part = downs[:, pl.ds(pl.multiple_of(c * share, share), share)]
            out[flip, k] = jnp.dot(hidden_ref[...], part, preferred_element_type=F32).astype(BF16)
        store = pltpu.make_async_copy(out.at[flip], out_refs[flip], out_sem.at[flip])
        store.start()
        stores.append(store)
    for store in stores:
        store.wait()


def channel_mixer(core, mine, other, gain, weights):
    owners, tokens, share = mine.shape
    peers, units, depth = weights.shape[0], weights.shape[1] // 3, weights.shape[2]
    anywhere = pl.BlockSpec(memory_space=pl.ANY)
    out = shape((owners, tokens, share), BF16)
    return pl.pallas_call(
        mixer_kernel,
        in_specs=[smem(), anywhere, anywhere, vmem(), anywhere],
        out_specs=[anywhere, anywhere],
        out_shape=(out, out),
        scratch_shapes=[
            pltpu.VMEM((2, owners, tokens, share), BF16),
            pltpu.VMEM((tokens, peers * depth), BF16),
            pltpu.VMEM((2 * units, peers * depth), BF16),
            pltpu.VMEM((units, peers * depth), BF16),
            pltpu.VMEM((tokens, units), BF16),
            pltpu.VMEM((2, owners, tokens, share), BF16),
            pltpu.SemaphoreType.DMA((2,)),
            pltpu.SemaphoreType.DMA((peers,)),
            pltpu.SemaphoreType.DMA((peers,)),
            pltpu.SemaphoreType.DMA((2,)),
        ],
        cost_estimate=pl.CostEstimate(
            flops=12 * tokens * owners * share * units, transcendentals=0, bytes_accessed=14_000_000
        ),
        name="channel_mixer",
    )(core, mine, other, gain, weights)


def out_kernel(parts_ref, own_ref, out_ref):
    total = None
    for k in range(parts_ref.shape[0]):
        part = parts_ref[k].astype(F32)
        total = part if total is None else total + part
    out_ref[...] = (own_ref[...].astype(F32) + total).astype(BF16)


def add_down(parts, own):
    return pl.pallas_call(out_kernel, out_shape=shape(own.shape, BF16), name="add_down")(parts, own)


def to_partner(value):
    return lax.ppermute(value, "tp", [(i, i ^ 1) for i in range(lax.axis_size("tp"))])


def exchange(value):
    peers = lax.axis_size("tp")
    rows = [[i for i in range(peers) if i % 2 == core] for core in range(2)]
    return lax.all_to_all(value, "tp", 0, 0, axis_index_groups=rows, tiled=True)


def sum_pairs(both):
    return (both[0].astype(F32) + to_partner(both[1]).astype(F32)).astype(BF16)


def on_device(
    residual,
    values,
    out_gate,
    writes,
    reads,
    step_raw,
    decay_rate,
    decay_jump,
    documents,
    taps_values,
    taps_write,
    taps_read,
    mixer_gain,
    mixer_out,
    channel_gain,
    gate_weight,
    up_weight,
    down_rows,
):
    heads = step_raw.shape[0]
    owners = lax.axis_size("tp") // 2
    me = lax.axis_index("tp").astype(jnp.int32)
    at = me.reshape(1)
    core = (me % 2).reshape(1)
    late = jnp.concatenate([gate_weight.T, up_weight.T, down_rows.T], axis=0)
    weights = lax.all_gather(late, "sp", axis=0)

    docs = documents.reshape(-1, BLOCK)
    before = from_behind(pack_edge(values, writes, reads, docs), "sp", 1)
    rate = decay_rate.reshape(-1, 1)
    sv, sw, run, step, enter, send = local_states(
        before, values, writes, step_raw, rate, decay_jump, docs, taps_values, taps_write
    )
    near = from_behind(send, "sp", 1)
    sr, mixed, reach = local_mix(before, reads, docs, taps_read, sv, sw, run, step, enter)
    far = from_behind(join_states(send, near, heads), "sp", 2)
    both = project(
        core, near, far, sr, mixed, reach, out_gate, mixer_gain.reshape(1, -1), mixer_out, owners
    )
    own_after, spread = after_mix(at, exchange(sum_pairs(both)), residual)
    mine = exchange(spread)
    other = to_partner(mine)
    gain = channel_gain.reshape(2 * owners, 1, -1)
    both = channel_mixer(core, mine, other, gain, weights)
    return add_down(exchange(sum_pairs(both)), own_after)


def solution(mesh):
    return jax.shard_map(
        on_device,
        mesh=mesh,
        in_specs=(
            P(("grp", "sp"), None),
            P(("grp", "sp"), "tp"),
            P(("grp", "sp"), "tp"),
            P(("grp", "sp"), "tp"),
            P(("grp", "sp"), "tp"),
            P("tp", ("grp", "sp")),
            P("tp"),
            P("tp", ("grp", "sp")),
            P(("grp", "sp")),
            P(None, "tp"),
            P(None, "tp"),
            P(None, "tp"),
            P("tp"),
            P("tp", None),
            P(),
            P("sp", "tp"),
            P("sp", "tp"),
            P("sp", "tp"),
        ),
        out_specs=P(("grp", "sp"), "tp"),
        check_vma=False,
    )
```

time: 220 us -> 181 us (0.82)
  Pallas kernels: 0 us -> 35.9 us
  other arithmetic: 35.5 us -> 4.99 us
  waiting for transfers between devices: 58 us -> 28.5 us
  blocking collectives: 33.3 us -> 53.6 us
  matrix products: 18.2 us -> 0 us
  local copies, waits for them, and re-layouts: 19.5 us -> 3.78 us
    all_to_all x2 -> x0, waiting for transfers between devices: 52.8 us -> none  [the longest x1 26.4 us: sum_at_owner(): lax.all_to_all(cut_along(value, dim, peers), axis, 0, 0, tiled=True)]
    pallas_call x0 -> x8, Pallas kernels: none -> 35.9 us  [the longest x1 12.4 us: channel_mixer(): pl.pallas_call(mixer_kernel, in_specs=[smem(), anywhere, anywhere, vmem()...]
    ppermute x0 -> x3, starting transfers between devices: none -> 22.8 us  [to_partner(): lax.ppermute(value, 'tp', [(i, i ^ 1) for i in range(lax.axis_size('tp'))])]
    all_to_all x2 -> x0, starting transfers between devices: 20.4 us -> none  [the longest x1 15 us: sum_at_owner(): lax.all_to_all(cut_along(value, dim, peers), axis, 0, 0, tiled=True)]
    all_to_all x1 -> x3, blocking collectives: 33.3 us -> 53.6 us  [exchange(): return lax.all_to_all(value, 'tp', 0, 0, axis_index_groups=rows, tiled=True)]
    all_gather x1, waiting for transfers between devices: 0.01 us -> 18.7 us  [on_device(): weights = lax.all_gather(late, 'sp', axis=0)]
    dot_general x7 -> x0, matrix products: 18.2 us -> none  [the longest x1 8.48 us: down_product(): lax.dot_general(hidden, rows, (((1,), (1,)), ((), ())), preferred_element...]
    convert_element_type x14 -> x2, other arithmetic: 12.8 us -> 3.02 us  [sum_pairs(): return (both[0].astype(F32) + to_partner(both[1]).astype(F32)).astype(BF16)]
  transfers between devices with their start and end apart: 6 -> 7, of which waited for: 3 -> 7; matrix products, arithmetic and copies ran while one was open for 25% -> 2% of each run, Pallas kernels for 0% -> 12%
where the time goes in v2:
time: 181 us
  blocking collectives  53.6 us (30%)
  starting transfers between devices  40.3 us (22%)
  Pallas kernels  35.9 us (20%)
  waiting for transfers between devices  28.5 us (16%)
  between operations  13.5 us (7%)
  other arithmetic  4.99 us (3%)
  local copies, waits for them, and re-layouts  3.78 us (2%)
    all_to_all x3, blocking collectives, exchange(): return lax.all_to_all(value, 'tp', 0, 0, axis_index_groups=rows, tiled=True)  53.6 us
    ppermute x3, starting transfers between devices, to_partner(): lax.ppermute(value, 'tp', [(i, i ^ 1) for i in range(lax.axis_size('tp'))])  22.8 us
    all_gather x1, waiting for transfers between devices, on_device(): weights = lax.all_gather(late, 'sp', axis=0)  18.7 us
    ppermute x3, starting transfers between devices, from_behind(): return lax.ppermute(value, axis, pairs)  17.5 us
    pallas_call x1, Pallas kernels, channel_mixer(): pl.pallas_call(mixer_kernel, in_specs=[smem(), anywhere, anywhere, vmem()...  12.4 us
    ppermute x3, waiting for transfers between devices, to_partner(): lax.ppermute(value, 'tp', [(i, i ^ 1) for i in range(lax.axis_size('tp'))])  6.67 us
    pallas_call x1, Pallas kernels, project(): pl.pallas_call(project_kernel, in_specs=[smem()] + [vmem()] * 8, out_shap...  6.49 us
    pallas_call x1, Pallas kernels, local_states(): pl.pallas_call(state_kernel, out_shape=(shape((tokens, wide), BF16), shap...  5.04 us
  transfers between devices with their start and end apart: 7, of which 7 were waited for; matrix products, arithmetic and copies ran while one was open for 2% of the time, Pallas kernels for 12%

profile of v2, /device:TPU:33, one launch (start us, length us, event | category | flops | bytes accessed | tf_op | source)
XLA Modules:
  0.0 180.5 jit_solution(10634646887868274994)
XLA Ops:
  6.5 0.0 copy-start.5
  6.5 0.0 all-gather.3.cloned.1.call-start
  6.6 0.0 copy-start.4
  6.6 2.0 %pad_maximum_fusion = bf16[2112,128]{1,0:T(8,128)(2,1)} fusion(bf16[704,128]{1,0:T(8,128)(2,1)} %bitcast.8, bf16[704,128]{1,0:T(8,128)(2,1)} %bitcast.9, bf16[704,128]{1,0:T(8,128)(2,1)} %bitcast.10), kind=kLoop, calls=%fused_computation.2 | loop fusion | flops 1622016 | bytes 1081344 | tf_op jit(solution)/shard_map/concatenate | solution.py:593
  8.5 0.1 all-gather.3.cloned.1.call-update
  8.6 1.5 pack_edge.1
  10.1 5.2 %collective-permute-start = (bf16[16,896]{1,0:T(8,128)(2,1)}, bf16[16,896]{1,0:T(8,128)(2,1)S(1)}, u32[]{:S(2)}, u32[]{:S(2)}) collective-permute-start(bf16[16,896]{1,0:T(8,128)(2,1)} %pack_edge.1), channel_id=1, source_target_pairs={{0,8},{8,16},{16,24},{24,32},{32,40},{40,48},{48,56},{56,64},{64,7... | collective-permute-start | bytes 86024 | tf_op jit(solution)/shard_map/ppermute | solution.py:25
  15.4 0.0 copy-done.5
  15.4 0.7 copy.20.rate_ref
  16.0 0.5 collective-permute-done.before_ref
  16.5 0.0 copy-start.7
  16.5 0.6 copy-done.7
  17.1 5.0 %local_states.1 = (bf16[512,512]{1,0:T(8,128)(2,1)}, bf16[512,128]{1,0:T(8,128)(2,1)}, f32[8,512]{1,0:T(8,128)}, f32[8,512]{1,0:T(8,128)}, bf16[3,512,128]{2,1,0:T(8,128)(2,1)}, /*index=5*/bf16[528,128]{1,0:T(8,128)(2,1)}) custom-call(bf16[16,896]{1,0:T(8,128)(2,1)} %copy-done.7, bf16[512,512]{1,0:T(8,128)(2,1)} %values_ref.3, bf16[512,128]{1,0:T(8,128)(2,1)} %writes_ref.3, ...), custom_call_target="tpu_custom_call" | custom-call | flops 400000000 | bytes 4000000 | tf_op jit(solution)/shard_map/local_states/pallas_call | solution.py:212
  22.2 4.4 %collective-permute-start.1 = (bf16[528,128]{1,0:T(8,128)(2,1)}, bf16[528,128]{1,0:T(8,128)(2,1)S(1)}, u32[]{:S(2)}, u32[]{:S(2)}) collective-permute-start(bf16[528,128]{1,0:T(8,128)(2,1)} %get-tuple-element.20.own_ref), channel_id=1, source_target_pairs={{0,8},{8,16},{16,24},{24,32},{32,40},{40,48},{48,56},{56,64},{64,7... | collective-permute-start | bytes 405512 | tf_op jit(solution)/shard_map/ppermute | solution.py:25
  26.6 2.3 %collective-permute-done.1.near_ref = bf16[528,128]{1,0:T(8,128)(2,1)S(1)} collective-permute-done((bf16[528,128]{1,0:T(8,128)(2,1)}, bf16[528,128]{1,0:T(8,128)(2,1)S(1)}, u32[]{:S(2)}, u32[]{:S(2)}) %collective-permute-start.1) | collective-permute-done | bytes 135200 | tf_op jit(solution)/shard_map/ppermute | solution.py:25
  28.9 0.0 copy-start.1
  28.9 0.6 copy-done.1
  29.5 1.7 join_states.1
  31.2 7.8 %collective-permute-start.2 = (bf16[512,128]{1,0:T(8,128)(2,1)}, bf16[512,128]{1,0:T(8,128)(2,1)S(1)}, u32[]{:S(2)}, u32[]{:S(2)}) collective-permute-start(bf16[512,128]{1,0:T(8,128)(2,1)} %join_states.1), channel_id=1, source_target_pairs={{0,16},{8,24},{16,32},{24,40},{32,48},{40,56},{48,64},{56,72},{64,... | collective-permute-start | bytes 393224 | tf_op jit(solution)/shard_map/ppermute | solution.py:25
  39.1 0.0 copy-done.4
  39.1 0.6 reshape.22.gain_ref
  39.7 4.1 %local_mix.1 = (bf16[512,128]{1,0:T(8,128)(2,1)}, f32[512,512]{1,0:T(8,128)}, f32[8,512]{1,0:T(8,128)}) custom-call(bf16[16,896]{1,0:T(8,128)(2,1)} %copy-done.7, bf16[512,128]{1,0:T(8,128)(2,1)} %reads_ref.3, s32[4,128]{1,0:T(4,128)} %bitcast.13, bf16[4,128]{1,0:T(4,128)(2,1)} %taps_ref.1, bf16[512,512]{1,0:T(8,128)(2,1)} %get-tuple-element.21.sv_ref, ...), custom_call_target="tpu_custom_call" | custom-call | flops 800000000 | bytes 4000000 | tf_op jit(solution)/shard_map/local_mix/pallas_call | solution.py:333
  43.8 0.3 collective-permute-done.2.far_ref
  44.1 0.0 copy-start.2
  44.1 0.7 copy-done.2
  44.8 6.5 %project.1 = (bf16[4,512,256]{2,1,0:T(8,128)(2,1)}, bf16[4,512,256]{2,1,0:T(8,128)(2,1)}) custom-call(s32[1]{0:T(128)} %bitcast.core_ref.at_ref, bf16[528,128]{1,0:T(8,128)(2,1)} %copy-done.1, bf16[512,128]{1,0:T(8,128)(2,1)} %copy-done.2, bf16[512,128]{1,0:T(8,128)(2,1)} %get-tuple-element.26.sr_ref, f32[512,512]{1,0:T(8,128)} %get-tuple-element.27.mixed_ref, ...), custom_call_target="tpu_custom_call" | custom-call | flops 1073741824 | bytes 6000000 | tf_op jit(solution)/shard_map/project/pallas_call | solution.py:407
  51.3 18.4 %collective-permute-start.3 = (bf16[4,512,256]{2,1,0:T(8,128)(2,1)}, bf16[4,512,256]{2,1,0:T(8,128)(2,1)S(1)}, u32[]{:S(2)}, u32[]{:S(2)}) collective-permute-start(bf16[4,512,256]{2,1,0:T(8,128)(2,1)} %get-tuple-element.30), channel_id=1, source_target_pairs={{0,1},{1,0},{2,3},{3,2},{4,5},{5,4},{6,7},{7,6},{8,9},{9,8},{10,11... | collective-permute-start | bytes 3145736 | tf_op jit(solution)/shard_map/ppermute | solution.py:555
  69.6 2.5 %collective-permute-done.3 = bf16[4,512,256]{2,1,0:T(8,128)(2,1)S(1)} collective-permute-done((bf16[4,512,256]{2,1,0:T(8,128)(2,1)}, bf16[4,512,256]{2,1,0:T(8,128)(2,1)S(1)}, u32[]{:S(2)}, u32[]{:S(2)}) %collective-permute-start.3) | collective-permute-done | bytes 1048608 | tf_op jit(solution)/shard_map/ppermute | solution.py:555
  72.1 1.5 add_convert_fusion.1
  73.6 18.0 %all_to_all.15.parts_ref = bf16[4,512,256]{2,1,0:T(8,128)(2,1)} all-to-all(bf16[4,512,256]{2,1,0:T(8,128)(2,1)S(1)} %add_convert_fusion.1), channel_id=1, replica_groups={{0,2,4,6},{1,3,5,7},{8,10,12,14},{9,11,13,15},{16,18,20,22},{17,19,21,2..., dimensions={0} | all-to-all | bytes 2097152 | tf_op jit(solution)/shard_map/all_to_all | solution.py:561
  91.7 0.0 copy-start.3
  91.7 2.5 %after_mix.1 = (bf16[512,256]{1,0:T(8,128)(2,1)}, bf16[4,512,256]{2,1,0:T(8,128)(2,1)}) custom-call(s32[1]{0:T(128)} %bitcast.1.at_ref, bf16[4,512,256]{2,1,0:T(8,128)(2,1)} %all_to_all.15.parts_ref, bf16[512,2048]{1,0:T(8,128)(2,1)} %residual_ref.1), custom_call_target="tpu_custom_call" | custom-call | tf_op jit(solution)/shard_map/after_mix/pallas_call | solution.py:431
  94.2 17.5 %all_to_all.16.mine_ref = bf16[4,512,256]{2,1,0:T(8,128)(2,1)S(1)} all-to-all(bf16[4,512,256]{2,1,0:T(8,128)(2,1)} %get-tuple-element.31), channel_id=1, replica_groups={{0,2,4,6},{1,3,5,7},{8,10,12,14},{9,11,13,15},{16,18,20,22},{17,19,21,2..., dimensions={0} | all-to-all | bytes 2097152 | tf_op jit(solution)/shard_map/all_to_all | solution.py:561
  111.7 0.0 copy-start
  111.7 2.1 %collective-permute-start.4 = (bf16[4,512,256]{2,1,0:T(8,128)(2,1)S(1)}, bf16[4,512,256]{2,1,0:T(8,128)(2,1)S(1)}, u32[]{:S(2)}, u32[]{:S(2)}) collective-permute-start(bf16[4,512,256]{2,1,0:T(8,128)(2,1)S(1)} %all_to_all.16.mine_ref), channel_id=1, source_target_pairs={{0,1},{1,0},{2,3},{3,2},{4,5},{5,4},{6,7},{7,6},{8,9},{9,8},{10,11... | collective-permute-start | bytes 3145736 | tf_op jit(solution)/shard_map/ppermute | solution.py:555
  113.8 0.0 copy-done.3
  113.8 0.6 reshape.25.gain_ref
  114.4 1.7 collective-permute-done.4.other_ref
  116.0 0.0 copy-start.6
  116.0 18.7 %all-gather.3.cloned.1.call-done = bf16[33792,128]{1,0:T(8,128)(2,1)} async-done(((bf16[2112,128]{1,0:T(8,128)(2,1)}), bf16[33792,128]{1,0:T(8,128)(2,1)}) %all-gather.3.cloned.1.call-update) | async-done | bytes 8650768 | tf_op jit(solution)/shard_map/all_gather | solution.py:594
  134.8 0.0 copy-done
  134.8 0.0 copy-done.6
  134.8 12.4 %channel_mixer.1 = (bf16[4,512,256]{2,1,0:T(8,128)(2,1)}, bf16[4,512,256]{2,1,0:T(8,128)(2,1)}) custom-call(s32[1]{0:T(128)} %bitcast.core_ref.at_ref, bf16[4,512,256]{2,1,0:T(8,128)(2,1)} %copy-done, bf16[4,512,256]{2,1,0:T(8,128)(2,1)} %copy-done.6, bf16[8,1,256]{2,1,0:T(2,128)(2,1)} %reshape.25.gain_ref, bf16[16,2112,128]{2,1,0:T(8,128)(2,1)} %bitcast.15), custom_call_target="tpu_custom_call" | custom-call | flops 4429185024 | bytes 14000000 | tf_op jit(solution)/shard_map/channel_mixer/pallas_call | solution.py:518
  147.1 2.3 %collective-permute-start.5 = (bf16[4,512,256]{2,1,0:T(8,128)(2,1)}, bf16[4,512,256]{2,1,0:T(8,128)(2,1)S(1)}, u32[]{:S(2)}, u32[]{:S(2)}) collective-permute-start(bf16[4,512,256]{2,1,0:T(8,128)(2,1)} %get-tuple-element.33), channel_id=1, source_target_pairs={{0,1},{1,0},{2,3},{3,2},{4,5},{5,4},{6,7},{7,6},{8,9},{9,8},{10,11... | collective-permute-start | bytes 3145736 | tf_op jit(solution)/shard_map/ppermute | solution.py:555
  149.4 2.5 %collective-permute-done.5 = bf16[4,512,256]{2,1,0:T(8,128)(2,1)S(1)} collective-permute-done((bf16[4,512,256]{2,1,0:T(8,128)(2,1)}, bf16[4,512,256]{2,1,0:T(8,128)(2,1)S(1)}, u32[]{:S(2)}, u32[]{:S(2)}) %collective-permute-start.5) | collective-permute-done | bytes 1048608 | tf_op jit(solution)/shard_map/ppermute | solution.py:555
  151.9 1.5 add_convert_fusion
  153.4 18.1 %all_to_all.17.parts_ref = bf16[4,512,256]{2,1,0:T(8,128)(2,1)} all-to-all(bf16[4,512,256]{2,1,0:T(8,128)(2,1)S(1)} %add_convert_fusion), channel_id=1, replica_groups={{0,2,4,6},{1,3,5,7},{8,10,12,14},{9,11,13,15},{16,18,20,22},{17,19,21,2..., dimensions={0} | all-to-all | bytes 2097152 | tf_op jit(solution)/shard_map/all_to_all | solution.py:561
  171.5 2.1 %add_down.1 = bf16[512,256]{1,0:T(8,128)(2,1)} custom-call(bf16[4,512,256]{2,1,0:T(8,128)(2,1)} %all_to_all.17.parts_ref, bf16[512,256]{1,0:T(8,128)(2,1)} %get-tuple-element.34.own_ref), custom_call_target="tpu_custom_call" | custom-call | tf_op jit(solution)/shard_map/add_down/pallas_call | solution.py:551
Async XLA Ops:
  6.5 8.8 %copy-start.5 = (f32[8]{0:T(128)S(1)}, f32[8]{0:T(128)}, u32[]{:S(2)}) copy-start(f32[8]{0:T(128)} %param.24) | copy-start | bytes 100
  6.5 128.2 %all-gather.3.cloned.1.call-start = ((), (), s32[]{:S(2)}) async-start(), calls=%async_computation.3 | async-start | bytes 9191424 | tf_op jit(solution)/shard_map/all_gather | solution.py:594
  6.6 32.5 %copy-start.4 = (bf16[512]{0:T(512)(128)(2,1)S(1)}, bf16[512]{0:T(512)(128)(2,1)}, u32[]{:S(2)}) copy-start(bf16[512]{0:T(512)(128)(2,1)} %param.30) | copy-start | bytes 3076
  10.1 6.4 %collective-permute-start = (bf16[16,896]{1,0:T(8,128)(2,1)}, bf16[16,896]{1,0:T(8,128)(2,1)S(1)}, u32[]{:S(2)}, u32[]{:S(2)}) collective-permute-start(bf16[16,896]{1,0:T(8,128)(2,1)} %pack_edge.1), channel_id=1, source_target_pairs={{0,8},{8,16},{16,24},{24,32},{32,40},{40,48},{48,56},{56,64},{64,7... | collective-permute-start | bytes 86024 | tf_op jit(solution)/shard_map/ppermute | solution.py:25
  16.5 0.6 copy-start.7
  22.2 6.7 %collective-permute-start.1 = (bf16[528,128]{1,0:T(8,128)(2,1)}, bf16[528,128]{1,0:T(8,128)(2,1)S(1)}, u32[]{:S(2)}, u32[]{:S(2)}) collective-permute-start(bf16[528,128]{1,0:T(8,128)(2,1)} %get-tuple-element.20.own_ref), channel_id=1, source_target_pairs={{0,8},{8,16},{16,24},{24,32},{32,40},{40,48},{48,56},{56,64},{64,7... | collective-permute-start | bytes 405512 | tf_op jit(solution)/shard_map/ppermute | solution.py:25
  28.9 0.6 copy-start.1
  31.2 12.9 %collective-permute-start.2 = (bf16[512,128]{1,0:T(8,128)(2,1)}, bf16[512,128]{1,0:T(8,128)(2,1)S(1)}, u32[]{:S(2)}, u32[]{:S(2)}) collective-permute-start(bf16[512,128]{1,0:T(8,128)(2,1)} %join_states.1), channel_id=1, source_target_pairs={{0,16},{8,24},{16,32},{24,40},{32,48},{40,56},{48,64},{56,72},{64,... | collective-permute-start | bytes 393224 | tf_op jit(solution)/shard_map/ppermute | solution.py:25
  44.1 0.7 copy-start.2
  51.3 20.9 %collective-permute-start.3 = (bf16[4,512,256]{2,1,0:T(8,128)(2,1)}, bf16[4,512,256]{2,1,0:T(8,128)(2,1)S(1)}, u32[]{:S(2)}, u32[]{:S(2)}) collective-permute-start(bf16[4,512,256]{2,1,0:T(8,128)(2,1)} %get-tuple-element.30), channel_id=1, source_target_pairs={{0,1},{1,0},{2,3},{3,2},{4,5},{5,4},{6,7},{7,6},{8,9},{9,8},{10,11... | collective-permute-start | bytes 3145736 | tf_op jit(solution)/shard_map/ppermute | solution.py:555
  91.7 22.1 %copy-start.3 = (bf16[2048]{0:T(1024)(128)(2,1)S(1)}, bf16[2048]{0:T(1024)(128)(2,1)}, u32[]{:S(2)}) copy-start(bf16[2048]{0:T(1024)(128)(2,1)} %param.32) | copy-start | bytes 12292
  111.7 23.1 %copy-start = (bf16[4,512,256]{2,1,0:T(8,128)(2,1)}, bf16[4,512,256]{2,1,0:T(8,128)(2,1)S(1)}, u32[]{:S(2)}) copy-start(bf16[4,512,256]{2,1,0:T(8,128)(2,1)S(1)} %all_to_all.16.mine_ref) | copy-start | bytes 3145732
  111.7 4.4 %collective-permute-start.4 = (bf16[4,512,256]{2,1,0:T(8,128)(2,1)S(1)}, bf16[4,512,256]{2,1,0:T(8,128)(2,1)S(1)}, u32[]{:S(2)}, u32[]{:S(2)}) collective-permute-start(bf16[4,512,256]{2,1,0:T(8,128)(2,1)S(1)} %all_to_all.16.mine_ref), channel_id=1, source_target_pairs={{0,1},{1,0},{2,3},{3,2},{4,5},{5,4},{6,7},{7,6},{8,9},{9,8},{10,11... | collective-permute-start | bytes 3145736 | tf_op jit(solution)/shard_map/ppermute | solution.py:555
  116.0 18.7 %copy-start.6 = (bf16[4,512,256]{2,1,0:T(8,128)(2,1)}, bf16[4,512,256]{2,1,0:T(8,128)(2,1)S(1)}, u32[]{:S(2)}) copy-start(bf16[4,512,256]{2,1,0:T(8,128)(2,1)S(1)} %collective-permute-done.4.other_ref) | copy-start | bytes 3145732
  147.1 4.8 %collective-permute-start.5 = (bf16[4,512,256]{2,1,0:T(8,128)(2,1)}, bf16[4,512,256]{2,1,0:T(8,128)(2,1)S(1)}, u32[]{:S(2)}, u32[]{:S(2)}) collective-permute-start(bf16[4,512,256]{2,1,0:T(8,128)(2,1)} %get-tuple-element.33), channel_id=1, source_target_pairs={{0,1},{1,0},{2,3},{3,2},{4,5},{5,4},{6,7},{7,6},{8,9},{9,8},{10,11... | collective-permute-start | bytes 3145736 | tf_op jit(solution)/shard_map/ppermute | solution.py:555
Sparse Core Ops, SparseCore 0:
  9.1 125.5 all-gather.2

commit v3 on v2

--- a/solution.py
+++ b/solution.py
@@ -7,8 +7,7 @@
 from jax.experimental.pallas import tpu as pltpu
 from jax.sharding import PartitionSpec as P
 
-HEADS = 64
-GROUPS = 8
+
 BLOCK = 128
 EDGE = 16
 LANES = 128
@@ -273,7 +272,6 @@
     tokens, narrow = reads_ref.shape
     wide = sv_ref.shape[1]
     blocks = tokens // BLOCK
-    heads = step_ref.shape[0]
     docs = doc_rows(docs_ref)
     place_docs(dext_ref, before_ref.at[:, wide + 2 * narrow :], docs, blocks)
     ext_ref[0:EDGE] = before_ref[:, wide + narrow : wide + 2 * narrow].astype(F32)
@@ -447,32 +445,26 @@
     )(at, parts, residual)
 
 
-def mixer_kernel(at_ref, mine_ref, other_ref, gain_ref, weight_ref, *refs):
-    out_refs = refs[:2]
-    after, normal, late, downs, hidden_ref, out, after_sem, late_sem, down_sem, out_sem = refs[2:]
-    _, owners, tokens, share = after.shape
-    peers, _, depth = weight_ref.shape
-    units = hidden_ref.shape[1]
-    core = at_ref[0]
+def mixer_kernel(peers, at_ref, mine_ref, other_ref, gain_ref, weight_ref, *refs):
+    down_refs = refs[:peers]
+    out_refs = refs[peers : peers + 2]
+    after, normal, late, downs, hidden_ref, out, after_sem, late_sem, down_sem, out_sem = refs[
+        peers + 2 :
+    ]
+    _, owners, _, share = after.shape
+    _, units, _ = downs.shape
+    core, place = at_ref[0], at_ref[1]
 
     loads = [
         pltpu.make_async_copy(ref, after.at[k], after_sem.at[k])
         for k, ref in enumerate((mine_ref, other_ref))
     ]
-    heavy, rows = [], []
-    for k in range(peers):
-        cols = pl.ds(k * depth, depth)
-        heavy.append(
-            pltpu.make_async_copy(
-                weight_ref.at[k, pl.ds(0, 2 * units)], late.at[:, cols], late_sem.at[k]
-            )
-        )
-        rows.append(
-            pltpu.make_async_copy(
-                weight_ref.at[k, pl.ds(2 * units, units)], downs.at[:, cols], down_sem.at[k]
-            )
-        )
-    for copy in (*loads, *heavy, *rows):
+    heavy = pltpu.make_async_copy(weight_ref, late, late_sem)
+    rows = []
+    for k, ref in enumerate(down_refs):
+        index = lax.rem(place - k + peers, peers)
+        rows.append(pltpu.make_async_copy(ref, downs.at[index], down_sem.at[k]))
+    for copy in (*loads, heavy):
         copy.start()
 
     for copy in loads:
@@ -489,11 +481,14 @@
             normal[:, pl.ds(pl.multiple_of(c * share, share), share)] = (
                 after[flip, k].astype(F32) * scale * gain_ref[c].astype(F32)
             ).astype(BF16)
-    for copy in heavy:
-        copy.wait()
+    heavy.wait()
+    for copy in rows:
+        copy.start()
     across = (((1,), (1,)), ((), ()))
-    gate = lax.dot_general(normal[...], late[0:units], across, preferred_element_type=F32)
-    up = lax.dot_general(normal[...], late[units:], across, preferred_element_type=F32)
+    gates = jnp.concatenate([late[k, 0:units] for k in range(peers)], axis=1)
+    gate = lax.dot_general(normal[...], gates, across, preferred_element_type=F32)
+    ups = jnp.concatenate([late[k, units:] for k in range(peers)], axis=1)
+    up = lax.dot_general(normal[...], ups, across, preferred_element_type=F32)
     hidden_ref[...] = (silu(gate) * up).astype(BF16)
     for copy in rows:
         copy.wait()
@@ -501,42 +496,57 @@
     for flip in (1, 0):
         for k in range(owners):
             c = 2 * k + (core ^ flip)
-            part = downs[:, pl.ds(pl.multiple_of(c * share, share), share)]
+            part = jnp.concatenate([downs[2 * c], downs[2 * c + 1]], axis=1)
             out[flip, k] = jnp.dot(hidden_ref[...], part, preferred_element_type=F32).astype(BF16)
-        store = pltpu.make_async_copy(out.at[flip], out_refs[flip], out_sem.at[flip])
-        store.start()
-        stores.append(store)
+            store = pltpu.make_async_copy(
+                out.at[flip, k], out_refs[flip].at[k], out_sem.at[flip, k]
+            )
+            store.start()
+            stores.append(store)
     for store in stores:
         store.wait()
 
 
-def channel_mixer(core, mine, other, gain, weights):
+def channel_mixer(at, mine, other, gain, weights, downs):
     owners, tokens, share = mine.shape
-    peers, units, depth = weights.shape[0], weights.shape[1] // 3, weights.shape[2]
+    peers, units, depth = len(downs), *downs[0].shape
     anywhere = pl.BlockSpec(memory_space=pl.ANY)
     out = shape((owners, tokens, share), BF16)
     return pl.pallas_call(
-        mixer_kernel,
-        in_specs=[smem(), anywhere, anywhere, vmem(), anywhere],
+        functools.partial(mixer_kernel, peers),
+        in_specs=[smem(), anywhere, anywhere, vmem(), anywhere] + [anywhere] * peers,
         out_specs=[anywhere, anywhere],
         out_shape=(out, out),
         scratch_shapes=[
             pltpu.VMEM((2, owners, tokens, share), BF16),
             pltpu.VMEM((tokens, peers * depth), BF16),
-            pltpu.VMEM((2 * units, peers * depth), BF16),
-            pltpu.VMEM((units, peers * depth), BF16),
+            pltpu.VMEM((peers, 2 * units, depth), BF16),
+            pltpu.VMEM((peers, units, depth), BF16),
             pltpu.VMEM((tokens, units), BF16),
             pltpu.VMEM((2, owners, tokens, share), BF16),
             pltpu.SemaphoreType.DMA((2,)),
+            pltpu.SemaphoreType.DMA,
             pltpu.SemaphoreType.DMA((peers,)),
-            pltpu.SemaphoreType.DMA((peers,)),
-            pltpu.SemaphoreType.DMA((2,)),
+            pltpu.SemaphoreType.DMA((2, owners)),
         ],
         cost_estimate=pl.CostEstimate(
             flops=12 * tokens * owners * share * units, transcendentals=0, bytes_accessed=14_000_000
         ),
         name="channel_mixer",
-    )(core, mine, other, gain, weights)
+    )(at, mine, other, gain, weights, *downs)
+
+
+def ring_of(value, axis):
+    peers = lax.axis_size(axis)
+    found = {0: value}
+    up = down = value
+    for k in range(1, peers // 2 + 1):
+        up = lax.ppermute(up, axis, [(i, (i + 1) % peers) for i in range(peers)])
+        found[k] = up
+        if k < peers - k:
+            down = lax.ppermute(down, axis, [(i, (i - 1) % peers) for i in range(peers)])
+            found[peers - k] = down
+    return [found[k] for k in range(peers)]
 
 
 def out_kernel(parts_ref, own_ref, out_ref):
@@ -590,8 +600,10 @@
     me = lax.axis_index("tp").astype(jnp.int32)
     at = me.reshape(1)
     core = (me % 2).reshape(1)
-    late = jnp.concatenate([gate_weight.T, up_weight.T, down_rows.T], axis=0)
+    place = jnp.stack([me % 2, lax.axis_index("sp").astype(jnp.int32)])
+    late = jnp.concatenate([gate_weight.T, up_weight.T], axis=0)
     weights = lax.all_gather(late, "sp", axis=0)
+    downs = ring_of(down_rows.T, "sp")
 
     docs = documents.reshape(-1, BLOCK)
     before = from_behind(pack_edge(values, writes, reads, docs), "sp", 1)
@@ -601,16 +613,20 @@
     )
     near = from_behind(send, "sp", 1)
     sr, mixed, reach = local_mix(before, reads, docs, taps_read, sv, sw, run, step, enter)
-    far = from_behind(join_states(send, near, heads), "sp", 2)
-    both = project(
-        core, near, far, sr, mixed, reach, out_gate, mixer_gain.reshape(1, -1), mixer_out, owners
-    )
-    own_after, spread = after_mix(at, exchange(sum_pairs(both)), residual)
+    joined = join_states(send, near, heads)
+    far = from_behind(joined, "sp", 2)
+    gain = mixer_gain.reshape(1, -1)
+    both = project(core, near, far, sr, mixed, reach, out_gate, gain, mixer_out, owners)
+    parts = sum_pairs(both)
+    parts = exchange(parts)
+    own_after, spread = after_mix(at, parts, residual)
     mine = exchange(spread)
     other = to_partner(mine)
     gain = channel_gain.reshape(2 * owners, 1, -1)
-    both = channel_mixer(core, mine, other, gain, weights)
-    return add_down(exchange(sum_pairs(both)), own_after)
+    both = channel_mixer(place, mine, other, gain, weights, downs)
+    parts = sum_pairs(both)
+    parts = exchange(parts)
+    return add_down(parts, own_after)
 
 
 def solution(mesh):

time: 181 us -> 208 us (1.15)
  starting transfers between devices: 40.3 us -> 77.8 us
  blocking collectives: 53.6 us -> 35.8 us
  waiting for transfers between devices: 28.5 us -> 34 us
    ppermute x0 -> x15, starting transfers between devices: none -> 29.1 us  [the longest x7 28.8 us: ring_of(): lax.ppermute(down, axis, [(i, (i - 1) % peers) for i in range(peers)])]
    ppermute x0 -> x15, waiting for transfers between devices: none -> 26.6 us  [the longest x8 14.5 us: ring_of(): up = lax.ppermute(up, axis, [(i, (i + 1) % peers) for i in range(peers)])]
    all_gather x1, waiting for transfers between devices: 18.7 us -> 0.01 us  [on_device(): weights = lax.all_gather(late, 'sp', axis=0)]
    all_to_all x3 -> x2, blocking collectives: 53.6 us -> 35.8 us  [exchange(): return lax.all_to_all(value, 'tp', 0, 0, axis_index_groups=rows, tiled=True)]
    ppermute x3, starting transfers between devices: 22.8 us -> 27.6 us  [to_partner(): lax.ppermute(value, 'tp', [(i, i ^ 1) for i in range(lax.axis_size('tp'))])]
    all_to_all x0 -> x1, starting transfers between devices: none -> 3.61 us  [exchange(): return lax.all_to_all(value, 'tp', 0, 0, axis_index_groups=rows, tiled=True)]
  transfers between devices with their start and end apart: 7 -> 23, of which waited for: 7 -> 13; matrix products, arithmetic and copies ran while one was open for 2% -> 2% of each run, Pallas kernels for 12% -> 10%
where the time goes in v3:
time: 208 us; the launch traced here: 206 us
  starting transfers between devices  77.8 us (37%)
  blocking collectives  35.8 us (17%)
  waiting for transfers between devices  34 us (16%)
  Pallas kernels  34 us (16%)
  between operations  13.6 us (7%)
  local copies, waits for them, and re-layouts  5.41 us (3%)
  other arithmetic  5.41 us (3%)
    all_to_all x2, blocking collectives, exchange(): return lax.all_to_all(value, 'tp', 0, 0, axis_index_groups=rows, tiled=True)  35.8 us
    ppermute x7, starting transfers between devices, ring_of(): lax.ppermute(down, axis, [(i, (i - 1) % peers) for i in range(peers)])  28.8 us
    ppermute x3, starting transfers between devices, to_partner(): lax.ppermute(value, 'tp', [(i, i ^ 1) for i in range(lax.axis_size('tp'))])  27.6 us
    ppermute x3, starting transfers between devices, from_behind(): return lax.ppermute(value, axis, pairs)  17.5 us
    ppermute x8, waiting for transfers between devices, ring_of(): up = lax.ppermute(up, axis, [(i, (i + 1) % peers) for i in range(peers)])  14.5 us
    ppermute x7, waiting for transfers between devices, ring_of(): lax.ppermute(down, axis, [(i, (i - 1) % peers) for i in range(peers)])  12.1 us
    pallas_call x1, Pallas kernels, channel_mixer(): pl.pallas_call(functools.partial(mixer_kernel, peers), in_specs=[smem(),...  10.4 us
    pallas_call x1, Pallas kernels, project(): pl.pallas_call(project_kernel, in_specs=[smem()] + [vmem()] * 8, out_shap...  6.54 us
  transfers between devices with their start and end apart: 23, of which 13 were waited for; matrix products, arithmetic and copies ran while one was open for 2% of the time, Pallas kernels for 10%

profile of v3, /device:TPU:33, one launch (start us, length us, event | category | flops | bytes accessed | tf_op | source)
XLA Modules:
  0.0 206.0 jit_solution(13680013869217231899)
XLA Ops:
  6.6 1.8 pad_maximum_fusion
  8.4 1.5 pack_edge.1
  9.9 5.2 %collective-permute-start = (bf16[16,896]{1,0:T(8,128)(2,1)}, bf16[16,896]{1,0:T(8,128)(2,1)S(1)}, u32[]{:S(2)}, u32[]{:S(2)}) collective-permute-start(bf16[16,896]{1,0:T(8,128)(2,1)} %pack_edge.1), channel_id=1, source_target_pairs={{0,8},{8,16},{16,24},{24,32},{32,40},{40,48},{48,56},{56,64},{64,7... | collective-permute-start | bytes 86024 | tf_op jit(solution)/shard_map/ppermute | solution.py:24
  15.2 1.3 copy.20.rate_ref
  16.5 0.6 copy-done.18
  17.1 5.1 %local_states.1 = (bf16[512,512]{1,0:T(8,128)(2,1)}, bf16[512,128]{1,0:T(8,128)(2,1)}, f32[8,512]{1,0:T(8,128)}, f32[8,512]{1,0:T(8,128)}, bf16[3,512,128]{2,1,0:T(8,128)(2,1)}, /*index=5*/bf16[528,128]{1,0:T(8,128)(2,1)}) custom-call(bf16[16,896]{1,0:T(8,128)(2,1)} %copy-done.18, bf16[512,512]{1,0:T(8,128)(2,1)} %values_ref.3, bf16[512,128]{1,0:T(8,128)(2,1)} %writes_ref.3, ...), custom_call_target="tpu_custom_call" | custom-call | flops 400000000 | bytes 4000000 | tf_op jit(solution)/shard_map/local_states/pallas_call | solution.py:211
  22.2 4.4 %collective-permute-start.1 = (bf16[528,128]{1,0:T(8,128)(2,1)}, bf16[528,128]{1,0:T(8,128)(2,1)S(1)}, u32[]{:S(2)}, u32[]{:S(2)}) collective-permute-start(bf16[528,128]{1,0:T(8,128)(2,1)} %get-tuple-element.20.own_ref), channel_id=1, source_target_pairs={{0,8},{8,16},{16,24},{24,32},{32,40},{40,48},{48,56},{56,64},{64,7... | collective-permute-start | bytes 405512 | tf_op jit(solution)/shard_map/ppermute | solution.py:24
  26.6 2.3 %collective-permute-done.1.near_ref = bf16[528,128]{1,0:T(8,128)(2,1)S(1)} collective-permute-done((bf16[528,128]{1,0:T(8,128)(2,1)}, bf16[528,128]{1,0:T(8,128)(2,1)S(1)}, u32[]{:S(2)}, u32[]{:S(2)}) %collective-permute-start.1) | collective-permute-done | bytes 135200 | tf_op jit(solution)/shard_map/ppermute | solution.py:24
  28.9 0.6 copy-done.1
  29.5 1.7 join_states.1
  31.2 7.8 %collective-permute-start.2 = (bf16[512,128]{1,0:T(8,128)(2,1)}, bf16[512,128]{1,0:T(8,128)(2,1)S(1)}, u32[]{:S(2)}, u32[]{:S(2)}) collective-permute-start(bf16[512,128]{1,0:T(8,128)(2,1)} %join_states.1), channel_id=1, source_target_pairs={{0,16},{8,24},{16,32},{24,40},{32,48},{40,56},{48,64},{56,72},{64,... | collective-permute-start | bytes 393224 | tf_op jit(solution)/shard_map/ppermute | solution.py:24
  39.1 0.6 reshape.19.gain_ref
  39.6 4.1 %local_mix.1 = (bf16[512,128]{1,0:T(8,128)(2,1)}, f32[512,512]{1,0:T(8,128)}, f32[8,512]{1,0:T(8,128)}) custom-call(bf16[16,896]{1,0:T(8,128)(2,1)} %copy-done.18, bf16[512,128]{1,0:T(8,128)(2,1)} %reads_ref.3, s32[4,128]{1,0:T(4,128)} %bitcast.13, bf16[4,128]{1,0:T(4,128)(2,1)} %taps_ref.1, bf16[512,512]{1,0:T(8,128)(2,1)} %get-tuple-element.21.sv_ref, ...), custom_call_target="tpu_custom_call" | custom-call | flops 800000000 | bytes 4000000 | tf_op jit(solution)/shard_map/local_mix/pallas_call | solution.py:331
  43.8 0.7 copy-done.2
  44.4 6.5 %project.1 = (bf16[4,512,256]{2,1,0:T(8,128)(2,1)}, bf16[4,512,256]{2,1,0:T(8,128)(2,1)}) custom-call(s32[1]{0:T(128)} %bitcast.core_ref, bf16[528,128]{1,0:T(8,128)(2,1)} %copy-done.1, bf16[512,128]{1,0:T(8,128)(2,1)} %copy-done.2, bf16[512,128]{1,0:T(8,128)(2,1)} %get-tuple-element.26.sr_ref, f32[512,512]{1,0:T(8,128)} %get-tuple-element.27.mixed_ref, ...), custom_call_target="tpu_custom_call" | custom-call | flops 1073741824 | bytes 6000000 | tf_op jit(solution)/shard_map/project/pallas_call | solution.py:405
  50.9 18.2 %collective-permute-start.3 = (bf16[4,512,256]{2,1,0:T(8,128)(2,1)}, bf16[4,512,256]{2,1,0:T(8,128)(2,1)S(1)}, u32[]{:S(2)}, u32[]{:S(2)}) collective-permute-start(bf16[4,512,256]{2,1,0:T(8,128)(2,1)} %get-tuple-element.30), channel_id=1, source_target_pairs={{0,1},{1,0},{2,3},{3,2},{4,5},{5,4},{6,7},{7,6},{8,9},{9,8},{10,11... | collective-permute-start | bytes 3145736 | tf_op jit(solution)/shard_map/ppermute | solution.py:565
  69.2 2.5 %collective-permute-done.3 = bf16[4,512,256]{2,1,0:T(8,128)(2,1)S(1)} collective-permute-done((bf16[4,512,256]{2,1,0:T(8,128)(2,1)}, bf16[4,512,256]{2,1,0:T(8,128)(2,1)S(1)}, u32[]{:S(2)}, u32[]{:S(2)}) %collective-permute-start.3) | collective-permute-done | bytes 1048608 | tf_op jit(solution)/shard_map/ppermute | solution.py:565
  71.7 1.5 add_convert_fusion.1
  73.2 18.0 %all_to_all.15.parts_ref = bf16[4,512,256]{2,1,0:T(8,128)(2,1)} all-to-all(bf16[4,512,256]{2,1,0:T(8,128)(2,1)S(1)} %add_convert_fusion.1), channel_id=1, replica_groups={{0,2,4,6},{1,3,5,7},{8,10,12,14},{9,11,13,15},{16,18,20,22},{17,19,21,2..., dimensions={0} | all-to-all | bytes 2097152 | tf_op jit(solution)/shard_map/all_to_all | solution.py:571
  91.2 2.6 %after_mix.1 = (bf16[512,256]{1,0:T(8,128)(2,1)}, bf16[4,512,256]{2,1,0:T(8,128)(2,1)}) custom-call(s32[1]{0:T(128)} %bitcast.2.at_ref, bf16[4,512,256]{2,1,0:T(8,128)(2,1)} %all_to_all.15.parts_ref, bf16[512,2048]{1,0:T(8,128)(2,1)} %residual_ref.1), custom_call_target="tpu_custom_call" | custom-call | tf_op jit(solution)/shard_map/after_mix/pallas_call | solution.py:429
  93.7 3.6 %all-to-all-start.1 = ((bf16[4,512,256]{2,1,0:T(8,128)(2,1)}), bf16[4,512,256]{2,1,0:T(8,128)(2,1)S(1)}, u32[]{:S(2)}, u32[]{:S(2)}) async-start(bf16[4,512,256]{2,1,0:T(8,128)(2,1)} %get-tuple-element.31), calls=%async_computation.1 | async-start | bytes 2097152 | tf_op jit(solution)/shard_map/all_to_all | solution.py:571
  97.5 10.1 %collective-permute-start.13 = (bf16[704,128]{1,0:T(8,128)(2,1)S(1)}, bf16[704,128]{1,0:T(8,128)(2,1)S(1)}, u32[]{:S(2)}, u32[]{:S(2)}) collective-permute-start(bf16[704,128]{1,0:T(8,128)(2,1)S(1)} %bitcast.18), channel_id=1, source_target_pairs={{0,120},{8,0},{16,8},{24,16},{32,24},{40,32},{48,40},{56,48},{64,5... | collective-permute-start | bytes 540680 | tf_op jit(solution)/shard_map/ppermute | solution.py:547
  107.6 5.6 %collective-permute-done.5.refs_1_ = bf16[704,128]{1,0:T(8,128)(2,1)S(1)} collective-permute-done((bf16[704,128]{1,0:T(8,128)(2,1)S(1)}, bf16[704,128]{1,0:T(8,128)(2,1)S(1)}, u32[]{:S(2)}, u32[]{:S(2)}) %collective-permute-start.5) | collective-permute-done | bytes 180256 | tf_op jit(solution)/shard_map/ppermute | solution.py:544
  113.3 2.7 %collective-permute-start.14 = (bf16[704,128]{1,0:T(8,128)(2,1)S(1)}, bf16[704,128]{1,0:T(8,128)(2,1)S(1)}, u32[]{:S(2)}, u32[]{:S(2)}) collective-permute-start(bf16[704,128]{1,0:T(8,128)(2,1)S(1)} %collective-permute-done.13.refs_15_), channel_id=1, source_target_pairs={{0,120},{8,0},{16,8},{24,16},{32,24},{40,32},{48,40},{56,48},{64,5... | collective-permute-start | bytes 540680 | tf_op jit(solution)/shard_map/ppermute | solution.py:547
  115.9 3.3 %collective-permute-done.6.refs_2_ = bf16[704,128]{1,0:T(8,128)(2,1)S(1)} collective-permute-done((bf16[704,128]{1,0:T(8,128)(2,1)S(1)}, bf16[704,128]{1,0:T(8,128)(2,1)S(1)}, u32[]{:S(2)}, u32[]{:S(2)}) %collective-permute-start.6) | collective-permute-done | bytes 180256 | tf_op jit(solution)/shard_map/ppermute | solution.py:544
  119.3 2.3 %collective-permute-start.4 = (bf16[4,512,256]{2,1,0:T(8,128)(2,1)S(1)}, bf16[4,512,256]{2,1,0:T(8,128)(2,1)S(1)}, u32[]{:S(2)}, u32[]{:S(2)}) collective-permute-start(bf16[4,512,256]{2,1,0:T(8,128)(2,1)S(1)} %all-to-all-done.1.mine_ref), channel_id=1, source_target_pairs={{0,1},{1,0},{2,3},{3,2},{4,5},{5,4},{6,7},{7,6},{8,9},{9,8},{10,11... | collective-permute-start | bytes 3145736 | tf_op jit(solution)/shard_map/ppermute | solution.py:565
  121.6 2.8 %collective-permute-start.15 = (bf16[704,128]{1,0:T(8,128)(2,1)S(1)}, bf16[704,128]{1,0:T(8,128)(2,1)S(1)}, u32[]{:S(2)}, u32[]{:S(2)}) collective-permute-start(bf16[704,128]{1,0:T(8,128)(2,1)S(1)} %collective-permute-done.14.refs_14_), channel_id=1, source_target_pairs={{0,120},{8,0},{16,8},{24,16},{32,24},{40,32},{48,40},{56,48},{64,5... | collective-permute-start | bytes 540680 | tf_op jit(solution)/shard_map/ppermute | solution.py:547
  124.4 0.4 collective-permute-done.7.refs_3_
  124.8 3.4 %collective-permute-done.15.refs_13_ = bf16[704,128]{1,0:T(8,128)(2,1)S(1)} collective-permute-done((bf16[704,128]{1,0:T(8,128)(2,1)S(1)}, bf16[704,128]{1,0:T(8,128)(2,1)S(1)}, u32[]{:S(2)}, u32[]{:S(2)}) %collective-permute-start.15) | collective-permute-done | bytes 180256 | tf_op jit(solution)/shard_map/ppermute | solution.py:547
  128.2 3.4 %collective-permute-start.16 = (bf16[704,128]{1,0:T(8,128)(2,1)S(1)}, bf16[704,128]{1,0:T(8,128)(2,1)S(1)}, u32[]{:S(2)}, u32[]{:S(2)}) collective-permute-start(bf16[704,128]{1,0:T(8,128)(2,1)S(1)} %collective-permute-done.15.refs_13_), channel_id=1, source_target_pairs={{0,120},{8,0},{16,8},{24,16},{32,24},{40,32},{48,40},{56,48},{64,5... | collective-permute-start | bytes 540680 | tf_op jit(solution)/shard_map/ppermute | solution.py:547
  131.6 2.9 %collective-permute-done.16.refs_12_ = bf16[704,128]{1,0:T(8,128)(2,1)S(1)} collective-permute-done((bf16[704,128]{1,0:T(8,128)(2,1)S(1)}, bf16[704,128]{1,0:T(8,128)(2,1)S(1)}, u32[]{:S(2)}, u32[]{:S(2)}) %collective-permute-start.16) | collective-permute-done | bytes 180256 | tf_op jit(solution)/shard_map/ppermute | solution.py:547
  134.5 3.4 %collective-permute-start.17 = (bf16[704,128]{1,0:T(8,128)(2,1)S(1)}, bf16[704,128]{1,0:T(8,128)(2,1)S(1)}, u32[]{:S(2)}, u32[]{:S(2)}) collective-permute-start(bf16[704,128]{1,0:T(8,128)(2,1)S(1)} %collective-permute-done.16.refs_12_), channel_id=1, source_target_pairs={{0,120},{8,0},{16,8},{24,16},{32,24},{40,32},{48,40},{56,48},{64,5... | collective-permute-start | bytes 540680 | tf_op jit(solution)/shard_map/ppermute | solution.py:547
  138.0 2.4 %collective-permute-done.17.refs_11_ = bf16[704,128]{1,0:T(8,128)(2,1)S(1)} collective-permute-done((bf16[704,128]{1,0:T(8,128)(2,1)S(1)}, bf16[704,128]{1,0:T(8,128)(2,1)S(1)}, u32[]{:S(2)}, u32[]{:S(2)}) %collective-permute-start.17) | collective-permute-done | bytes 180256 | tf_op jit(solution)/shard_map/ppermute | solution.py:547
  140.4 3.1 %collective-permute-start.18 = (bf16[704,128]{1,0:T(8,128)(2,1)S(1)}, bf16[704,128]{1,0:T(8,128)(2,1)}, u32[]{:S(2)}, u32[]{:S(2)}) collective-permute-start(bf16[704,128]{1,0:T(8,128)(2,1)S(1)} %collective-permute-done.17.refs_11_), channel_id=1, source_target_pairs={{0,120},{8,0},{16,8},{24,16},{32,24},{40,32},{48,40},{56,48},{64,5... | collective-permute-start | bytes 540680 | tf_op jit(solution)/shard_map/ppermute | solution.py:547
  143.6 2.3 %collective-permute-done.18.refs_10_ = bf16[704,128]{1,0:T(8,128)(2,1)} collective-permute-done((bf16[704,128]{1,0:T(8,128)(2,1)S(1)}, bf16[704,128]{1,0:T(8,128)(2,1)}, u32[]{:S(2)}, u32[]{:S(2)}) %collective-permute-start.18) | collective-permute-done | bytes 180256 | tf_op jit(solution)/shard_map/ppermute | solution.py:547
  145.9 3.2 %collective-permute-start.19 = (bf16[704,128]{1,0:T(8,128)(2,1)}, bf16[704,128]{1,0:T(8,128)(2,1)}, u32[]{:S(2)}, u32[]{:S(2)}) collective-permute-start(bf16[704,128]{1,0:T(8,128)(2,1)} %collective-permute-done.18.refs_10_), channel_id=1, source_target_pairs={{0,120},{8,0},{16,8},{24,16},{32,24},{40,32},{48,40},{56,48},{64,5... | collective-permute-start | bytes 540680 | tf_op jit(solution)/shard_map/ppermute | solution.py:547
  149.2 0.5 collective-permute-done.11.refs_7_
  149.6 0.6 reshape.22.gain_ref
  150.2 0.6 pad_add_fusion.at_ref
  150.8 1.1 collective-permute-done.19.refs_9_
  151.9 4.7 %collective-permute-done.12.refs_8_ = bf16[704,128]{1,0:T(8,128)(2,1)} collective-permute-done((bf16[704,128]{1,0:T(8,128)(2,1)}, bf16[704,128]{1,0:T(8,128)(2,1)}, u32[]{:S(2)}, u32[]{:S(2)}) %collective-permute-start.12) | collective-permute-done | bytes 180256 | tf_op jit(solution)/shard_map/ppermute | solution.py:544
  156.8 0.9 copy-done.5
  157.7 10.4 %channel_mixer.1 = (bf16[4,512,256]{2,1,0:T(8,128)(2,1)}, bf16[4,512,256]{2,1,0:T(8,128)(2,1)}) custom-call(s32[2]{0:T(128)} %pad_add_fusion.at_ref, bf16[4,512,256]{2,1,0:T(8,128)(2,1)} %copy-done, bf16[4,512,256]{2,1,0:T(8,128)(2,1)} %copy-done.5, bf16[8,1,256]{2,1,0:T(2,128)(2,1)} %reshape.22.gain_ref, bf16[16,1408,128]{2,1,0:T(8,128)(2,1)} %bitcast.15, ...), custom_call_target="tpu_custom_call" | custom-call | flops 4429185024 | bytes 14000000 | tf_op jit(solution)/shard_map/channel_mixer/pallas_call | solution.py:515
  168.1 7.1 %collective-permute-start.20 = (bf16[4,512,256]{2,1,0:T(8,128)(2,1)}, bf16[4,512,256]{2,1,0:T(8,128)(2,1)S(1)}, u32[]{:S(2)}, u32[]{:S(2)}) collective-permute-start(bf16[4,512,256]{2,1,0:T(8,128)(2,1)} %get-tuple-element.33), channel_id=1, source_target_pairs={{0,1},{1,0},{2,3},{3,2},{4,5},{5,4},{6,7},{7,6},{8,9},{9,8},{10,11... | collective-permute-start | bytes 3145736 | tf_op jit(solution)/shard_map/ppermute | solution.py:565
  175.2 2.5 %collective-permute-done.20 = bf16[4,512,256]{2,1,0:T(8,128)(2,1)S(1)} collective-permute-done((bf16[4,512,256]{2,1,0:T(8,128)(2,1)}, bf16[4,512,256]{2,1,0:T(8,128)(2,1)S(1)}, u32[]{:S(2)}, u32[]{:S(2)}) %collective-permute-start.20) | collective-permute-done | bytes 1048608 | tf_op jit(solution)/shard_map/ppermute | solution.py:565
  177.7 1.5 add_convert_fusion
  179.2 17.8 %all_to_all.16.parts_ref = bf16[4,512,256]{2,1,0:T(8,128)(2,1)} all-to-all(bf16[4,512,256]{2,1,0:T(8,128)(2,1)S(1)} %add_convert_fusion), channel_id=1, replica_groups={{0,2,4,6},{1,3,5,7},{8,10,12,14},{9,11,13,15},{16,18,20,22},{17,19,21,2..., dimensions={0} | all-to-all | bytes 2097152 | tf_op jit(solution)/shard_map/all_to_all | solution.py:571
  197.0 2.1 %add_down.1 = bf16[512,256]{1,0:T(8,128)(2,1)} custom-call(bf16[4,512,256]{2,1,0:T(8,128)(2,1)} %all_to_all.16.parts_ref, bf16[512,256]{1,0:T(8,128)(2,1)} %get-tuple-element.34.own_ref), custom_call_target="tpu_custom_call" | custom-call | tf_op jit(solution)/shard_map/add_down/pallas_call | solution.py:561
  (54 shorter events, 0.4 us)
Async XLA Ops:
  6.5 32.5 %copy-start.4 = (bf16[512]{0:T(512)(128)(2,1)S(1)}, bf16[512]{0:T(512)(128)(2,1)}, u32[]{:S(2)}) copy-start(bf16[512]{0:T(512)(128)(2,1)} %param.30) | copy-start | bytes 3076
  6.5 150.1 %all-gather.3.cloned.1.call-start = ((), (), s32[]{:S(2)}) async-start(), calls=%async_computation.3 | async-start | bytes 6127616 | tf_op jit(solution)/shard_map/all_gather | solution.py:605
  9.9 6.6 %collective-permute-start = (bf16[16,896]{1,0:T(8,128)(2,1)}, bf16[16,896]{1,0:T(8,128)(2,1)S(1)}, u32[]{:S(2)}, u32[]{:S(2)}) collective-permute-start(bf16[16,896]{1,0:T(8,128)(2,1)} %pack_edge.1), channel_id=1, source_target_pairs={{0,8},{8,16},{16,24},{24,32},{32,40},{40,48},{48,56},{56,64},{64,7... | collective-permute-start | bytes 86024 | tf_op jit(solution)/shard_map/ppermute | solution.py:24
  16.5 0.6 copy-start.18
  22.2 6.7 %collective-permute-start.1 = (bf16[528,128]{1,0:T(8,128)(2,1)}, bf16[528,128]{1,0:T(8,128)(2,1)S(1)}, u32[]{:S(2)}, u32[]{:S(2)}) collective-permute-start(bf16[528,128]{1,0:T(8,128)(2,1)} %get-tuple-element.20.own_ref), channel_id=1, source_target_pairs={{0,8},{8,16},{16,24},{24,32},{32,40},{40,48},{48,56},{56,64},{64,7... | collective-permute-start | bytes 405512 | tf_op jit(solution)/shard_map/ppermute | solution.py:24
  28.9 0.7 copy-start.1
  31.2 12.6 %collective-permute-start.2 = (bf16[512,128]{1,0:T(8,128)(2,1)}, bf16[512,128]{1,0:T(8,128)(2,1)S(1)}, u32[]{:S(2)}, u32[]{:S(2)}) collective-permute-start(bf16[512,128]{1,0:T(8,128)(2,1)} %join_states.1), channel_id=1, source_target_pairs={{0,16},{8,24},{16,32},{24,40},{32,48},{40,56},{48,64},{56,72},{64,... | collective-permute-start | bytes 393224 | tf_op jit(solution)/shard_map/ppermute | solution.py:24
  43.7 0.7 copy-start.2
  50.9 20.7 %collective-permute-start.3 = (bf16[4,512,256]{2,1,0:T(8,128)(2,1)}, bf16[4,512,256]{2,1,0:T(8,128)(2,1)S(1)}, u32[]{:S(2)}, u32[]{:S(2)}) collective-permute-start(bf16[4,512,256]{2,1,0:T(8,128)(2,1)} %get-tuple-element.30), channel_id=1, source_target_pairs={{0,1},{1,0},{2,3},{3,2},{4,5},{5,4},{6,7},{7,6},{8,9},{9,8},{10,11... | collective-permute-start | bytes 3145736 | tf_op jit(solution)/shard_map/ppermute | solution.py:565
  91.2 6.2 %copy-start.6 = (bf16[128,704]{0,1:T(8,128)(2,1)S(1)}, bf16[128,704]{0,1:T(8,128)(2,1)}, u32[]{:S(2)}) copy-start(bf16[128,704]{0,1:T(8,128)(2,1)} %param.35) | copy-start | bytes 540676
  91.2 58.5 %copy-start.3 = (bf16[2048]{0:T(1024)(128)(2,1)S(1)}, bf16[2048]{0:T(1024)(128)(2,1)}, u32[]{:S(2)}) copy-start(bf16[2048]{0:T(1024)(128)(2,1)} %param.32) | copy-start | bytes 12292
  93.7 25.5 %all-to-all-start.1 = ((bf16[4,512,256]{2,1,0:T(8,128)(2,1)}), bf16[4,512,256]{2,1,0:T(8,128)(2,1)S(1)}, u32[]{:S(2)}, u32[]{:S(2)}) async-start(bf16[4,512,256]{2,1,0:T(8,128)(2,1)} %get-tuple-element.31), calls=%async_computation.1 | async-start | bytes 2097152 | tf_op jit(solution)/shard_map/all_to_all | solution.py:571
  97.4 15.9 %collective-permute-start.5 = (bf16[704,128]{1,0:T(8,128)(2,1)S(1)}, bf16[704,128]{1,0:T(8,128)(2,1)S(1)}, u32[]{:S(2)}, u32[]{:S(2)}) collective-permute-start(bf16[704,128]{1,0:T(8,128)(2,1)S(1)} %bitcast.17), channel_id=1, source_target_pairs={{0,8},{8,16},{16,24},{24,32},{32,40},{40,48},{48,56},{56,64},{64,7... | collective-permute-start | bytes 540680 | tf_op jit(solution)/shard_map/ppermute | solution.py:544
  97.5 15.8 %collective-permute-start.13 = (bf16[704,128]{1,0:T(8,128)(2,1)S(1)}, bf16[704,128]{1,0:T(8,128)(2,1)S(1)}, u32[]{:S(2)}, u32[]{:S(2)}) collective-permute-start(bf16[704,128]{1,0:T(8,128)(2,1)S(1)} %bitcast.18), channel_id=1, source_target_pairs={{0,120},{8,0},{16,8},{24,16},{32,24},{40,32},{48,40},{56,48},{64,5... | collective-permute-start | bytes 540680 | tf_op jit(solution)/shard_map/ppermute | solution.py:547
  113.3 43.4 %copy-start.7 = (bf16[704,128]{1,0:T(8,128)(2,1)}, bf16[704,128]{1,0:T(8,128)(2,1)S(1)}, u32[]{:S(2)}) copy-start(bf16[704,128]{1,0:T(8,128)(2,1)S(1)} %collective-permute-done.5.refs_1_) | copy-start | bytes 540676
  113.3 6.0 %collective-permute-start.6 = (bf16[704,128]{1,0:T(8,128)(2,1)S(1)}, bf16[704,128]{1,0:T(8,128)(2,1)S(1)}, u32[]{:S(2)}, u32[]{:S(2)}) collective-permute-start(bf16[704,128]{1,0:T(8,128)(2,1)S(1)} %collective-permute-done.5.refs_1_), channel_id=1, source_target_pairs={{0,8},{8,16},{16,24},{24,32},{32,40},{40,48},{48,56},{56,64},{64,7... | collective-permute-start | bytes 540680 | tf_op jit(solution)/shard_map/ppermute | solution.py:544
  113.3 43.4 %copy-start.8 = (bf16[704,128]{1,0:T(8,128)(2,1)}, bf16[704,128]{1,0:T(8,128)(2,1)S(1)}, u32[]{:S(2)}) copy-start(bf16[704,128]{1,0:T(8,128)(2,1)S(1)} %collective-permute-done.13.refs_15_) | copy-start | bytes 540676
  113.3 8.3 %collective-permute-start.14 = (bf16[704,128]{1,0:T(8,128)(2,1)S(1)}, bf16[704,128]{1,0:T(8,128)(2,1)S(1)}, u32[]{:S(2)}, u32[]{:S(2)}) collective-permute-start(bf16[704,128]{1,0:T(8,128)(2,1)S(1)} %collective-permute-done.13.refs_15_), channel_id=1, source_target_pairs={{0,120},{8,0},{16,8},{24,16},{32,24},{40,32},{48,40},{56,48},{64,5... | collective-permute-start | bytes 540680 | tf_op jit(solution)/shard_map/ppermute | solution.py:547
  119.3 37.4 %copy-start.9 = (bf16[704,128]{1,0:T(8,128)(2,1)}, bf16[704,128]{1,0:T(8,128)(2,1)S(1)}, u32[]{:S(2)}) copy-start(bf16[704,128]{1,0:T(8,128)(2,1)S(1)} %collective-permute-done.6.refs_2_) | copy-start | bytes 540676
  119.3 5.6 %collective-permute-start.7 = (bf16[704,128]{1,0:T(8,128)(2,1)S(1)}, bf16[704,128]{1,0:T(8,128)(2,1)S(1)}, u32[]{:S(2)}, u32[]{:S(2)}) collective-permute-start(bf16[704,128]{1,0:T(8,128)(2,1)S(1)} %collective-permute-done.6.refs_2_), channel_id=1, source_target_pairs={{0,8},{8,16},{16,24},{24,32},{32,40},{40,48},{48,56},{56,64},{64,7... | collective-permute-start | bytes 540680 | tf_op jit(solution)/shard_map/ppermute | solution.py:544
  119.3 37.4 %copy-start = (bf16[4,512,256]{2,1,0:T(8,128)(2,1)}, bf16[4,512,256]{2,1,0:T(8,128)(2,1)S(1)}, u32[]{:S(2)}) copy-start(bf16[4,512,256]{2,1,0:T(8,128)(2,1)S(1)} %all-to-all-done.1.mine_ref) | copy-start | bytes 3145732
  119.3 37.4 %collective-permute-start.4 = (bf16[4,512,256]{2,1,0:T(8,128)(2,1)S(1)}, bf16[4,512,256]{2,1,0:T(8,128)(2,1)S(1)}, u32[]{:S(2)}, u32[]{:S(2)}) collective-permute-start(bf16[4,512,256]{2,1,0:T(8,128)(2,1)S(1)} %all-to-all-done.1.mine_ref), channel_id=1, source_target_pairs={{0,1},{1,0},{2,3},{3,2},{4,5},{5,4},{6,7},{7,6},{8,9},{9,8},{10,11... | collective-permute-start | bytes 3145736 | tf_op jit(solution)/shard_map/ppermute | solution.py:565
  121.6 35.1 %copy-start.10 = (bf16[704,128]{1,0:T(8,128)(2,1)}, bf16[704,128]{1,0:T(8,128)(2,1)S(1)}, u32[]{:S(2)}) copy-start(bf16[704,128]{1,0:T(8,128)(2,1)S(1)} %collective-permute-done.14.refs_14_) | copy-start | bytes 540676
  121.6 6.6 %collective-permute-start.15 = (bf16[704,128]{1,0:T(8,128)(2,1)S(1)}, bf16[704,128]{1,0:T(8,128)(2,1)S(1)}, u32[]{:S(2)}, u32[]{:S(2)}) collective-permute-start(bf16[704,128]{1,0:T(8,128)(2,1)S(1)} %collective-permute-done.14.refs_14_), channel_id=1, source_target_pairs={{0,120},{8,0},{16,8},{24,16},{32,24},{40,32},{48,40},{56,48},{64,5... | collective-permute-start | bytes 540680 | tf_op jit(solution)/shard_map/ppermute | solution.py:547
  124.8 31.9 %copy-start.11 = (bf16[704,128]{1,0:T(8,128)(2,1)}, bf16[704,128]{1,0:T(8,128)(2,1)S(1)}, u32[]{:S(2)}) copy-start(bf16[704,128]{1,0:T(8,128)(2,1)S(1)} %collective-permute-done.7.refs_3_) | copy-start | bytes 540676
  124.8 6.8 %collective-permute-start.8 = (bf16[704,128]{1,0:T(8,128)(2,1)S(1)}, bf16[704,128]{1,0:T(8,128)(2,1)S(1)}, u32[]{:S(2)}, u32[]{:S(2)}) collective-permute-start(bf16[704,128]{1,0:T(8,128)(2,1)S(1)} %collective-permute-done.7.refs_3_), channel_id=1, source_target_pairs={{0,8},{8,16},{16,24},{24,32},{32,40},{40,48},{48,56},{56,64},{64,7... | collective-permute-start | bytes 540680 | tf_op jit(solution)/shard_map/ppermute | solution.py:544
  128.2 28.5 %copy-start.12 = (bf16[704,128]{1,0:T(8,128)(2,1)}, bf16[704,128]{1,0:T(8,128)(2,1)S(1)}, u32[]{:S(2)}) copy-start(bf16[704,128]{1,0:T(8,128)(2,1)S(1)} %collective-permute-done.15.refs_13_) | copy-start | bytes 540676
  128.2 6.3 %collective-permute-start.16 = (bf16[704,128]{1,0:T(8,128)(2,1)S(1)}, bf16[704,128]{1,0:T(8,128)(2,1)S(1)}, u32[]{:S(2)}, u32[]{:S(2)}) collective-permute-start(bf16[704,128]{1,0:T(8,128)(2,1)S(1)} %collective-permute-done.15.refs_13_), channel_id=1, source_target_pairs={{0,120},{8,0},{16,8},{24,16},{32,24},{40,32},{48,40},{56,48},{64,5... | collective-permute-start | bytes 540680 | tf_op jit(solution)/shard_map/ppermute | solution.py:547
  131.6 25.1 %copy-start.13 = (bf16[704,128]{1,0:T(8,128)(2,1)}, bf16[704,128]{1,0:T(8,128)(2,1)S(1)}, u32[]{:S(2)}) copy-start(bf16[704,128]{1,0:T(8,128)(2,1)S(1)} %collective-permute-done.8.refs_4_) | copy-start | bytes 540676
  131.6 6.3 %collective-permute-start.9 = (bf16[704,128]{1,0:T(8,128)(2,1)S(1)}, bf16[704,128]{1,0:T(8,128)(2,1)S(1)}, u32[]{:S(2)}, u32[]{:S(2)}) collective-permute-start(bf16[704,128]{1,0:T(8,128)(2,1)S(1)} %collective-permute-done.8.refs_4_), channel_id=1, source_target_pairs={{0,8},{8,16},{16,24},{24,32},{32,40},{40,48},{48,56},{56,64},{64,7... | collective-permute-start | bytes 540680 | tf_op jit(solution)/shard_map/ppermute | solution.py:544
  134.5 22.2 %copy-start.14 = (bf16[704,128]{1,0:T(8,128)(2,1)}, bf16[704,128]{1,0:T(8,128)(2,1)S(1)}, u32[]{:S(2)}) copy-start(bf16[704,128]{1,0:T(8,128)(2,1)S(1)} %collective-permute-done.16.refs_12_) | copy-start | bytes 540676
  134.5 5.9 %collective-permute-start.17 = (bf16[704,128]{1,0:T(8,128)(2,1)S(1)}, bf16[704,128]{1,0:T(8,128)(2,1)S(1)}, u32[]{:S(2)}, u32[]{:S(2)}) collective-permute-start(bf16[704,128]{1,0:T(8,128)(2,1)S(1)} %collective-permute-done.16.refs_12_), channel_id=1, source_target_pairs={{0,120},{8,0},{16,8},{24,16},{32,24},{40,32},{48,40},{56,48},{64,5... | collective-permute-start | bytes 540680 | tf_op jit(solution)/shard_map/ppermute | solution.py:547
  137.9 2.4 %copy-start.15 = (bf16[704,128]{1,0:T(8,128)(2,1)}, bf16[704,128]{1,0:T(8,128)(2,1)S(1)}, u32[]{:S(2)}) copy-start(bf16[704,128]{1,0:T(8,128)(2,1)S(1)} %collective-permute-done.9.refs_5_) | copy-start | bytes 540676
  137.9 5.6 %collective-permute-start.10 = (bf16[704,128]{1,0:T(8,128)(2,1)S(1)}, bf16[704,128]{1,0:T(8,128)(2,1)S(1)}, u32[]{:S(2)}, u32[]{:S(2)}) collective-permute-start(bf16[704,128]{1,0:T(8,128)(2,1)S(1)} %collective-permute-done.9.refs_5_), channel_id=1, source_target_pairs={{0,8},{8,16},{16,24},{24,32},{32,40},{40,48},{48,56},{56,64},{64,7... | collective-permute-start | bytes 540680 | tf_op jit(solution)/shard_map/ppermute | solution.py:544
  140.4 3.1 %copy-start.16 = (bf16[704,128]{1,0:T(8,128)(2,1)}, bf16[704,128]{1,0:T(8,128)(2,1)S(1)}, u32[]{:S(2)}) copy-start(bf16[704,128]{1,0:T(8,128)(2,1)S(1)} %collective-permute-done.17.refs_11_) | copy-start | bytes 540676
  140.4 5.6 %collective-permute-start.18 = (bf16[704,128]{1,0:T(8,128)(2,1)S(1)}, bf16[704,128]{1,0:T(8,128)(2,1)}, u32[]{:S(2)}, u32[]{:S(2)}) collective-permute-start(bf16[704,128]{1,0:T(8,128)(2,1)S(1)} %collective-permute-done.17.refs_11_), channel_id=1, source_target_pairs={{0,120},{8,0},{16,8},{24,16},{32,24},{40,32},{48,40},{56,48},{64,5... | collective-permute-start | bytes 540680 | tf_op jit(solution)/shard_map/ppermute | solution.py:547
  143.5 2.4 %copy-start.17 = (bf16[704,128]{1,0:T(8,128)(2,1)}, bf16[704,128]{1,0:T(8,128)(2,1)S(1)}, u32[]{:S(2)}) copy-start(bf16[704,128]{1,0:T(8,128)(2,1)S(1)} %collective-permute-done.10.refs_6_) | copy-start | bytes 540676
  143.5 6.1 %collective-permute-start.11 = (bf16[704,128]{1,0:T(8,128)(2,1)S(1)}, bf16[704,128]{1,0:T(8,128)(2,1)}, u32[]{:S(2)}, u32[]{:S(2)}) collective-permute-start(bf16[704,128]{1,0:T(8,128)(2,1)S(1)} %collective-permute-done.10.refs_6_), channel_id=1, source_target_pairs={{0,8},{8,16},{16,24},{24,32},{32,40},{40,48},{48,56},{56,64},{64,7... | collective-permute-start | bytes 540680 | tf_op jit(solution)/shard_map/ppermute | solution.py:544
  145.9 6.0 %collective-permute-start.19 = (bf16[704,128]{1,0:T(8,128)(2,1)}, bf16[704,128]{1,0:T(8,128)(2,1)}, u32[]{:S(2)}, u32[]{:S(2)}) collective-permute-start(bf16[704,128]{1,0:T(8,128)(2,1)} %collective-permute-done.18.refs_10_), channel_id=1, source_target_pairs={{0,120},{8,0},{16,8},{24,16},{32,24},{40,32},{48,40},{56,48},{64,5... | collective-permute-start | bytes 540680 | tf_op jit(solution)/shard_map/ppermute | solution.py:547
  149.6 7.0 %collective-permute-start.12 = (bf16[704,128]{1,0:T(8,128)(2,1)}, bf16[704,128]{1,0:T(8,128)(2,1)}, u32[]{:S(2)}, u32[]{:S(2)}) collective-permute-start(bf16[704,128]{1,0:T(8,128)(2,1)} %collective-permute-done.11.refs_7_), channel_id=1, source_target_pairs={{0,8},{8,16},{16,24},{24,32},{32,40},{40,48},{48,56},{56,64},{64,7... | collective-permute-start | bytes 540680 | tf_op jit(solution)/shard_map/ppermute | solution.py:544
  156.7 1.0 copy-start.5
  168.1 9.6 %collective-permute-start.20 = (bf16[4,512,256]{2,1,0:T(8,128)(2,1)}, bf16[4,512,256]{2,1,0:T(8,128)(2,1)S(1)}, u32[]{:S(2)}, u32[]{:S(2)}) collective-permute-start(bf16[4,512,256]{2,1,0:T(8,128)(2,1)} %get-tuple-element.33), channel_id=1, source_target_pairs={{0,1},{1,0},{2,3},{3,2},{4,5},{5,4},{6,7},{7,6},{8,9},{9,8},{10,11... | collective-permute-start | bytes 3145736 | tf_op jit(solution)/shard_map/ppermute | solution.py:565
Sparse Core Ops, SparseCore 0:
  9.1 102.8 all-gather.2

commit v4 on v3

--- a/solution.py
+++ b/solution.py
@@ -156,7 +156,8 @@
     raw = step_ref[...].astype(F32)
     step = jnp.maximum(raw, 0.0) + jnp.log1p(jnp.exp(-jnp.abs(raw)))
     stepped_ref[...] = step
-    log_decay = jump_ref[...] - rate_ref[...] * step
+    rate = jnp.concatenate([jnp.full((1, tokens), rate_ref[h], F32) for h in range(heads)])
+    log_decay = jump_ref[...] - rate * step
     held = None
     total = jnp.zeros((heads, 1), F32)
     head_size = wide // heads
@@ -210,6 +211,7 @@
     blocks = tokens // BLOCK
     return pl.pallas_call(
         state_kernel,
+        in_specs=[vmem()] * 4 + [smem()] + [vmem()] * 4,
         out_shape=(
             shape((tokens, wide), BF16),
             shape((tokens, narrow), BF16),
@@ -445,7 +447,7 @@
     )(at, parts, residual)
 
 
-def mixer_kernel(peers, at_ref, mine_ref, other_ref, gain_ref, weight_ref, *refs):
+def mixer_kernel(peers, at_ref, place_ref, group_ref, mine_ref, other_ref, gain_ref, weight_ref, *refs):
     down_refs = refs[:peers]
     out_refs = refs[peers : peers + 2]
     after, normal, late, downs, hidden_ref, out, after_sem, late_sem, down_sem, out_sem = refs[
@@ -453,7 +455,7 @@
     ]
     _, owners, _, share = after.shape
     _, units, _ = downs.shape
-    core, place = at_ref[0], at_ref[1]
+    core, place, group = at_ref[0], place_ref[0], group_ref[0]
 
     loads = [
         pltpu.make_async_copy(ref, after.at[k], after_sem.at[k])
@@ -462,7 +464,8 @@
     heavy = pltpu.make_async_copy(weight_ref, late, late_sem)
     rows = []
     for k, ref in enumerate(down_refs):
-        index = lax.rem(place - k + peers, peers)
+        turn = jnp.where(lax.rem(group, 2) == 0, peers - k, k)
+        index = lax.rem(place + turn, peers)
         rows.append(pltpu.make_async_copy(ref, downs.at[index], down_sem.at[k]))
     for copy in (*loads, heavy):
         copy.start()
@@ -478,8 +481,9 @@
     for flip in range(2):
         for k in range(owners):
             c = 2 * k + (core ^ flip)
-            normal[:, pl.ds(pl.multiple_of(c * share, share), share)] = (
-                after[flip, k].astype(F32) * scale * gain_ref[c].astype(F32)
+            cols = pl.ds(pl.multiple_of(c * share, share), share)
+            normal[:, cols] = (
+                after[flip, k].astype(F32) * scale * gain_ref[:, cols].astype(F32)
             ).astype(BF16)
     heavy.wait()
     for copy in rows:
@@ -507,14 +511,14 @@
         store.wait()
 
 
-def channel_mixer(at, mine, other, gain, weights, downs):
+def channel_mixer(at, place, group, mine, other, gain, weights, downs):
     owners, tokens, share = mine.shape
     peers, units, depth = len(downs), *downs[0].shape
     anywhere = pl.BlockSpec(memory_space=pl.ANY)
     out = shape((owners, tokens, share), BF16)
     return pl.pallas_call(
         functools.partial(mixer_kernel, peers),
-        in_specs=[smem(), anywhere, anywhere, vmem(), anywhere] + [anywhere] * peers,
+        in_specs=[smem()] * 3 + [anywhere, anywhere, vmem(), anywhere] + [anywhere] * peers,
         out_specs=[anywhere, anywhere],
         out_shape=(out, out),
         scratch_shapes=[
@@ -533,19 +537,23 @@
             flops=12 * tokens * owners * share * units, transcendentals=0, bytes_accessed=14_000_000
         ),
         name="channel_mixer",
-    )(at, mine, other, gain, weights, *downs)
-
-
-def ring_of(value, axis):
-    peers = lax.axis_size(axis)
+    )(at, place, group, mine, other, gain, weights, *downs)
+
+
+def gathered(value, axis, groups):
+    peers, count = lax.axis_size(axis), lax.axis_size(groups)
+    around = [
+        (g * peers + i, g * peers + (i + 1 - 2 * (g % 2)) % peers)
+        for g in range(count)
+        for i in range(peers)
+    ]
+    across = [(g, g ^ 1) for g in range(count)]
     found = {0: value}
-    up = down = value
     for k in range(1, peers // 2 + 1):
-        up = lax.ppermute(up, axis, [(i, (i + 1) % peers) for i in range(peers)])
-        found[k] = up
+        value = lax.ppermute(value, (groups, axis), around)
+        found[k] = value
         if k < peers - k:
-            down = lax.ppermute(down, axis, [(i, (i - 1) % peers) for i in range(peers)])
-            found[peers - k] = down
+            found[peers - k] = lax.ppermute(value, groups, across)
     return [found[k] for k in range(peers)]
 
 
@@ -600,30 +608,30 @@
     me = lax.axis_index("tp").astype(jnp.int32)
     at = me.reshape(1)
     core = (me % 2).reshape(1)
-    place = jnp.stack([me % 2, lax.axis_index("sp").astype(jnp.int32)])
+    place = lax.axis_index("sp").astype(jnp.int32).reshape(1)
+    group = lax.axis_index("grp").astype(jnp.int32).reshape(1)
     late = jnp.concatenate([gate_weight.T, up_weight.T], axis=0)
     weights = lax.all_gather(late, "sp", axis=0)
-    downs = ring_of(down_rows.T, "sp")
+    downs = gathered(down_rows.T, "sp", "grp")
 
     docs = documents.reshape(-1, BLOCK)
     before = from_behind(pack_edge(values, writes, reads, docs), "sp", 1)
-    rate = decay_rate.reshape(-1, 1)
     sv, sw, run, step, enter, send = local_states(
-        before, values, writes, step_raw, rate, decay_jump, docs, taps_values, taps_write
+        before, values, writes, step_raw, decay_rate, decay_jump, docs, taps_values, taps_write
     )
     near = from_behind(send, "sp", 1)
+    gains = mixer_gain.reshape(1, -1), channel_gain.reshape(1, -1)
+    near, gains = lax.optimization_barrier((near, gains))
     sr, mixed, reach = local_mix(before, reads, docs, taps_read, sv, sw, run, step, enter)
     joined = join_states(send, near, heads)
     far = from_behind(joined, "sp", 2)
-    gain = mixer_gain.reshape(1, -1)
-    both = project(core, near, far, sr, mixed, reach, out_gate, gain, mixer_out, owners)
+    both = project(core, near, far, sr, mixed, reach, out_gate, gains[0], mixer_out, owners)
     parts = sum_pairs(both)
     parts = exchange(parts)
     own_after, spread = after_mix(at, parts, residual)
     mine = exchange(spread)
     other = to_partner(mine)
-    gain = channel_gain.reshape(2 * owners, 1, -1)
-    both = channel_mixer(place, mine, other, gain, weights, downs)
+    both = channel_mixer(core, place, group, mine, other, gains[1], weights, downs)
     parts = sum_pairs(both)
     parts = exchange(parts)
     return add_down(parts, own_after)

time: 208 us -> 216 us (1.038)
  waiting for transfers between devices: 34 us -> 57.8 us
  starting transfers between devices: 77.8 us -> 65 us
    ppermute x15, waiting for transfers between devices: 26.6 us -> 50.1 us  [the longest x8 37.8 us: gathered(): value = lax.ppermute(value, (groups, axis), around)]
    ppermute x15, starting transfers between devices: 29.1 us -> 14.4 us  [the longest x7 14.2 us: gathered(): found[peers - k] = lax.ppermute(value, groups, across)]
  transfers between devices with their start and end apart: 23 -> 23, of which waited for: 13 -> 17; matrix products, arithmetic and copies ran while one was open for 2% -> 1% of each run, Pallas kernels for 10% -> 10%
where the time goes in v4:
time: 216 us
  starting transfers between devices  65 us (30%)
  waiting for transfers between devices  57.8 us (27%)
  blocking collectives  35.7 us (17%)
  Pallas kernels  33.9 us (16%)
  between operations  13.6 us (6%)
  other arithmetic  4.83 us (2%)
  local copies, waits for them, and re-layouts  4.67 us (2%)
    ppermute x8, waiting for transfers between devices, gathered(): value = lax.ppermute(value, (groups, axis), around)  37.8 us
    all_to_all x2, blocking collectives, exchange(): return lax.all_to_all(value, 'tp', 0, 0, axis_index_groups=rows, tiled=True)  35.7 us
    ppermute x3, starting transfers between devices, to_partner(): lax.ppermute(value, 'tp', [(i, i ^ 1) for i in range(lax.axis_size('tp'))])  29.5 us
    ppermute x3, starting transfers between devices, from_behind(): return lax.ppermute(value, axis, pairs)  17.5 us
    ppermute x7, starting transfers between devices, gathered(): found[peers - k] = lax.ppermute(value, groups, across)  14.2 us
    ppermute x7, waiting for transfers between devices, gathered(): found[peers - k] = lax.ppermute(value, groups, across)  12.3 us
    pallas_call x1, Pallas kernels, channel_mixer(): pl.pallas_call(functools.partial(mixer_kernel, peers), in_specs=[smem()]...  10.4 us
    pallas_call x1, Pallas kernels, project(): pl.pallas_call(project_kernel, in_specs=[smem()] + [vmem()] * 8, out_shap...  6.56 us
  transfers between devices with their start and end apart: 23, of which 17 were waited for; matrix products, arithmetic and copies ran while one was open for 1% of the time, Pallas kernels for 10%

profile of v4, /device:TPU:33, one launch (start us, length us, event | category | flops | bytes accessed | tf_op | source)
XLA Modules:
  0.0 215.5 jit_solution(8313956629374373223)
XLA Ops:
  6.6 1.8 pad_maximum_fusion
  8.4 1.5 pack_edge.1
  9.9 5.2 %collective-permute-start = (bf16[16,896]{1,0:T(8,128)(2,1)}, bf16[16,896]{1,0:T(8,128)(2,1)S(1)}, u32[]{:S(2)}, u32[]{:S(2)}) collective-permute-start(bf16[16,896]{1,0:T(8,128)(2,1)} %pack_edge.1), channel_id=1, source_target_pairs={{0,8},{8,16},{16,24},{24,32},{32,40},{40,48},{48,56},{56,64},{64,7... | collective-permute-start | bytes 86024 | tf_op jit(solution)/shard_map/ppermute | solution.py:24
  15.2 1.2 collective-permute-done.before_ref
  16.4 0.6 copy-done.17
  17.0 5.0 %local_states.1 = (bf16[512,512]{1,0:T(8,128)(2,1)}, bf16[512,128]{1,0:T(8,128)(2,1)}, f32[8,512]{1,0:T(8,128)}, f32[8,512]{1,0:T(8,128)}, bf16[3,512,128]{2,1,0:T(8,128)(2,1)}, /*index=5*/bf16[528,128]{1,0:T(8,128)(2,1)}) custom-call(bf16[16,896]{1,0:T(8,128)(2,1)} %copy-done.17, bf16[512,512]{1,0:T(8,128)(2,1)} %values_ref.3, bf16[512,128]{1,0:T(8,128)(2,1)} %writes_ref.3, ...), custom_call_target="tpu_custom_call" | custom-call | flops 400000000 | bytes 4000000 | tf_op jit(solution)/shard_map/local_states/pallas_call | solution.py:212
  21.9 4.4 %collective-permute-start.1 = (bf16[528,128]{1,0:T(8,128)(2,1)}, bf16[528,128]{1,0:T(8,128)(2,1)S(1)}, u32[]{:S(2)}, u32[]{:S(2)}) collective-permute-start(bf16[528,128]{1,0:T(8,128)(2,1)} %get-tuple-element.23.own_ref), channel_id=1, source_target_pairs={{0,8},{8,16},{16,24},{24,32},{32,40},{40,48},{48,56},{56,64},{64,7... | collective-permute-start | bytes 405512 | tf_op jit(solution)/shard_map/ppermute | solution.py:24
  26.4 0.5 reshape.26.gain_ref
  26.9 0.6 reshape.27.gain_ref
  27.5 1.1 collective-permute-done.1.near_ref
  28.7 0.6 copy-done.1
  29.3 1.7 join_states.1
  31.0 7.9 %collective-permute-start.2 = (bf16[512,128]{1,0:T(8,128)(2,1)}, bf16[512,128]{1,0:T(8,128)(2,1)S(1)}, u32[]{:S(2)}, u32[]{:S(2)}) collective-permute-start(bf16[512,128]{1,0:T(8,128)(2,1)} %join_states.1), channel_id=1, source_target_pairs={{0,16},{8,24},{16,32},{24,40},{32,48},{40,56},{48,64},{56,72},{64,... | collective-permute-start | bytes 393224 | tf_op jit(solution)/shard_map/ppermute | solution.py:24
  38.8 4.1 %local_mix.1 = (bf16[512,128]{1,0:T(8,128)(2,1)}, f32[512,512]{1,0:T(8,128)}, f32[8,512]{1,0:T(8,128)}) custom-call(bf16[16,896]{1,0:T(8,128)(2,1)} %copy-done.17, bf16[512,128]{1,0:T(8,128)(2,1)} %reads_ref.3, s32[4,128]{1,0:T(4,128)} %bitcast.13, bf16[4,128]{1,0:T(4,128)(2,1)} %taps_ref.1, bf16[512,512]{1,0:T(8,128)(2,1)} %get-tuple-element.25.sv_ref, ...), custom_call_target="tpu_custom_call" | custom-call | flops 800000000 | bytes 4000000 | tf_op jit(solution)/shard_map/local_mix/pallas_call | solution.py:333
  43.2 0.7 copy-done.2
  43.9 6.6 %project.1 = (bf16[4,512,256]{2,1,0:T(8,128)(2,1)}, bf16[4,512,256]{2,1,0:T(8,128)(2,1)}) custom-call(s32[1]{0:T(128)} %bitcast.core_ref.at_ref, bf16[528,128]{1,0:T(8,128)(2,1)} %copy-done.1, bf16[512,128]{1,0:T(8,128)(2,1)} %copy-done.2, bf16[512,128]{1,0:T(8,128)(2,1)} %get-tuple-element.30.sr_ref, f32[512,512]{1,0:T(8,128)} %get-tuple-element.31.mixed_ref, ...), custom_call_target="tpu_custom_call" | custom-call | flops 1073741824 | bytes 6000000 | tf_op jit(solution)/shard_map/project/pallas_call | solution.py:407
  50.4 18.1 %collective-permute-start.3 = (bf16[4,512,256]{2,1,0:T(8,128)(2,1)}, bf16[4,512,256]{2,1,0:T(8,128)(2,1)S(1)}, u32[]{:S(2)}, u32[]{:S(2)}) collective-permute-start(bf16[4,512,256]{2,1,0:T(8,128)(2,1)} %get-tuple-element.35), channel_id=1, source_target_pairs={{0,1},{1,0},{2,3},{3,2},{4,5},{5,4},{6,7},{7,6},{8,9},{9,8},{10,11... | collective-permute-start | bytes 3145736 | tf_op jit(solution)/shard_map/ppermute | solution.py:573
  68.6 2.5 %collective-permute-done.3 = bf16[4,512,256]{2,1,0:T(8,128)(2,1)S(1)} collective-permute-done((bf16[4,512,256]{2,1,0:T(8,128)(2,1)}, bf16[4,512,256]{2,1,0:T(8,128)(2,1)S(1)}, u32[]{:S(2)}, u32[]{:S(2)}) %collective-permute-start.3) | collective-permute-done | bytes 1048608 | tf_op jit(solution)/shard_map/ppermute | solution.py:573
  71.1 1.5 add_convert_fusion.1
  72.6 18.0 %all_to_all.15.parts_ref = bf16[4,512,256]{2,1,0:T(8,128)(2,1)} all-to-all(bf16[4,512,256]{2,1,0:T(8,128)(2,1)S(1)} %add_convert_fusion.1), channel_id=1, replica_groups={{0,2,4,6},{1,3,5,7},{8,10,12,14},{9,11,13,15},{16,18,20,22},{17,19,21,2..., dimensions={0} | all-to-all | bytes 2097152 | tf_op jit(solution)/shard_map/all_to_all | solution.py:579
  90.6 2.6 %after_mix.1 = (bf16[512,256]{1,0:T(8,128)(2,1)}, bf16[4,512,256]{2,1,0:T(8,128)(2,1)}) custom-call(s32[1]{0:T(128)} %bitcast.3.at_ref, bf16[4,512,256]{2,1,0:T(8,128)(2,1)} %all_to_all.15.parts_ref, bf16[512,2048]{1,0:T(8,128)(2,1)} %residual_ref.1), custom_call_target="tpu_custom_call" | custom-call | tf_op jit(solution)/shard_map/after_mix/pallas_call | solution.py:431
  93.1 3.6 %all-to-all-start.1 = ((bf16[4,512,256]{2,1,0:T(8,128)(2,1)}), bf16[4,512,256]{2,1,0:T(8,128)(2,1)S(1)}, u32[]{:S(2)}, u32[]{:S(2)}) async-start(bf16[4,512,256]{2,1,0:T(8,128)(2,1)} %get-tuple-element.36), calls=%async_computation.1 | async-start | bytes 2097152 | tf_op jit(solution)/shard_map/all_to_all | solution.py:579
  96.9 16.3 %collective-permute-done.5.refs_1_ = bf16[704,128]{1,0:T(8,128)(2,1)S(1)} collective-permute-done((bf16[704,128]{1,0:T(8,128)(2,1)S(1)}, bf16[704,128]{1,0:T(8,128)(2,1)S(1)}, u32[]{:S(2)}, u32[]{:S(2)}) %collective-permute-start.5) | collective-permute-done | bytes 180256 | tf_op jit(solution)/shard_map/ppermute | solution.py:553
  113.2 6.0 %collective-permute-done.6.refs_2_ = bf16[704,128]{1,0:T(8,128)(2,1)S(1)} collective-permute-done((bf16[704,128]{1,0:T(8,128)(2,1)S(1)}, bf16[704,128]{1,0:T(8,128)(2,1)S(1)}, u32[]{:S(2)}, u32[]{:S(2)}) %collective-permute-start.6) | collective-permute-done | bytes 180256 | tf_op jit(solution)/shard_map/ppermute | solution.py:553
  119.2 2.3 %collective-permute-start.4 = (bf16[4,512,256]{2,1,0:T(8,128)(2,1)S(1)}, bf16[4,512,256]{2,1,0:T(8,128)(2,1)S(1)}, u32[]{:S(2)}, u32[]{:S(2)}) collective-permute-start(bf16[4,512,256]{2,1,0:T(8,128)(2,1)S(1)} %all-to-all-done.1.mine_ref), channel_id=1, source_target_pairs={{0,1},{1,0},{2,3},{3,2},{4,5},{5,4},{6,7},{7,6},{8,9},{9,8},{10,11... | collective-permute-start | bytes 3145736 | tf_op jit(solution)/shard_map/ppermute | solution.py:573
  121.5 3.3 %collective-permute-done.7.refs_3_ = bf16[704,128]{1,0:T(8,128)(2,1)S(1)} collective-permute-done((bf16[704,128]{1,0:T(8,128)(2,1)S(1)}, bf16[704,128]{1,0:T(8,128)(2,1)S(1)}, u32[]{:S(2)}, u32[]{:S(2)}) %collective-permute-start.7) | collective-permute-done | bytes 180256 | tf_op jit(solution)/shard_map/ppermute | solution.py:553
  124.8 5.6 %collective-permute-done.8.refs_4_ = bf16[704,128]{1,0:T(8,128)(2,1)S(1)} collective-permute-done((bf16[704,128]{1,0:T(8,128)(2,1)S(1)}, bf16[704,128]{1,0:T(8,128)(2,1)S(1)}, u32[]{:S(2)}, u32[]{:S(2)}) %collective-permute-start.8) | collective-permute-done | bytes 180256 | tf_op jit(solution)/shard_map/ppermute | solution.py:553
  130.3 5.7 %collective-permute-done.9.refs_5_ = bf16[704,128]{1,0:T(8,128)(2,1)S(1)} collective-permute-done((bf16[704,128]{1,0:T(8,128)(2,1)S(1)}, bf16[704,128]{1,0:T(8,128)(2,1)S(1)}, u32[]{:S(2)}, u32[]{:S(2)}) %collective-permute-start.9) | collective-permute-done | bytes 180256 | tf_op jit(solution)/shard_map/ppermute | solution.py:553
  136.0 4.6 %collective-permute-start.19 = (bf16[704,128]{1,0:T(8,128)(2,1)S(1)}, bf16[704,128]{1,0:T(8,128)(2,1)S(1)}, u32[]{:S(2)}, u32[]{:S(2)}) collective-permute-start(bf16[704,128]{1,0:T(8,128)(2,1)S(1)} %collective-permute-done.5.refs_1_), channel_id=1, source_target_pairs={{0,128},{128,0},{1,129},{129,1},{2,130},{130,2},{3,131},{131,3},{4... | collective-permute-start | bytes 540680 | tf_op jit(solution)/shard_map/ppermute | solution.py:556
  140.7 1.4 collective-permute-start.17
  142.1 0.8 collective-permute-done.10.refs_6_
  142.9 0.6 collective-permute-done.19.refs_15_
  143.5 4.9 %collective-permute-start.16 = (bf16[704,128]{1,0:T(8,128)(2,1)S(1)}, bf16[704,128]{1,0:T(8,128)(2,1)S(1)}, u32[]{:S(2)}, u32[]{:S(2)}) collective-permute-start(bf16[704,128]{1,0:T(8,128)(2,1)S(1)} %collective-permute-done.8.refs_4_), channel_id=1, source_target_pairs={{0,128},{128,0},{1,129},{129,1},{2,130},{130,2},{3,131},{131,3},{4... | collective-permute-start | bytes 540680 | tf_op jit(solution)/shard_map/ppermute | solution.py:556
  148.6 1.3 collective-permute-start.14
  149.9 0.3 collective-permute-done.11.refs_7_
  150.2 1.8 collective-permute-start.13
  151.9 0.7 collective-permute-done.16.refs_12_
  152.7 0.7 copy-done.16
  153.4 3.3 %collective-permute-done.15.refs_11_ = bf16[704,128]{1,0:T(8,128)(2,1)} collective-permute-done((bf16[704,128]{1,0:T(8,128)(2,1)S(1)}, bf16[704,128]{1,0:T(8,128)(2,1)}, u32[]{:S(2)}, u32[]{:S(2)}) %collective-permute-start.15) | collective-permute-done | bytes 180256 | tf_op jit(solution)/shard_map/ppermute | solution.py:556
  156.7 3.8 %collective-permute-done.14.refs_10_ = bf16[704,128]{1,0:T(8,128)(2,1)} collective-permute-done((bf16[704,128]{1,0:T(8,128)(2,1)S(1)}, bf16[704,128]{1,0:T(8,128)(2,1)}, u32[]{:S(2)}, u32[]{:S(2)}) %collective-permute-start.14) | collective-permute-done | bytes 180256 | tf_op jit(solution)/shard_map/ppermute | solution.py:556
  160.4 3.9 %collective-permute-done.13.refs_9_ = bf16[704,128]{1,0:T(8,128)(2,1)} collective-permute-done((bf16[704,128]{1,0:T(8,128)(2,1)}, bf16[704,128]{1,0:T(8,128)(2,1)}, u32[]{:S(2)}, u32[]{:S(2)}) %collective-permute-start.13) | collective-permute-done | bytes 180256 | tf_op jit(solution)/shard_map/ppermute | solution.py:556
  164.4 0.9 copy-done.5
  165.3 10.4 %channel_mixer.1 = (bf16[4,512,256]{2,1,0:T(8,128)(2,1)}, bf16[4,512,256]{2,1,0:T(8,128)(2,1)}) custom-call(s32[1]{0:T(128)} %bitcast.core_ref.at_ref, s32[1]{0:T(128)} %bitcast.1.place_ref, s32[1]{0:T(128)} %bitcast.2.group_ref, bf16[4,512,256]{2,1,0:T(8,128)(2,1)} %copy-done, bf16[4,512,256]{2,1,0:T(8,128)(2,1)} %copy-done.5, ...), custom_call_target="tpu_custom_call" | custom-call | flops 4429185024 | bytes 14000000 | tf_op jit(solution)/shard_map/channel_mixer/pallas_call | solution.py:519
  175.7 9.1 %collective-permute-start.20 = (bf16[4,512,256]{2,1,0:T(8,128)(2,1)}, bf16[4,512,256]{2,1,0:T(8,128)(2,1)S(1)}, u32[]{:S(2)}, u32[]{:S(2)}) collective-permute-start(bf16[4,512,256]{2,1,0:T(8,128)(2,1)} %get-tuple-element.39), channel_id=1, source_target_pairs={{0,1},{1,0},{2,3},{3,2},{4,5},{5,4},{6,7},{7,6},{8,9},{9,8},{10,11... | collective-permute-start | bytes 3145736 | tf_op jit(solution)/shard_map/ppermute | solution.py:573
  184.8 2.5 %collective-permute-done.20 = bf16[4,512,256]{2,1,0:T(8,128)(2,1)S(1)} collective-permute-done((bf16[4,512,256]{2,1,0:T(8,128)(2,1)}, bf16[4,512,256]{2,1,0:T(8,128)(2,1)S(1)}, u32[]{:S(2)}, u32[]{:S(2)}) %collective-permute-start.20) | collective-permute-done | bytes 1048608 | tf_op jit(solution)/shard_map/ppermute | solution.py:573
  187.3 1.5 add_convert_fusion
  188.8 17.7 %all_to_all.16.parts_ref = bf16[4,512,256]{2,1,0:T(8,128)(2,1)} all-to-all(bf16[4,512,256]{2,1,0:T(8,128)(2,1)S(1)} %add_convert_fusion), channel_id=1, replica_groups={{0,2,4,6},{1,3,5,7},{8,10,12,14},{9,11,13,15},{16,18,20,22},{17,19,21,2..., dimensions={0} | all-to-all | bytes 2097152 | tf_op jit(solution)/shard_map/all_to_all | solution.py:579
  206.5 2.1 add_down.1
  (50 shorter events, 0.7 us)
Async XLA Ops:
  6.5 19.8 %copy-start.4 = (bf16[512]{0:T(512)(128)(2,1)S(1)}, bf16[512]{0:T(512)(128)(2,1)}, u32[]{:S(2)}) copy-start(bf16[512]{0:T(512)(128)(2,1)} %param.30) | copy-start | bytes 3076
  6.5 20.4 %copy-start.3 = (bf16[2048]{0:T(1024)(128)(2,1)S(1)}, bf16[2048]{0:T(1024)(128)(2,1)}, u32[]{:S(2)}) copy-start(bf16[2048]{0:T(1024)(128)(2,1)} %param.32) | copy-start | bytes 12292
  6.6 157.8 %all-gather.3.cloned.1.call-start = ((), (), s32[]{:S(2)}) async-start(), calls=%async_computation.3 | async-start | bytes 6127616 | tf_op jit(solution)/shard_map/all_gather | solution.py:614
  9.9 6.4 %collective-permute-start = (bf16[16,896]{1,0:T(8,128)(2,1)}, bf16[16,896]{1,0:T(8,128)(2,1)S(1)}, u32[]{:S(2)}, u32[]{:S(2)}) collective-permute-start(bf16[16,896]{1,0:T(8,128)(2,1)} %pack_edge.1), channel_id=1, source_target_pairs={{0,8},{8,16},{16,24},{24,32},{32,40},{40,48},{48,56},{56,64},{64,7... | collective-permute-start | bytes 86024 | tf_op jit(solution)/shard_map/ppermute | solution.py:24
  16.4 0.6 copy-start.17
  21.9 6.7 %collective-permute-start.1 = (bf16[528,128]{1,0:T(8,128)(2,1)}, bf16[528,128]{1,0:T(8,128)(2,1)S(1)}, u32[]{:S(2)}, u32[]{:S(2)}) collective-permute-start(bf16[528,128]{1,0:T(8,128)(2,1)} %get-tuple-element.23.own_ref), channel_id=1, source_target_pairs={{0,8},{8,16},{16,24},{24,32},{32,40},{40,48},{48,56},{56,64},{64,7... | collective-permute-start | bytes 405512 | tf_op jit(solution)/shard_map/ppermute | solution.py:24
  28.7 0.6 copy-start.1
  31.0 12.2 %collective-permute-start.2 = (bf16[512,128]{1,0:T(8,128)(2,1)}, bf16[512,128]{1,0:T(8,128)(2,1)S(1)}, u32[]{:S(2)}, u32[]{:S(2)}) collective-permute-start(bf16[512,128]{1,0:T(8,128)(2,1)} %join_states.1), channel_id=1, source_target_pairs={{0,16},{8,24},{16,32},{24,40},{32,48},{40,56},{48,64},{56,72},{64,... | collective-permute-start | bytes 393224 | tf_op jit(solution)/shard_map/ppermute | solution.py:24
  43.2 0.7 copy-start.2
  50.4 20.6 %collective-permute-start.3 = (bf16[4,512,256]{2,1,0:T(8,128)(2,1)}, bf16[4,512,256]{2,1,0:T(8,128)(2,1)S(1)}, u32[]{:S(2)}, u32[]{:S(2)}) collective-permute-start(bf16[4,512,256]{2,1,0:T(8,128)(2,1)} %get-tuple-element.35), channel_id=1, source_target_pairs={{0,1},{1,0},{2,3},{3,2},{4,5},{5,4},{6,7},{7,6},{8,9},{9,8},{10,11... | collective-permute-start | bytes 3145736 | tf_op jit(solution)/shard_map/ppermute | solution.py:573
  90.6 6.2 %copy-start.6 = (bf16[128,704]{0,1:T(8,128)(2,1)S(1)}, bf16[128,704]{0,1:T(8,128)(2,1)}, u32[]{:S(2)}) copy-start(bf16[128,704]{0,1:T(8,128)(2,1)} %param.35) | copy-start | bytes 540676
  93.1 26.1 %all-to-all-start.1 = ((bf16[4,512,256]{2,1,0:T(8,128)(2,1)}), bf16[4,512,256]{2,1,0:T(8,128)(2,1)S(1)}, u32[]{:S(2)}, u32[]{:S(2)}) async-start(bf16[4,512,256]{2,1,0:T(8,128)(2,1)} %get-tuple-element.36), calls=%async_computation.1 | async-start | bytes 2097152 | tf_op jit(solution)/shard_map/all_to_all | solution.py:579
  96.8 16.4 %collective-permute-start.5 = (bf16[704,128]{1,0:T(8,128)(2,1)S(1)}, bf16[704,128]{1,0:T(8,128)(2,1)S(1)}, u32[]{:S(2)}, u32[]{:S(2)}) collective-permute-start(bf16[704,128]{1,0:T(8,128)(2,1)S(1)} %bitcast.16), channel_id=1, source_target_pairs={{0,8},{8,16},{16,24},{24,32},{32,40},{40,48},{48,56},{56,64},{64,7... | collective-permute-start | bytes 540680 | tf_op jit(solution)/shard_map/ppermute | solution.py:553
  113.2 51.1 %copy-start.7 = (bf16[704,128]{1,0:T(8,128)(2,1)}, bf16[704,128]{1,0:T(8,128)(2,1)S(1)}, u32[]{:S(2)}) copy-start(bf16[704,128]{1,0:T(8,128)(2,1)S(1)} %collective-permute-done.5.refs_1_) | copy-start | bytes 540676
  113.2 6.0 %collective-permute-start.6 = (bf16[704,128]{1,0:T(8,128)(2,1)S(1)}, bf16[704,128]{1,0:T(8,128)(2,1)S(1)}, u32[]{:S(2)}, u32[]{:S(2)}) collective-permute-start(bf16[704,128]{1,0:T(8,128)(2,1)S(1)} %collective-permute-done.5.refs_1_), channel_id=1, source_target_pairs={{0,8},{8,16},{16,24},{24,32},{32,40},{40,48},{48,56},{56,64},{64,7... | collective-permute-start | bytes 540680 | tf_op jit(solution)/shard_map/ppermute | solution.py:553
  119.2 45.1 %copy-start.8 = (bf16[704,128]{1,0:T(8,128)(2,1)}, bf16[704,128]{1,0:T(8,128)(2,1)S(1)}, u32[]{:S(2)}) copy-start(bf16[704,128]{1,0:T(8,128)(2,1)S(1)} %collective-permute-done.6.refs_2_) | copy-start | bytes 540676
  119.2 5.6 %collective-permute-start.7 = (bf16[704,128]{1,0:T(8,128)(2,1)S(1)}, bf16[704,128]{1,0:T(8,128)(2,1)S(1)}, u32[]{:S(2)}, u32[]{:S(2)}) collective-permute-start(bf16[704,128]{1,0:T(8,128)(2,1)S(1)} %collective-permute-done.6.refs_2_), channel_id=1, source_target_pairs={{0,8},{8,16},{16,24},{24,32},{32,40},{40,48},{48,56},{56,64},{64,7... | collective-permute-start | bytes 540680 | tf_op jit(solution)/shard_map/ppermute | solution.py:553
  119.2 45.1 %copy-start = (bf16[4,512,256]{2,1,0:T(8,128)(2,1)}, bf16[4,512,256]{2,1,0:T(8,128)(2,1)S(1)}, u32[]{:S(2)}) copy-start(bf16[4,512,256]{2,1,0:T(8,128)(2,1)S(1)} %all-to-all-done.1.mine_ref) | copy-start | bytes 3145732
  119.2 45.0 %collective-permute-start.4 = (bf16[4,512,256]{2,1,0:T(8,128)(2,1)S(1)}, bf16[4,512,256]{2,1,0:T(8,128)(2,1)S(1)}, u32[]{:S(2)}, u32[]{:S(2)}) collective-permute-start(bf16[4,512,256]{2,1,0:T(8,128)(2,1)S(1)} %all-to-all-done.1.mine_ref), channel_id=1, source_target_pairs={{0,1},{1,0},{2,3},{3,2},{4,5},{5,4},{6,7},{7,6},{8,9},{9,8},{10,11... | collective-permute-start | bytes 3145736 | tf_op jit(solution)/shard_map/ppermute | solution.py:573
  124.8 39.6 %copy-start.9 = (bf16[704,128]{1,0:T(8,128)(2,1)}, bf16[704,128]{1,0:T(8,128)(2,1)S(1)}, u32[]{:S(2)}) copy-start(bf16[704,128]{1,0:T(8,128)(2,1)S(1)} %collective-permute-done.7.refs_3_) | copy-start | bytes 540676
  124.8 5.6 %collective-permute-start.8 = (bf16[704,128]{1,0:T(8,128)(2,1)S(1)}, bf16[704,128]{1,0:T(8,128)(2,1)S(1)}, u32[]{:S(2)}, u32[]{:S(2)}) collective-permute-start(bf16[704,128]{1,0:T(8,128)(2,1)S(1)} %collective-permute-done.7.refs_3_), channel_id=1, source_target_pairs={{0,8},{8,16},{16,24},{24,32},{32,40},{40,48},{48,56},{56,64},{64,7... | collective-permute-start | bytes 540680 | tf_op jit(solution)/shard_map/ppermute | solution.py:553
  130.3 34.0 %copy-start.10 = (bf16[704,128]{1,0:T(8,128)(2,1)}, bf16[704,128]{1,0:T(8,128)(2,1)S(1)}, u32[]{:S(2)}) copy-start(bf16[704,128]{1,0:T(8,128)(2,1)S(1)} %collective-permute-done.8.refs_4_) | copy-start | bytes 540676
  130.3 5.7 %collective-permute-start.9 = (bf16[704,128]{1,0:T(8,128)(2,1)S(1)}, bf16[704,128]{1,0:T(8,128)(2,1)S(1)}, u32[]{:S(2)}, u32[]{:S(2)}) collective-permute-start(bf16[704,128]{1,0:T(8,128)(2,1)S(1)} %collective-permute-done.8.refs_4_), channel_id=1, source_target_pairs={{0,8},{8,16},{16,24},{24,32},{32,40},{40,48},{48,56},{56,64},{64,7... | collective-permute-start | bytes 540680 | tf_op jit(solution)/shard_map/ppermute | solution.py:553
  136.0 28.3 %copy-start.11 = (bf16[704,128]{1,0:T(8,128)(2,1)}, bf16[704,128]{1,0:T(8,128)(2,1)S(1)}, u32[]{:S(2)}) copy-start(bf16[704,128]{1,0:T(8,128)(2,1)S(1)} %collective-permute-done.9.refs_5_) | copy-start | bytes 540676
  136.0 6.8 %collective-permute-start.10 = (bf16[704,128]{1,0:T(8,128)(2,1)S(1)}, bf16[704,128]{1,0:T(8,128)(2,1)S(1)}, u32[]{:S(2)}, u32[]{:S(2)}) collective-permute-start(bf16[704,128]{1,0:T(8,128)(2,1)S(1)} %collective-permute-done.9.refs_5_), channel_id=1, source_target_pairs={{0,8},{8,16},{16,24},{24,32},{32,40},{40,48},{48,56},{56,64},{64,7... | collective-permute-start | bytes 540680 | tf_op jit(solution)/shard_map/ppermute | solution.py:553
  136.0 7.5 %collective-permute-start.19 = (bf16[704,128]{1,0:T(8,128)(2,1)S(1)}, bf16[704,128]{1,0:T(8,128)(2,1)S(1)}, u32[]{:S(2)}, u32[]{:S(2)}) collective-permute-start(bf16[704,128]{1,0:T(8,128)(2,1)S(1)} %collective-permute-done.5.refs_1_), channel_id=1, source_target_pairs={{0,128},{128,0},{1,129},{129,1},{2,130},{130,2},{3,131},{131,3},{4... | collective-permute-start | bytes 540680 | tf_op jit(solution)/shard_map/ppermute | solution.py:556
  140.7 7.8 %collective-permute-start.18 = (bf16[704,128]{1,0:T(8,128)(2,1)S(1)}, bf16[704,128]{1,0:T(8,128)(2,1)S(1)}, u32[]{:S(2)}, u32[]{:S(2)}) collective-permute-start(bf16[704,128]{1,0:T(8,128)(2,1)S(1)} %collective-permute-done.6.refs_2_), channel_id=1, source_target_pairs={{0,128},{128,0},{1,129},{129,1},{2,130},{130,2},{3,131},{131,3},{4... | collective-permute-start | bytes 540680 | tf_op jit(solution)/shard_map/ppermute | solution.py:556
  140.7 7.9 %collective-permute-start.17 = (bf16[704,128]{1,0:T(8,128)(2,1)S(1)}, bf16[704,128]{1,0:T(8,128)(2,1)S(1)}, u32[]{:S(2)}, u32[]{:S(2)}) collective-permute-start(bf16[704,128]{1,0:T(8,128)(2,1)S(1)} %collective-permute-done.7.refs_3_), channel_id=1, source_target_pairs={{0,128},{128,0},{1,129},{129,1},{2,130},{130,2},{3,131},{131,3},{4... | collective-permute-start | bytes 540680 | tf_op jit(solution)/shard_map/ppermute | solution.py:556
  142.9 21.5 %copy-start.12 = (bf16[704,128]{1,0:T(8,128)(2,1)}, bf16[704,128]{1,0:T(8,128)(2,1)S(1)}, u32[]{:S(2)}) copy-start(bf16[704,128]{1,0:T(8,128)(2,1)S(1)} %collective-permute-done.10.refs_6_) | copy-start | bytes 540676
  142.9 7.3 %collective-permute-start.11 = (bf16[704,128]{1,0:T(8,128)(2,1)S(1)}, bf16[704,128]{1,0:T(8,128)(2,1)}, u32[]{:S(2)}, u32[]{:S(2)}) collective-permute-start(bf16[704,128]{1,0:T(8,128)(2,1)S(1)} %collective-permute-done.10.refs_6_), channel_id=1, source_target_pairs={{0,8},{8,16},{16,24},{24,32},{32,40},{40,48},{48,56},{56,64},{64,7... | collective-permute-start | bytes 540680 | tf_op jit(solution)/shard_map/ppermute | solution.py:553
  143.5 20.8 %copy-start.13 = (bf16[704,128]{1,0:T(8,128)(2,1)}, bf16[704,128]{1,0:T(8,128)(2,1)S(1)}, u32[]{:S(2)}) copy-start(bf16[704,128]{1,0:T(8,128)(2,1)S(1)} %collective-permute-done.19.refs_15_) | copy-start | bytes 540676
  143.5 9.1 %collective-permute-start.16 = (bf16[704,128]{1,0:T(8,128)(2,1)S(1)}, bf16[704,128]{1,0:T(8,128)(2,1)S(1)}, u32[]{:S(2)}, u32[]{:S(2)}) collective-permute-start(bf16[704,128]{1,0:T(8,128)(2,1)S(1)} %collective-permute-done.8.refs_4_), channel_id=1, source_target_pairs={{0,128},{128,0},{1,129},{129,1},{2,130},{130,2},{3,131},{131,3},{4... | collective-permute-start | bytes 540680 | tf_op jit(solution)/shard_map/ppermute | solution.py:556
  148.4 16.0 %copy-start.14 = (bf16[704,128]{1,0:T(8,128)(2,1)}, bf16[704,128]{1,0:T(8,128)(2,1)S(1)}, u32[]{:S(2)}) copy-start(bf16[704,128]{1,0:T(8,128)(2,1)S(1)} %collective-permute-done.18.refs_14_) | copy-start | bytes 540676
  148.4 8.2 %collective-permute-start.15 = (bf16[704,128]{1,0:T(8,128)(2,1)S(1)}, bf16[704,128]{1,0:T(8,128)(2,1)}, u32[]{:S(2)}, u32[]{:S(2)}) collective-permute-start(bf16[704,128]{1,0:T(8,128)(2,1)S(1)} %collective-permute-done.9.refs_5_), channel_id=1, source_target_pairs={{0,128},{128,0},{1,129},{129,1},{2,130},{130,2},{3,131},{131,3},{4... | collective-permute-start | bytes 540680 | tf_op jit(solution)/shard_map/ppermute | solution.py:556
  148.6 4.1 %copy-start.15 = (bf16[704,128]{1,0:T(8,128)(2,1)}, bf16[704,128]{1,0:T(8,128)(2,1)S(1)}, u32[]{:S(2)}) copy-start(bf16[704,128]{1,0:T(8,128)(2,1)S(1)} %collective-permute-done.17.refs_13_) | copy-start | bytes 540676
  148.6 11.8 %collective-permute-start.14 = (bf16[704,128]{1,0:T(8,128)(2,1)S(1)}, bf16[704,128]{1,0:T(8,128)(2,1)}, u32[]{:S(2)}, u32[]{:S(2)}) collective-permute-start(bf16[704,128]{1,0:T(8,128)(2,1)S(1)} %collective-permute-done.10.refs_6_), channel_id=1, source_target_pairs={{0,128},{128,0},{1,129},{129,1},{2,130},{130,2},{3,131},{131,3},{4... | collective-permute-start | bytes 540680 | tf_op jit(solution)/shard_map/ppermute | solution.py:556
  150.2 14.1 %collective-permute-start.13 = (bf16[704,128]{1,0:T(8,128)(2,1)}, bf16[704,128]{1,0:T(8,128)(2,1)}, u32[]{:S(2)}, u32[]{:S(2)}) collective-permute-start(bf16[704,128]{1,0:T(8,128)(2,1)} %collective-permute-done.11.refs_7_), channel_id=1, source_target_pairs={{0,128},{128,0},{1,129},{129,1},{2,130},{130,2},{3,131},{131,3},{4... | collective-permute-start | bytes 540680 | tf_op jit(solution)/shard_map/ppermute | solution.py:556
  152.7 0.7 copy-start.16
  153.4 10.9 %collective-permute-start.12 = (bf16[704,128]{1,0:T(8,128)(2,1)}, bf16[704,128]{1,0:T(8,128)(2,1)}, u32[]{:S(2)}, u32[]{:S(2)}) collective-permute-start(bf16[704,128]{1,0:T(8,128)(2,1)} %collective-permute-done.11.refs_7_), channel_id=1, source_target_pairs={{0,8},{8,16},{16,24},{24,32},{32,40},{40,48},{48,56},{56,64},{64,7... | collective-permute-start | bytes 540680 | tf_op jit(solution)/shard_map/ppermute | solution.py:553
  164.3 1.0 copy-start.5
  175.7 11.6 %collective-permute-start.20 = (bf16[4,512,256]{2,1,0:T(8,128)(2,1)}, bf16[4,512,256]{2,1,0:T(8,128)(2,1)S(1)}, u32[]{:S(2)}, u32[]{:S(2)}) collective-permute-start(bf16[4,512,256]{2,1,0:T(8,128)(2,1)} %get-tuple-element.39), channel_id=1, source_target_pairs={{0,1},{1,0},{2,3},{3,2},{4,5},{5,4},{6,7},{7,6},{8,9},{9,8},{10,11... | collective-permute-start | bytes 3145736 | tf_op jit(solution)/shard_map/ppermute | solution.py:573
Sparse Core Ops, SparseCore 0:
  9.2 102.9 all-gather.2

commit v5 on v2

--- a/solution.py
+++ b/solution.py
@@ -7,8 +7,7 @@
 from jax.experimental.pallas import tpu as pltpu
 from jax.sharding import PartitionSpec as P
 
-HEADS = 64
-GROUPS = 8
+
 BLOCK = 128
 EDGE = 16
 LANES = 128
@@ -273,7 +272,6 @@
     tokens, narrow = reads_ref.shape
     wide = sv_ref.shape[1]
     blocks = tokens // BLOCK
-    heads = step_ref.shape[0]
     docs = doc_rows(docs_ref)
     place_docs(dext_ref, before_ref.at[:, wide + 2 * narrow :], docs, blocks)
     ext_ref[0:EDGE] = before_ref[:, wide + narrow : wide + 2 * narrow].astype(F32)
@@ -447,108 +445,178 @@
     )(at, parts, residual)
 
 
-def mixer_kernel(at_ref, mine_ref, other_ref, gain_ref, weight_ref, *refs):
-    out_refs = refs[:2]
-    after, normal, late, downs, hidden_ref, out, after_sem, late_sem, down_sem, out_sem = refs[2:]
-    _, owners, tokens, share = after.shape
-    peers, _, depth = weight_ref.shape
-    units = hidden_ref.shape[1]
-    core = at_ref[0]
-
-    loads = [
-        pltpu.make_async_copy(ref, after.at[k], after_sem.at[k])
-        for k, ref in enumerate((mine_ref, other_ref))
-    ]
-    heavy, rows = [], []
-    for k in range(peers):
-        cols = pl.ds(k * depth, depth)
-        heavy.append(
-            pltpu.make_async_copy(
-                weight_ref.at[k, pl.ds(0, 2 * units)], late.at[:, cols], late_sem.at[k]
-            )
-        )
-        rows.append(
-            pltpu.make_async_copy(
-                weight_ref.at[k, pl.ds(2 * units, units)], downs.at[:, cols], down_sem.at[k]
-            )
-        )
-    for copy in (*loads, *heavy, *rows):
-        copy.start()
-
-    for copy in loads:
-        copy.wait()
+def normal_kernel(at_ref, mine_ref, other_ref, gain_ref, out_ref):
+    owners, _, share = mine_ref.shape
+    core = lax.rem(at_ref[0], 2)
     square = None
-    for flip in range(2):
+    for ref in (mine_ref, other_ref):
         for k in range(owners):
-            x = after[flip, k].astype(F32)
+            x = ref[k].astype(F32)
             square = x * x if square is None else square + x * x
     scale = lax.rsqrt(jnp.sum(square, axis=1, keepdims=True) / (2 * owners * share) + norm_eps)
-    for flip in range(2):
+    for flip, ref in enumerate((mine_ref, other_ref)):
         for k in range(owners):
             c = 2 * k + (core ^ flip)
-            normal[:, pl.ds(pl.multiple_of(c * share, share), share)] = (
-                after[flip, k].astype(F32) * scale * gain_ref[c].astype(F32)
+            cols = pl.ds(pl.multiple_of(c * share, share), share)
+            out_ref[:, cols] = (
+                ref[k].astype(F32) * scale * gain_ref[:, cols].astype(F32)
             ).astype(BF16)
-    for copy in heavy:
+
+
+def normalised(at, mine, other, gain):
+    owners, tokens, share = mine.shape
+    return pl.pallas_call(
+        normal_kernel,
+        in_specs=[smem(), vmem(), vmem(), vmem()],
+        out_shape=shape((tokens, 2 * owners * share), BF16),
+        name="normalised",
+    )(at, mine, other, gain)
+
+
+def mixer_kernel(tiles, at_ref, normal_ref, weight_ref, *refs):
+    mine_far, other_far, mine_near, other_near = refs[:4]
+    late, downs, hidden_ref, far, near, late_sem, down_sem, far_sem, near_sem = refs[4:]
+    peers, units, _ = downs.shape
+    _, turns, _, _ = near.shape
+    core, chip = lax.rem(at_ref[0], 2), lax.div(at_ref[0], 2)
+
+    heavy = []
+    for t, (first, count) in enumerate(tiles):
+        heavy.append(
+            [
+                pltpu.make_async_copy(
+                    weight_ref.at[:, pl.ds(base + first, count)],
+                    late.at[:, pl.ds(base + first, count)],
+                    late_sem.at[t, half],
+                )
+                for half, base in enumerate((0, units))
+            ]
+        )
+    heavy.append([pltpu.make_async_copy(weight_ref.at[:, pl.ds(2 * units, units)], downs, down_sem)])
+    for copy in (*heavy[0], *heavy[1]):
+        copy.start()
+    across = (((1,), (1,)), ((), ()))
+    normal = normal_ref[...]
+    for t, (first, count) in enumerate(tiles):
+        for copy in heavy[t]:
+            copy.wait()
+        if t + 2 < len(heavy):
+            for copy in heavy[t + 2]:
+                copy.start()
+        products = []
+        for base in (first, units + first):
+            part = jnp.concatenate([late[k, base : base + count] for k in range(peers)], axis=1)
+            products.append(
+                lax.dot_general(normal, part, across, preferred_element_type=F32)
+            )
+        hidden_ref[:, first : first + count] = (silu(products[0]) * products[1]).astype(BF16)
+    heavy[-1][0].wait()
+    hidden = hidden_ref[...]
+    stores = []
+
+    def store(source, target, sem):
+        copy = pltpu.make_async_copy(source, target, sem)
+        copy.start()
+        stores.append(copy)
+
+    for turn in (2, 0, 1, 3):
+        for flip in (1, 0):
+            c = 2 * lax.rem(chip + turn, turns + 1) + (core ^ flip)
+            part = jnp.concatenate([downs[2 * c], downs[2 * c + 1]], axis=1)
+            product = jnp.dot(hidden, part, preferred_element_type=F32).astype(BF16)
+            if turn == 2:
+                far[flip] = product
+                store(far.at[flip], (mine_far, other_far)[flip], far_sem.at[flip])
+            else:
+                k = (0, 1, None, 2)[turn]
+                near[flip, k] = product
+                store(near.at[flip, k], (mine_near, other_near)[flip].at[k], near_sem.at[flip, k])
+    for copy in stores:
         copy.wait()
-    across = (((1,), (1,)), ((), ()))
-    gate = lax.dot_general(normal[...], late[0:units], across, preferred_element_type=F32)
-    up = lax.dot_general(normal[...], late[units:], across, preferred_element_type=F32)
-    hidden_ref[...] = (silu(gate) * up).astype(BF16)
-    for copy in rows:
-        copy.wait()
-    stores = []
-    for flip in (1, 0):
-        for k in range(owners):
-            c = 2 * k + (core ^ flip)
-            part = downs[:, pl.ds(pl.multiple_of(c * share, share), share)]
-            out[flip, k] = jnp.dot(hidden_ref[...], part, preferred_element_type=F32).astype(BF16)
-        store = pltpu.make_async_copy(out.at[flip], out_refs[flip], out_sem.at[flip])
-        store.start()
-        stores.append(store)
-    for store in stores:
-        store.wait()
-
-
-def channel_mixer(core, mine, other, gain, weights):
-    owners, tokens, share = mine.shape
+
+
+def channel_mixer(at, normal, weights, share):
+    tokens = normal.shape[0]
     peers, units, depth = weights.shape[0], weights.shape[1] // 3, weights.shape[2]
+    turns = normal.shape[1] // (2 * share) - 1
+    tiles = [(f, min(256, units - f)) for f in range(0, units, 256)]
     anywhere = pl.BlockSpec(memory_space=pl.ANY)
-    out = shape((owners, tokens, share), BF16)
+    far, near = shape((tokens, share), BF16), shape((turns, tokens, share), BF16)
     return pl.pallas_call(
-        mixer_kernel,
-        in_specs=[smem(), anywhere, anywhere, vmem(), anywhere],
-        out_specs=[anywhere, anywhere],
-        out_shape=(out, out),
+        functools.partial(mixer_kernel, tiles),
+        in_specs=[smem(), vmem(), anywhere],
+        out_specs=[anywhere] * 4,
+        out_shape=(far, far, near, near),
         scratch_shapes=[
-            pltpu.VMEM((2, owners, tokens, share), BF16),
-            pltpu.VMEM((tokens, peers * depth), BF16),
-            pltpu.VMEM((2 * units, peers * depth), BF16),
-            pltpu.VMEM((units, peers * depth), BF16),
+            pltpu.VMEM((peers, 2 * units, depth), BF16),
+            pltpu.VMEM((peers, units, depth), BF16),
             pltpu.VMEM((tokens, units), BF16),
-            pltpu.VMEM((2, owners, tokens, share), BF16),
+            pltpu.VMEM((2, tokens, share), BF16),
+            pltpu.VMEM((2, turns, tokens, share), BF16),
+            pltpu.SemaphoreType.DMA((len(tiles), 2)),
+            pltpu.SemaphoreType.DMA,
             pltpu.SemaphoreType.DMA((2,)),
-            pltpu.SemaphoreType.DMA((peers,)),
-            pltpu.SemaphoreType.DMA((peers,)),
-            pltpu.SemaphoreType.DMA((2,)),
+            pltpu.SemaphoreType.DMA((2, turns)),
         ],
         cost_estimate=pl.CostEstimate(
-            flops=12 * tokens * owners * share * units, transcendentals=0, bytes_accessed=14_000_000
+            flops=6 * tokens * normal.shape[1] * units, transcendentals=0, bytes_accessed=14_000_000
         ),
         name="channel_mixer",
-    )(core, mine, other, gain, weights)
-
-
-def out_kernel(parts_ref, own_ref, out_ref):
-    total = None
-    for k in range(parts_ref.shape[0]):
-        part = parts_ref[k].astype(F32)
-        total = part if total is None else total + part
-    out_ref[...] = (own_ref[...].astype(F32) + total).astype(BF16)
-
-
-def add_down(parts, own):
-    return pl.pallas_call(out_kernel, out_shape=shape(own.shape, BF16), name="add_down")(parts, own)
+    )(at, normal, weights)
+
+
+def halves_kernel(mine_ref, other_ref, low_ref, high_ref):
+    half = low_ref.shape[0]
+    low_ref[...] = (mine_ref[:half].astype(F32) + other_ref[:half].astype(F32)).astype(BF16)
+    high_ref[...] = (mine_ref[half:].astype(F32) + other_ref[half:].astype(F32)).astype(BF16)
+
+
+def halves(mine, other):
+    part = shape((mine.shape[0] // 2, mine.shape[1]), BF16)
+    return pl.pallas_call(halves_kernel, out_shape=(part, part), name="halves")(mine, other)
+
+
+def onward_kernel(mine_ref, other_ref, low_ref, high_ref, own_ref, right_ref, left_ref):
+    half = low_ref.shape[0]
+    for k, ref in enumerate((own_ref, right_ref, left_ref)):
+        for rows in (slice(0, half), slice(half, 2 * half)):
+            total = mine_ref[k, rows].astype(F32) + other_ref[k, rows].astype(F32)
+            if k == 1 and rows.start == 0:
+                total = total + low_ref[...].astype(F32)
+            if k == 2 and rows.start > 0:
+                total = total + high_ref[...].astype(F32)
+            ref[rows] = total.astype(BF16)
+
+
+def onward(mine, other, low, high):
+    part = shape(mine.shape[1:], BF16)
+    return pl.pallas_call(onward_kernel, out_shape=(part,) * 3, name="onward")(mine, other, low, high)
+
+
+def last_kernel(after_ref, own_ref, right_ref, left_ref, out_ref):
+    down = own_ref[...].astype(F32) + right_ref[...].astype(F32) + left_ref[...].astype(F32)
+    out_ref[...] = (after_ref[...].astype(F32) + down).astype(BF16)
+
+
+def add_last(after, own, right, left):
+    return pl.pallas_call(last_kernel, out_shape=shape(after.shape, BF16), name="add_last")(
+        after, own, right, left
+    )
+
+
+def to_chip(value, by):
+    peers = lax.axis_size("tp")
+    return lax.ppermute(value, "tp", [(i, (i + 2 * by) % peers) for i in range(peers)])
+
+
+def sum_round(parts, after):
+    mine_far, other_far, mine_near, other_near = parts
+    other_far = to_partner(other_far)
+    other_near = to_partner(other_near)
+    low, high = halves(mine_far, other_far)
+    low, high = to_chip(low, 1), to_chip(high, -1)
+    own, right, left = onward(mine_near, other_near, low, high)
+    return add_last(after, own, to_chip(right, 1), to_chip(left, -1))
 
 
 def to_partner(value):
@@ -608,9 +676,8 @@
     own_after, spread = after_mix(at, exchange(sum_pairs(both)), residual)
     mine = exchange(spread)
     other = to_partner(mine)
-    gain = channel_gain.reshape(2 * owners, 1, -1)
-    both = channel_mixer(core, mine, other, gain, weights)
-    return add_down(exchange(sum_pairs(both)), own_after)
+    normal = normalised(at, mine, other, channel_gain.reshape(1, -1))
+    return sum_round(channel_mixer(at, normal, weights, own_after.shape[1]), own_after)
 
 
 def solution(mesh):

time: 181 us -> 180 us (level)
  blocking collectives: 53.6 us -> 35.5 us
  starting transfers between devices: 40.3 us -> 45.8 us
  Pallas kernels: 35.9 us -> 41.2 us
  waiting for transfers between devices: 28.5 us -> 32.2 us
  local copies, waits for them, and re-layouts: 3.78 us -> 7.31 us
    all_to_all x3 -> x2, blocking collectives: 53.6 us -> 35.5 us  [exchange(): return lax.all_to_all(value, 'tp', 0, 0, axis_index_groups=rows, tiled=True)]
    ppermute x0 -> x4, waiting for transfers between devices: none -> 8.79 us  [to_chip(): lax.ppermute(value, 'tp', [(i, (i + 2 * by) % peers) for i in range(peers)])]
    pallas_call x2 -> x5, Pallas kernels: 14.5 us -> 19.9 us  [the longest x1 9.79 us: channel_mixer(): pl.pallas_call(functools.partial(mixer_kernel, tiles), in_specs=[smem(),...]
    ppermute x0 -> x4, starting transfers between devices: none -> 5.35 us  [to_chip(): lax.ppermute(value, 'tp', [(i, (i + 2 * by) % peers) for i in range(peers)])]
    all_gather x1, waiting for transfers between devices: 18.7 us -> 13.7 us  [on_device(): weights = lax.all_gather(late, 'sp', axis=0)]
    unnamed x16 -> x28, local copies, waits for them, and re-layouts: 1.92 us -> 5.45 us
    ppermute x3 -> x4, starting transfers between devices: 22.8 us -> 22.9 us  [to_partner(): lax.ppermute(value, 'tp', [(i, i ^ 1) for i in range(lax.axis_size('tp'))])]
    ppermute x3 -> x4, waiting for transfers between devices: 6.67 us -> 6.53 us  [to_partner(): lax.ppermute(value, 'tp', [(i, i ^ 1) for i in range(lax.axis_size('tp'))])]
  transfers between devices with their start and end apart: 7 -> 12, of which waited for: 7 -> 9; matrix products, arithmetic and copies ran while one was open for 2% -> 2% of each run, Pallas kernels for 12% -> 15%
where the time goes in v5:
time: 180 us; the launch traced here: 179 us
  starting transfers between devices  45.8 us (25%)
  Pallas kernels  41.2 us (23%)
  blocking collectives  35.5 us (20%)
  waiting for transfers between devices  32.2 us (18%)
  between operations  13.5 us (8%)
  local copies, waits for them, and re-layouts  7.31 us (4%)
  other arithmetic  3.47 us (2%)
    all_to_all x2, blocking collectives, exchange(): return lax.all_to_all(value, 'tp', 0, 0, axis_index_groups=rows, tiled=True)  35.5 us
    ppermute x4, starting transfers between devices, to_partner(): lax.ppermute(value, 'tp', [(i, i ^ 1) for i in range(lax.axis_size('tp'))])  22.9 us
    ppermute x3, starting transfers between devices, from_behind(): return lax.ppermute(value, axis, pairs)  17.5 us
    all_gather x1, waiting for transfers between devices, on_device(): weights = lax.all_gather(late, 'sp', axis=0)  13.7 us
    pallas_call x1, Pallas kernels, channel_mixer(): pl.pallas_call(functools.partial(mixer_kernel, tiles), in_specs=[smem(),...  9.79 us
    ppermute x4, waiting for transfers between devices, to_chip(): lax.ppermute(value, 'tp', [(i, (i + 2 * by) % peers) for i in range(peers)])  8.79 us
    ppermute x4, waiting for transfers between devices, to_partner(): lax.ppermute(value, 'tp', [(i, i ^ 1) for i in range(lax.axis_size('tp'))])  6.53 us
    pallas_call x1, Pallas kernels, project(): pl.pallas_call(project_kernel, in_specs=[smem()] + [vmem()] * 8, out_shap...  6.48 us
  transfers between devices with their start and end apart: 12, of which 9 were waited for; matrix products, arithmetic and copies ran while one was open for 2% of the time, Pallas kernels for 15%

profile of v5, /device:TPU:33, one launch (start us, length us, event | category | flops | bytes accessed | tf_op | source)
XLA Modules:
  0.0 179.0 jit_solution(9880702945506072784)
XLA Ops:
  6.6 2.0 %pad_maximum_fusion = bf16[2112,128]{1,0:T(8,128)(2,1)} fusion(bf16[704,128]{1,0:T(8,128)(2,1)} %bitcast.8, bf16[704,128]{1,0:T(8,128)(2,1)} %bitcast.9, bf16[704,128]{1,0:T(8,128)(2,1)} %bitcast.10), kind=kLoop, calls=%fused_computation.1 | loop fusion | flops 1622016 | bytes 1081344 | tf_op jit(solution)/shard_map/concatenate | solution.py:661
  8.6 1.5 pack_edge.1
  10.1 5.2 %collective-permute-start = (bf16[16,896]{1,0:T(8,128)(2,1)}, bf16[16,896]{1,0:T(8,128)(2,1)S(1)}, u32[]{:S(2)}, u32[]{:S(2)}) collective-permute-start(bf16[16,896]{1,0:T(8,128)(2,1)} %pack_edge.1), channel_id=1, source_target_pairs={{0,8},{8,16},{16,24},{24,32},{32,40},{40,48},{48,56},{56,64},{64,7... | collective-permute-start | bytes 86024 | tf_op jit(solution)/shard_map/ppermute | solution.py:24
  15.4 0.7 copy.19.rate_ref
  16.0 0.5 collective-permute-done.before_ref
  16.5 0.6 copy-done.13
  17.1 5.0 %local_states.1 = (bf16[512,512]{1,0:T(8,128)(2,1)}, bf16[512,128]{1,0:T(8,128)(2,1)}, f32[8,512]{1,0:T(8,128)}, f32[8,512]{1,0:T(8,128)}, bf16[3,512,128]{2,1,0:T(8,128)(2,1)}, /*index=5*/bf16[528,128]{1,0:T(8,128)(2,1)}) custom-call(bf16[16,896]{1,0:T(8,128)(2,1)} %copy-done.13, bf16[512,512]{1,0:T(8,128)(2,1)} %values_ref.3, bf16[512,128]{1,0:T(8,128)(2,1)} %writes_ref.3, ...), custom_call_target="tpu_custom_call" | custom-call | flops 400000000 | bytes 4000000 | tf_op jit(solution)/shard_map/local_states/pallas_call | solution.py:211
  22.2 4.4 %collective-permute-start.1 = (bf16[528,128]{1,0:T(8,128)(2,1)}, bf16[528,128]{1,0:T(8,128)(2,1)S(1)}, u32[]{:S(2)}, u32[]{:S(2)}) collective-permute-start(bf16[528,128]{1,0:T(8,128)(2,1)} %get-tuple-element.27.own_ref), channel_id=1, source_target_pairs={{0,8},{8,16},{16,24},{24,32},{32,40},{40,48},{48,56},{56,64},{64,7... | collective-permute-start | bytes 405512 | tf_op jit(solution)/shard_map/ppermute | solution.py:24
  26.6 2.3 %collective-permute-done.1.near_ref = bf16[528,128]{1,0:T(8,128)(2,1)S(1)} collective-permute-done((bf16[528,128]{1,0:T(8,128)(2,1)}, bf16[528,128]{1,0:T(8,128)(2,1)S(1)}, u32[]{:S(2)}, u32[]{:S(2)}) %collective-permute-start.1) | collective-permute-done | bytes 135200 | tf_op jit(solution)/shard_map/ppermute | solution.py:24
  28.9 0.7 copy-done.3
  29.5 1.7 join_states.1
  31.2 7.9 %collective-permute-start.2 = (bf16[512,128]{1,0:T(8,128)(2,1)}, bf16[512,128]{1,0:T(8,128)(2,1)S(1)}, u32[]{:S(2)}, u32[]{:S(2)}) collective-permute-start(bf16[512,128]{1,0:T(8,128)(2,1)} %join_states.1), channel_id=1, source_target_pairs={{0,16},{8,24},{16,32},{24,40},{32,48},{40,56},{48,64},{56,72},{64,... | collective-permute-start | bytes 393224 | tf_op jit(solution)/shard_map/ppermute | solution.py:24
  39.1 0.6 reshape.22.gain_ref
  39.7 4.1 %local_mix.1 = (bf16[512,128]{1,0:T(8,128)(2,1)}, f32[512,512]{1,0:T(8,128)}, f32[8,512]{1,0:T(8,128)}) custom-call(bf16[16,896]{1,0:T(8,128)(2,1)} %copy-done.13, bf16[512,128]{1,0:T(8,128)(2,1)} %reads_ref.3, s32[4,128]{1,0:T(4,128)} %bitcast.13, bf16[4,128]{1,0:T(4,128)(2,1)} %taps_ref.1, bf16[512,512]{1,0:T(8,128)(2,1)} %get-tuple-element.28.sv_ref, ...), custom_call_target="tpu_custom_call" | custom-call | flops 800000000 | bytes 4000000 | tf_op jit(solution)/shard_map/local_mix/pallas_call | solution.py:331
  43.8 0.3 collective-permute-done.2.far_ref
  44.1 0.7 copy-done.9
  44.8 6.5 %project.1 = (bf16[4,512,256]{2,1,0:T(8,128)(2,1)}, bf16[4,512,256]{2,1,0:T(8,128)(2,1)}) custom-call(s32[1]{0:T(128)} %bitcast.1.core_ref, bf16[528,128]{1,0:T(8,128)(2,1)} %copy-done.3, bf16[512,128]{1,0:T(8,128)(2,1)} %copy-done.9, bf16[512,128]{1,0:T(8,128)(2,1)} %get-tuple-element.33.sr_ref, f32[512,512]{1,0:T(8,128)} %get-tuple-element.34.mixed_ref, ...), custom_call_target="tpu_custom_call" | custom-call | flops 1073741824 | bytes 6000000 | tf_op jit(solution)/shard_map/project/pallas_call | solution.py:405
  51.2 18.4 %collective-permute-start.3 = (bf16[4,512,256]{2,1,0:T(8,128)(2,1)}, bf16[4,512,256]{2,1,0:T(8,128)(2,1)S(1)}, u32[]{:S(2)}, u32[]{:S(2)}) collective-permute-start(bf16[4,512,256]{2,1,0:T(8,128)(2,1)} %get-tuple-element.37), channel_id=1, source_target_pairs={{0,1},{1,0},{2,3},{3,2},{4,5},{5,4},{6,7},{7,6},{8,9},{9,8},{10,11... | collective-permute-start | bytes 3145736 | tf_op jit(solution)/shard_map/ppermute | solution.py:623
  69.6 2.5 %collective-permute-done.3 = bf16[4,512,256]{2,1,0:T(8,128)(2,1)S(1)} collective-permute-done((bf16[4,512,256]{2,1,0:T(8,128)(2,1)}, bf16[4,512,256]{2,1,0:T(8,128)(2,1)S(1)}, u32[]{:S(2)}, u32[]{:S(2)}) %collective-permute-start.3) | collective-permute-done | bytes 1048608 | tf_op jit(solution)/shard_map/ppermute | solution.py:623
  72.1 1.5 add_convert_fusion
  73.6 18.0 %all_to_all.10.parts_ref = bf16[4,512,256]{2,1,0:T(8,128)(2,1)} all-to-all(bf16[4,512,256]{2,1,0:T(8,128)(2,1)S(1)} %add_convert_fusion), channel_id=1, replica_groups={{0,2,4,6},{1,3,5,7},{8,10,12,14},{9,11,13,15},{16,18,20,22},{17,19,21,2..., dimensions={0} | all-to-all | bytes 2097152 | tf_op jit(solution)/shard_map/all_to_all | solution.py:629
  91.7 2.5 %after_mix.1 = (bf16[512,256]{1,0:T(8,128)(2,1)}, bf16[4,512,256]{2,1,0:T(8,128)(2,1)}) custom-call(s32[1]{0:T(128)} %bitcast.at_ref, bf16[4,512,256]{2,1,0:T(8,128)(2,1)} %all_to_all.10.parts_ref, bf16[512,2048]{1,0:T(8,128)(2,1)} %residual_ref.1), custom_call_target="tpu_custom_call" | custom-call | tf_op jit(solution)/shard_map/after_mix/pallas_call | solution.py:429
  94.2 17.5 %all_to_all.11.mine_ref = bf16[4,512,256]{2,1,0:T(8,128)(2,1)S(1)} all-to-all(bf16[4,512,256]{2,1,0:T(8,128)(2,1)} %get-tuple-element.39), channel_id=1, replica_groups={{0,2,4,6},{1,3,5,7},{8,10,12,14},{9,11,13,15},{16,18,20,22},{17,19,21,2..., dimensions={0} | all-to-all | bytes 2097152 | tf_op jit(solution)/shard_map/all_to_all | solution.py:629
  111.6 2.1 %collective-permute-start.4 = (bf16[4,512,256]{2,1,0:T(8,128)(2,1)S(1)}, bf16[4,512,256]{2,1,0:T(8,128)(2,1)S(1)}, u32[]{:S(2)}, u32[]{:S(2)}) collective-permute-start(bf16[4,512,256]{2,1,0:T(8,128)(2,1)S(1)} %all_to_all.11.mine_ref), channel_id=1, source_target_pairs={{0,1},{1,0},{2,3},{3,2},{4,5},{5,4},{6,7},{7,6},{8,9},{9,8},{10,11... | collective-permute-start | bytes 3145736 | tf_op jit(solution)/shard_map/ppermute | solution.py:623
  113.7 0.6 reshape.23.gain_ref
  114.3 1.7 collective-permute-done.4.other_ref
  116.0 1.0 copy-done.1
  117.1 4.0 %normalised.1.normal_ref = bf16[512,2048]{1,0:T(8,128)(2,1)} custom-call(s32[1]{0:T(128)} %bitcast.at_ref, bf16[4,512,256]{2,1,0:T(8,128)(2,1)} %copy-done, bf16[4,512,256]{2,1,0:T(8,128)(2,1)} %copy-done.1, bf16[1,2048]{1,0:T(2,128)(2,1)} %reshape.23.gain_ref), custom_call_target="tpu_custom_call" | custom-call | tf_op jit(solution)/shard_map/normalised/pallas_call | solution.py:468
  121.0 13.7 %all-gather.3.cloned.1.call-done = bf16[33792,128]{1,0:T(8,128)(2,1)} async-done(((bf16[2112,128]{1,0:T(8,128)(2,1)}), bf16[33792,128]{1,0:T(8,128)(2,1)}) %all-gather.3.cloned.1.call-update) | async-done | bytes 8650768 | tf_op jit(solution)/shard_map/all_gather | solution.py:662
  134.8 9.8 %channel_mixer.1 = (bf16[512,256]{1,0:T(8,128)(2,1)}, bf16[512,256]{1,0:T(8,128)(2,1)}, bf16[3,512,256]{2,1,0:T(8,128)(2,1)}, bf16[3,512,256]{2,1,0:T(8,128)(2,1)}) custom-call(s32[1]{0:T(128)} %bitcast.at_ref, bf16[512,2048]{1,0:T(8,128)(2,1)} %normalised.1.normal_ref, bf16[16,2112,128]{2,1,0:T(8,128)(2,1)} %bitcast.15), custom_call_target="tpu_custom_call" | custom-call | flops 4429185024 | bytes 14000000 | tf_op jit(solution)/shard_map/channel_mixer/pallas_call | solution.py:545
  144.6 2.3 %collective-permute-start.5 = (bf16[3,512,256]{2,1,0:T(8,128)(2,1)}, bf16[3,512,256]{2,1,0:T(8,128)(2,1)S(1)}, u32[]{:S(2)}, u32[]{:S(2)}) collective-permute-start(bf16[3,512,256]{2,1,0:T(8,128)(2,1)} %get-tuple-element.41), channel_id=1, source_target_pairs={{0,1},{1,0},{2,3},{3,2},{4,5},{5,4},{6,7},{7,6},{8,9},{9,8},{10,11... | collective-permute-start | bytes 2359304 | tf_op jit(solution)/shard_map/ppermute | solution.py:623
  146.8 0.1 collective-permute-start.6
  147.0 2.3 %collective-permute-done.6.other_ref = bf16[512,256]{1,0:T(8,128)(2,1)S(1)} collective-permute-done((bf16[512,256]{1,0:T(8,128)(2,1)}, bf16[512,256]{1,0:T(8,128)(2,1)S(1)}, u32[]{:S(2)}, u32[]{:S(2)}) %collective-permute-start.6) | collective-permute-done | bytes 262176 | tf_op jit(solution)/shard_map/ppermute | solution.py:623
  149.3 0.7 copy-done.6
  150.0 1.8 halves.1
  151.8 1.3 collective-permute-start.7
  153.1 1.4 collective-permute-start.8
  154.5 3.4 %collective-permute-done.7.low_ref = bf16[256,256]{1,0:T(8,128)(2,1)S(1)} collective-permute-done((bf16[256,256]{1,0:T(8,128)(2,1)}, bf16[256,256]{1,0:T(8,128)(2,1)S(1)}, u32[]{:S(2)}, u32[]{:S(2)}) %collective-permute-start.7) | collective-permute-done | bytes 131104 | tf_op jit(solution)/shard_map/ppermute | solution.py:609
  157.9 0.6 copy-done.7
  158.6 0.1 copy-done.8
  158.6 0.3 copy-done.2
  158.9 2.4 %onward.1 = (bf16[512,256]{1,0:T(8,128)(2,1)}, bf16[512,256]{1,0:T(8,128)(2,1)}, bf16[512,256]{1,0:T(8,128)(2,1)}) custom-call(bf16[3,512,256]{2,1,0:T(8,128)(2,1)} %get-tuple-element.40.mine_ref, bf16[3,512,256]{2,1,0:T(8,128)(2,1)} %copy-done.2, bf16[256,256]{1,0:T(8,128)(2,1)} %copy-done.7, bf16[256,256]{1,0:T(8,128)(2,1)} %copy-done.8), custom_call_target="tpu_custom_call" | custom-call | tf_op jit(solution)/shard_map/onward/pallas_call | solution.py:593
  161.3 0.8 collective-permute-start.9
  162.1 1.8 %collective-permute-start.10 = (bf16[512,256]{1,0:T(8,128)(2,1)}, bf16[512,256]{1,0:T(8,128)(2,1)S(1)}, u32[]{:S(2)}, u32[]{:S(2)}) collective-permute-start(bf16[512,256]{1,0:T(8,128)(2,1)} %get-tuple-element.48), channel_id=1, source_target_pairs={{0,6},{1,7},{2,0},{3,1},{4,2},{5,3},{6,4},{7,5},{8,14},{9,15},{10,... | collective-permute-start | bytes 786440 | tf_op jit(solution)/shard_map/ppermute | solution.py:609
  164.0 5.4 %collective-permute-done.9.right_ref = bf16[512,256]{1,0:T(8,128)(2,1)S(1)} collective-permute-done((bf16[512,256]{1,0:T(8,128)(2,1)}, bf16[512,256]{1,0:T(8,128)(2,1)S(1)}, u32[]{:S(2)}, u32[]{:S(2)}) %collective-permute-start.9) | collective-permute-done | bytes 262176 | tf_op jit(solution)/shard_map/ppermute | solution.py:609
  169.3 0.7 copy-done.4
  170.0 0.1 copy-done.5
  170.1 2.0 %add_last.1 = bf16[512,256]{1,0:T(8,128)(2,1)} custom-call(bf16[512,256]{1,0:T(8,128)(2,1)} %get-tuple-element.38.after_ref, bf16[512,256]{1,0:T(8,128)(2,1)} %get-tuple-element.46.own_ref, bf16[512,256]{1,0:T(8,128)(2,1)} %copy-done.4, bf16[512,256]{1,0:T(8,128)(2,1)} %copy-done.5), custom_call_target="tpu_custom_call" | custom-call | tf_op jit(solution)/shard_map/add_last/pallas_call | solution.py:602
  (23 shorter events, 0.1 us)
Async XLA Ops:
  6.5 8.8 %copy-start.12 = (f32[8]{0:T(128)S(1)}, f32[8]{0:T(128)}, u32[]{:S(2)}) copy-start(f32[8]{0:T(128)} %param.24) | copy-start | bytes 100
  6.5 128.2 %all-gather.3.cloned.1.call-start = ((), (), s32[]{:S(2)}) async-start(), calls=%async_computation.2 | async-start | bytes 9191424 | tf_op jit(solution)/shard_map/all_gather | solution.py:662
  6.6 32.5 %copy-start.11 = (bf16[512]{0:T(512)(128)(2,1)S(1)}, bf16[512]{0:T(512)(128)(2,1)}, u32[]{:S(2)}) copy-start(bf16[512]{0:T(512)(128)(2,1)} %param.30) | copy-start | bytes 3076
  10.1 6.4 %collective-permute-start = (bf16[16,896]{1,0:T(8,128)(2,1)}, bf16[16,896]{1,0:T(8,128)(2,1)S(1)}, u32[]{:S(2)}, u32[]{:S(2)}) collective-permute-start(bf16[16,896]{1,0:T(8,128)(2,1)} %pack_edge.1), channel_id=1, source_target_pairs={{0,8},{8,16},{16,24},{24,32},{32,40},{40,48},{48,56},{56,64},{64,7... | collective-permute-start | bytes 86024 | tf_op jit(solution)/shard_map/ppermute | solution.py:24
  16.5 0.6 copy-start.13
  22.2 6.7 %collective-permute-start.1 = (bf16[528,128]{1,0:T(8,128)(2,1)}, bf16[528,128]{1,0:T(8,128)(2,1)S(1)}, u32[]{:S(2)}, u32[]{:S(2)}) collective-permute-start(bf16[528,128]{1,0:T(8,128)(2,1)} %get-tuple-element.27.own_ref), channel_id=1, source_target_pairs={{0,8},{8,16},{16,24},{24,32},{32,40},{40,48},{48,56},{56,64},{64,7... | collective-permute-start | bytes 405512 | tf_op jit(solution)/shard_map/ppermute | solution.py:24
  28.9 0.7 copy-start.3
  31.2 12.9 %collective-permute-start.2 = (bf16[512,128]{1,0:T(8,128)(2,1)}, bf16[512,128]{1,0:T(8,128)(2,1)S(1)}, u32[]{:S(2)}, u32[]{:S(2)}) collective-permute-start(bf16[512,128]{1,0:T(8,128)(2,1)} %join_states.1), channel_id=1, source_target_pairs={{0,16},{8,24},{16,32},{24,40},{32,48},{40,56},{48,64},{56,72},{64,... | collective-permute-start | bytes 393224 | tf_op jit(solution)/shard_map/ppermute | solution.py:24
  44.1 0.7 copy-start.9
  51.2 20.9 %collective-permute-start.3 = (bf16[4,512,256]{2,1,0:T(8,128)(2,1)}, bf16[4,512,256]{2,1,0:T(8,128)(2,1)S(1)}, u32[]{:S(2)}, u32[]{:S(2)}) collective-permute-start(bf16[4,512,256]{2,1,0:T(8,128)(2,1)} %get-tuple-element.37), channel_id=1, source_target_pairs={{0,1},{1,0},{2,3},{3,2},{4,5},{5,4},{6,7},{7,6},{8,9},{9,8},{10,11... | collective-permute-start | bytes 3145736 | tf_op jit(solution)/shard_map/ppermute | solution.py:623
  91.7 22.1 %copy-start.10 = (bf16[2048]{0:T(1024)(128)(2,1)S(1)}, bf16[2048]{0:T(1024)(128)(2,1)}, u32[]{:S(2)}) copy-start(bf16[2048]{0:T(1024)(128)(2,1)} %param.32) | copy-start | bytes 12292
  111.6 4.4 %copy-start = (bf16[4,512,256]{2,1,0:T(8,128)(2,1)}, bf16[4,512,256]{2,1,0:T(8,128)(2,1)S(1)}, u32[]{:S(2)}) copy-start(bf16[4,512,256]{2,1,0:T(8,128)(2,1)S(1)} %all_to_all.11.mine_ref) | copy-start | bytes 3145732
  111.6 4.4 %collective-permute-start.4 = (bf16[4,512,256]{2,1,0:T(8,128)(2,1)S(1)}, bf16[4,512,256]{2,1,0:T(8,128)(2,1)S(1)}, u32[]{:S(2)}, u32[]{:S(2)}) collective-permute-start(bf16[4,512,256]{2,1,0:T(8,128)(2,1)S(1)} %all_to_all.11.mine_ref), channel_id=1, source_target_pairs={{0,1},{1,0},{2,3},{3,2},{4,5},{5,4},{6,7},{7,6},{8,9},{9,8},{10,11... | collective-permute-start | bytes 3145736 | tf_op jit(solution)/shard_map/ppermute | solution.py:623
  116.0 1.0 copy-start.1
  144.6 13.4 %collective-permute-start.5 = (bf16[3,512,256]{2,1,0:T(8,128)(2,1)}, bf16[3,512,256]{2,1,0:T(8,128)(2,1)S(1)}, u32[]{:S(2)}, u32[]{:S(2)}) collective-permute-start(bf16[3,512,256]{2,1,0:T(8,128)(2,1)} %get-tuple-element.41), channel_id=1, source_target_pairs={{0,1},{1,0},{2,3},{3,2},{4,5},{5,4},{6,7},{7,6},{8,9},{9,8},{10,11... | collective-permute-start | bytes 2359304 | tf_op jit(solution)/shard_map/ppermute | solution.py:623
  146.8 2.5 %collective-permute-start.6 = (bf16[512,256]{1,0:T(8,128)(2,1)}, bf16[512,256]{1,0:T(8,128)(2,1)S(1)}, u32[]{:S(2)}, u32[]{:S(2)}) collective-permute-start(bf16[512,256]{1,0:T(8,128)(2,1)} %get-tuple-element.43), channel_id=1, source_target_pairs={{0,1},{1,0},{2,3},{3,2},{4,5},{5,4},{6,7},{7,6},{8,9},{9,8},{10,11... | collective-permute-start | bytes 786440 | tf_op jit(solution)/shard_map/ppermute | solution.py:623
  149.3 0.7 copy-start.6
  151.8 6.1 %collective-permute-start.7 = (bf16[256,256]{1,0:T(8,128)(2,1)}, bf16[256,256]{1,0:T(8,128)(2,1)S(1)}, u32[]{:S(2)}, u32[]{:S(2)}) collective-permute-start(bf16[256,256]{1,0:T(8,128)(2,1)} %get-tuple-element.44), channel_id=1, source_target_pairs={{0,2},{1,3},{2,4},{3,5},{4,6},{5,7},{6,0},{7,1},{8,10},{9,11},{10,... | collective-permute-start | bytes 393224 | tf_op jit(solution)/shard_map/ppermute | solution.py:609
  153.1 4.8 %collective-permute-start.8 = (bf16[256,256]{1,0:T(8,128)(2,1)}, bf16[256,256]{1,0:T(8,128)(2,1)S(1)}, u32[]{:S(2)}, u32[]{:S(2)}) collective-permute-start(bf16[256,256]{1,0:T(8,128)(2,1)} %get-tuple-element.45), channel_id=1, source_target_pairs={{0,6},{1,7},{2,0},{3,1},{4,2},{5,3},{6,4},{7,5},{8,14},{9,15},{10,... | collective-permute-start | bytes 393224 | tf_op jit(solution)/shard_map/ppermute | solution.py:609
  157.9 0.6 copy-start.7
  157.9 0.7 copy-start.8
  157.9 1.0 copy-start.2
  161.3 8.0 %collective-permute-start.9 = (bf16[512,256]{1,0:T(8,128)(2,1)}, bf16[512,256]{1,0:T(8,128)(2,1)S(1)}, u32[]{:S(2)}, u32[]{:S(2)}) collective-permute-start(bf16[512,256]{1,0:T(8,128)(2,1)} %get-tuple-element.47), channel_id=1, source_target_pairs={{0,2},{1,3},{2,4},{3,5},{4,6},{5,7},{6,0},{7,1},{8,10},{9,11},{10,... | collective-permute-start | bytes 786440 | tf_op jit(solution)/shard_map/ppermute | solution.py:609
  162.1 7.2 %collective-permute-start.10 = (bf16[512,256]{1,0:T(8,128)(2,1)}, bf16[512,256]{1,0:T(8,128)(2,1)S(1)}, u32[]{:S(2)}, u32[]{:S(2)}) collective-permute-start(bf16[512,256]{1,0:T(8,128)(2,1)} %get-tuple-element.48), channel_id=1, source_target_pairs={{0,6},{1,7},{2,0},{3,1},{4,2},{5,3},{6,4},{7,5},{8,14},{9,15},{10,... | collective-permute-start | bytes 786440 | tf_op jit(solution)/shard_map/ppermute | solution.py:609
  169.3 0.7 copy-start.4
  169.3 0.8 copy-start.5
Sparse Core Ops, SparseCore 0:
  9.1 125.5 all-gather.2

commit v6 on v5

--- a/solution.py
+++ b/solution.py
@@ -565,43 +565,8 @@
     )(at, normal, weights)
 
 
-def halves_kernel(mine_ref, other_ref, low_ref, high_ref):
-    half = low_ref.shape[0]
-    low_ref[...] = (mine_ref[:half].astype(F32) + other_ref[:half].astype(F32)).astype(BF16)
-    high_ref[...] = (mine_ref[half:].astype(F32) + other_ref[half:].astype(F32)).astype(BF16)
-
-
-def halves(mine, other):
-    part = shape((mine.shape[0] // 2, mine.shape[1]), BF16)
-    return pl.pallas_call(halves_kernel, out_shape=(part, part), name="halves")(mine, other)
-
-
-def onward_kernel(mine_ref, other_ref, low_ref, high_ref, own_ref, right_ref, left_ref):
-    half = low_ref.shape[0]
-    for k, ref in enumerate((own_ref, right_ref, left_ref)):
-        for rows in (slice(0, half), slice(half, 2 * half)):
-            total = mine_ref[k, rows].astype(F32) + other_ref[k, rows].astype(F32)
-            if k == 1 and rows.start == 0:
-                total = total + low_ref[...].astype(F32)
-            if k == 2 and rows.start > 0:
-                total = total + high_ref[...].astype(F32)
-            ref[rows] = total.astype(BF16)
-
-
-def onward(mine, other, low, high):
-    part = shape(mine.shape[1:], BF16)
-    return pl.pallas_call(onward_kernel, out_shape=(part,) * 3, name="onward")(mine, other, low, high)
-
-
-def last_kernel(after_ref, own_ref, right_ref, left_ref, out_ref):
-    down = own_ref[...].astype(F32) + right_ref[...].astype(F32) + left_ref[...].astype(F32)
-    out_ref[...] = (after_ref[...].astype(F32) + down).astype(BF16)
-
-
-def add_last(after, own, right, left):
-    return pl.pallas_call(last_kernel, out_shape=shape(after.shape, BF16), name="add_last")(
-        after, own, right, left
-    )
+def to_partner(value):
+    return lax.ppermute(value, "tp", [(i, i ^ 1) for i in range(lax.axis_size("tp"))])
 
 
 def to_chip(value, by):
@@ -613,14 +578,17 @@
     mine_far, other_far, mine_near, other_near = parts
     other_far = to_partner(other_far)
     other_near = to_partner(other_near)
-    low, high = halves(mine_far, other_far)
-    low, high = to_chip(low, 1), to_chip(high, -1)
-    own, right, left = onward(mine_near, other_near, low, high)
-    return add_last(after, own, to_chip(right, 1), to_chip(left, -1))
-
-
-def to_partner(value):
-    return lax.ppermute(value, "tp", [(i, i ^ 1) for i in range(lax.axis_size("tp"))])
+    half = mine_far.shape[0] // 2
+    far = mine_far.astype(F32) + other_far.astype(F32)
+    low = to_chip(far[:half].astype(BF16), 1)
+    high = to_chip(far[half:].astype(BF16), -1)
+    near = mine_near.astype(F32) + other_near.astype(F32)
+    low = jnp.pad(low, ((0, half), (0, 0))).astype(F32)
+    high = jnp.pad(high, ((half, 0), (0, 0))).astype(F32)
+    right = to_chip((near[1] + low).astype(BF16), 1)
+    left = to_chip((near[2] + high).astype(BF16), -1)
+    down = near[0] + right.astype(F32) + left.astype(F32)
+    return (after.astype(F32) + down).astype(BF16)
 
 
 def exchange(value):

time: 180 us -> 175 us (0.972)
  Pallas kernels: 41.2 us -> 35.1 us
  local copies, waits for them, and re-layouts: 7.31 us -> 4.83 us
  other arithmetic: 3.47 us -> 5.57 us
    pallas_call x3 -> x0, Pallas kernels: 6.17 us -> none  [the longest x1 2.36 us: onward(): pl.pallas_call(onward_kernel, out_shape=(part,) * 3, name='onward')]
    unnamed x28 -> x20, local copies, waits for them, and re-layouts: 5.45 us -> 2.95 us
  transfers between devices with their start and end apart: 12 -> 12, of which waited for: 9 -> 10; matrix products, arithmetic and copies ran while one was open for 2% -> 3% of each run, Pallas kernels for 15% -> 15%
where the time goes in v6:
time: 175 us; the launch traced here: 174 us
  starting transfers between devices  45.7 us (26%)
  blocking collectives  35.6 us (20%)
  Pallas kernels  35.1 us (20%)
  waiting for transfers between devices  33.6 us (19%)
  between operations  13.5 us (8%)
  other arithmetic  5.57 us (3%)
  local copies, waits for them, and re-layouts  4.83 us (3%)
    all_to_all x2, blocking collectives, exchange(): return lax.all_to_all(value, 'tp', 0, 0, axis_index_groups=rows, tiled=True)  35.6 us
    ppermute x4, starting transfers between devices, to_partner(): lax.ppermute(value, 'tp', [(i, i ^ 1) for i in range(lax.axis_size('tp'))])  22.9 us
    ppermute x3, starting transfers between devices, from_behind(): return lax.ppermute(value, axis, pairs)  17.5 us
    all_gather x1, waiting for transfers between devices, on_device(): weights = lax.all_gather(late, 'sp', axis=0)  13.7 us
    ppermute x4, waiting for transfers between devices, to_chip(): lax.ppermute(value, 'tp', [(i, (i + 2 * by) % peers) for i in range(peers)])  10.3 us
    pallas_call x1, Pallas kernels, channel_mixer(): pl.pallas_call(functools.partial(mixer_kernel, tiles), in_specs=[smem(),...  9.83 us
    ppermute x4, waiting for transfers between devices, to_partner(): lax.ppermute(value, 'tp', [(i, i ^ 1) for i in range(lax.axis_size('tp'))])  6.53 us
    pallas_call x1, Pallas kernels, project(): pl.pallas_call(project_kernel, in_specs=[smem()] + [vmem()] * 8, out_shap...  6.47 us
  transfers between devices with their start and end apart: 12, of which 10 were waited for; matrix products, arithmetic and copies ran while one was open for 3% of the time, Pallas kernels for 15%

profile of v6, /device:TPU:33, one launch (start us, length us, event | category | flops | bytes accessed | tf_op | source)
XLA Modules:
  0.0 174.0 jit_solution(5798095636297070359)
XLA Ops:
  6.6 1.9 %pad_maximum_fusion = bf16[2112,128]{1,0:T(8,128)(2,1)} fusion(bf16[704,128]{1,0:T(8,128)(2,1)} %bitcast.30, bf16[704,128]{1,0:T(8,128)(2,1)} %bitcast.31, bf16[704,128]{1,0:T(8,128)(2,1)} %bitcast.32), kind=kLoop, calls=%fused_computation.2 | loop fusion | flops 1622016 | bytes 1081344 | tf_op jit(solution)/shard_map/concatenate | solution.py:629
  8.5 0.1 all-gather.3.cloned.1.call-update
  8.6 1.5 pack_edge.1
  10.1 5.2 %collective-permute-start = (bf16[16,896]{1,0:T(8,128)(2,1)}, bf16[16,896]{1,0:T(8,128)(2,1)S(1)}, u32[]{:S(2)}, u32[]{:S(2)}) collective-permute-start(bf16[16,896]{1,0:T(8,128)(2,1)} %pack_edge.1), channel_id=1, source_target_pairs={{0,8},{8,16},{16,24},{24,32},{32,40},{40,48},{48,56},{56,64},{64,7... | collective-permute-start | bytes 86024 | tf_op jit(solution)/shard_map/ppermute | solution.py:24
  15.3 0.7 copy.19.rate_ref
  16.0 0.5 collective-permute-done.before_ref
  16.5 0.6 copy-done.9
  17.1 5.0 %local_states.1 = (bf16[512,512]{1,0:T(8,128)(2,1)}, bf16[512,128]{1,0:T(8,128)(2,1)}, f32[8,512]{1,0:T(8,128)}, f32[8,512]{1,0:T(8,128)}, bf16[3,512,128]{2,1,0:T(8,128)(2,1)}, /*index=5*/bf16[528,128]{1,0:T(8,128)(2,1)}) custom-call(bf16[16,896]{1,0:T(8,128)(2,1)} %copy-done.9, bf16[512,512]{1,0:T(8,128)(2,1)} %values_ref.3, bf16[512,128]{1,0:T(8,128)(2,1)} %writes_ref.3, ...), custom_call_target="tpu_custom_call" | custom-call | flops 400000000 | bytes 4000000 | tf_op jit(solution)/shard_map/local_states/pallas_call | solution.py:211
  22.1 4.4 %collective-permute-start.1 = (bf16[528,128]{1,0:T(8,128)(2,1)}, bf16[528,128]{1,0:T(8,128)(2,1)S(1)}, u32[]{:S(2)}, u32[]{:S(2)}) collective-permute-start(bf16[528,128]{1,0:T(8,128)(2,1)} %get-tuple-element.22.own_ref), channel_id=1, source_target_pairs={{0,8},{8,16},{16,24},{24,32},{32,40},{40,48},{48,56},{56,64},{64,7... | collective-permute-start | bytes 405512 | tf_op jit(solution)/shard_map/ppermute | solution.py:24
  26.6 2.3 %collective-permute-done.1.near_ref = bf16[528,128]{1,0:T(8,128)(2,1)S(1)} collective-permute-done((bf16[528,128]{1,0:T(8,128)(2,1)}, bf16[528,128]{1,0:T(8,128)(2,1)S(1)}, u32[]{:S(2)}, u32[]{:S(2)}) %collective-permute-start.1) | collective-permute-done | bytes 135200 | tf_op jit(solution)/shard_map/ppermute | solution.py:24
  28.9 0.6 copy-done.3
  29.5 1.7 join_states.1
  31.2 7.8 %collective-permute-start.2 = (bf16[512,128]{1,0:T(8,128)(2,1)}, bf16[512,128]{1,0:T(8,128)(2,1)S(1)}, u32[]{:S(2)}, u32[]{:S(2)}) collective-permute-start(bf16[512,128]{1,0:T(8,128)(2,1)} %join_states.1), channel_id=1, source_target_pairs={{0,16},{8,24},{16,32},{24,40},{32,48},{40,56},{48,64},{56,72},{64,... | collective-permute-start | bytes 393224 | tf_op jit(solution)/shard_map/ppermute | solution.py:24
  39.0 0.6 reshape.22.gain_ref
  39.6 4.1 %local_mix.1 = (bf16[512,128]{1,0:T(8,128)(2,1)}, f32[512,512]{1,0:T(8,128)}, f32[8,512]{1,0:T(8,128)}) custom-call(bf16[16,896]{1,0:T(8,128)(2,1)} %copy-done.9, bf16[512,128]{1,0:T(8,128)(2,1)} %reads_ref.3, s32[4,128]{1,0:T(4,128)} %bitcast.35, bf16[4,128]{1,0:T(4,128)(2,1)} %taps_ref.1, bf16[512,512]{1,0:T(8,128)(2,1)} %get-tuple-element.23.sv_ref, ...), custom_call_target="tpu_custom_call" | custom-call | flops 800000000 | bytes 4000000 | tf_op jit(solution)/shard_map/local_mix/pallas_call | solution.py:331
  43.7 0.3 collective-permute-done.2.far_ref
  44.0 0.7 copy-done.5
  44.7 6.5 %project.1 = (bf16[4,512,256]{2,1,0:T(8,128)(2,1)}, bf16[4,512,256]{2,1,0:T(8,128)(2,1)}) custom-call(s32[1]{0:T(128)} %bitcast.1.core_ref, bf16[528,128]{1,0:T(8,128)(2,1)} %copy-done.3, bf16[512,128]{1,0:T(8,128)(2,1)} %copy-done.5, bf16[512,128]{1,0:T(8,128)(2,1)} %get-tuple-element.28.sr_ref, f32[512,512]{1,0:T(8,128)} %get-tuple-element.29.mixed_ref, ...), custom_call_target="tpu_custom_call" | custom-call | flops 1073741824 | bytes 6000000 | tf_op jit(solution)/shard_map/project/pallas_call | solution.py:405
  51.2 18.4 %collective-permute-start.3 = (bf16[4,512,256]{2,1,0:T(8,128)(2,1)}, bf16[4,512,256]{2,1,0:T(8,128)(2,1)S(1)}, u32[]{:S(2)}, u32[]{:S(2)}) collective-permute-start(bf16[4,512,256]{2,1,0:T(8,128)(2,1)} %get-tuple-element.32), channel_id=1, source_target_pairs={{0,1},{1,0},{2,3},{3,2},{4,5},{5,4},{6,7},{7,6},{8,9},{9,8},{10,11... | collective-permute-start | bytes 3145736 | tf_op jit(solution)/shard_map/ppermute | solution.py:569
  69.6 2.5 %collective-permute-done.3 = bf16[4,512,256]{2,1,0:T(8,128)(2,1)S(1)} collective-permute-done((bf16[4,512,256]{2,1,0:T(8,128)(2,1)}, bf16[4,512,256]{2,1,0:T(8,128)(2,1)S(1)}, u32[]{:S(2)}, u32[]{:S(2)}) %collective-permute-start.3) | collective-permute-done | bytes 1048608 | tf_op jit(solution)/shard_map/ppermute | solution.py:569
  72.1 1.5 add_convert_fusion
  73.6 18.0 %all_to_all.10.parts_ref = bf16[4,512,256]{2,1,0:T(8,128)(2,1)} all-to-all(bf16[4,512,256]{2,1,0:T(8,128)(2,1)S(1)} %add_convert_fusion), channel_id=1, replica_groups={{0,2,4,6},{1,3,5,7},{8,10,12,14},{9,11,13,15},{16,18,20,22},{17,19,21,2..., dimensions={0} | all-to-all | bytes 2097152 | tf_op jit(solution)/shard_map/all_to_all | solution.py:597
  91.6 2.5 %after_mix.1 = (bf16[512,256]{1,0:T(8,128)(2,1)}, bf16[4,512,256]{2,1,0:T(8,128)(2,1)}) custom-call(s32[1]{0:T(128)} %bitcast.at_ref, bf16[4,512,256]{2,1,0:T(8,128)(2,1)} %all_to_all.10.parts_ref, bf16[512,2048]{1,0:T(8,128)(2,1)} %residual_ref.1), custom_call_target="tpu_custom_call" | custom-call | tf_op jit(solution)/shard_map/after_mix/pallas_call | solution.py:429
  94.1 17.6 %all_to_all.11.mine_ref = bf16[4,512,256]{2,1,0:T(8,128)(2,1)S(1)} all-to-all(bf16[4,512,256]{2,1,0:T(8,128)(2,1)} %get-tuple-element.34), channel_id=1, replica_groups={{0,2,4,6},{1,3,5,7},{8,10,12,14},{9,11,13,15},{16,18,20,22},{17,19,21,2..., dimensions={0} | all-to-all | bytes 2097152 | tf_op jit(solution)/shard_map/all_to_all | solution.py:597
  111.7 2.1 %collective-permute-start.4 = (bf16[4,512,256]{2,1,0:T(8,128)(2,1)S(1)}, bf16[4,512,256]{2,1,0:T(8,128)(2,1)S(1)}, u32[]{:S(2)}, u32[]{:S(2)}) collective-permute-start(bf16[4,512,256]{2,1,0:T(8,128)(2,1)S(1)} %all_to_all.11.mine_ref), channel_id=1, source_target_pairs={{0,1},{1,0},{2,3},{3,2},{4,5},{5,4},{6,7},{7,6},{8,9},{9,8},{10,11... | collective-permute-start | bytes 3145736 | tf_op jit(solution)/shard_map/ppermute | solution.py:569
  113.8 0.6 reshape.23.gain_ref
  114.4 1.7 collective-permute-done.4.other_ref
  116.1 1.0 copy-done.1
  117.1 4.0 %normalised.1.normal_ref = bf16[512,2048]{1,0:T(8,128)(2,1)} custom-call(s32[1]{0:T(128)} %bitcast.at_ref, bf16[4,512,256]{2,1,0:T(8,128)(2,1)} %copy-done, bf16[4,512,256]{2,1,0:T(8,128)(2,1)} %copy-done.1, bf16[1,2048]{1,0:T(2,128)(2,1)} %reshape.23.gain_ref), custom_call_target="tpu_custom_call" | custom-call | tf_op jit(solution)/shard_map/normalised/pallas_call | solution.py:468
  121.1 13.7 %all-gather.3.cloned.1.call-done = bf16[33792,128]{1,0:T(8,128)(2,1)} async-done(((bf16[2112,128]{1,0:T(8,128)(2,1)}), bf16[33792,128]{1,0:T(8,128)(2,1)}) %all-gather.3.cloned.1.call-update) | async-done | bytes 8650768 | tf_op jit(solution)/shard_map/all_gather | solution.py:630
  134.8 9.8 %channel_mixer.1 = (bf16[512,256]{1,0:T(8,128)(2,1)}, bf16[512,256]{1,0:T(8,128)(2,1)}, bf16[3,512,256]{2,1,0:T(8,128)(2,1)}, bf16[3,512,256]{2,1,0:T(8,128)(2,1)}) custom-call(s32[1]{0:T(128)} %bitcast.at_ref, bf16[512,2048]{1,0:T(8,128)(2,1)} %normalised.1.normal_ref, bf16[16,2112,128]{2,1,0:T(8,128)(2,1)} %bitcast.37), custom_call_target="tpu_custom_call" | custom-call | flops 4429185024 | bytes 14000000 | tf_op jit(solution)/shard_map/channel_mixer/pallas_call | solution.py:545
  144.6 2.3 %collective-permute-start.5 = (bf16[3,512,256]{2,1,0:T(8,128)(2,1)}, bf16[3,512,256]{2,1,0:T(8,128)(2,1)S(1)}, u32[]{:S(2)}, u32[]{:S(2)}) collective-permute-start(bf16[3,512,256]{2,1,0:T(8,128)(2,1)} %get-tuple-element.36), channel_id=1, source_target_pairs={{0,1},{1,0},{2,3},{3,2},{4,5},{5,4},{6,7},{7,6},{8,9},{9,8},{10,11... | collective-permute-start | bytes 2359304 | tf_op jit(solution)/shard_map/ppermute | solution.py:569
  146.9 0.1 collective-permute-start.6
  147.0 2.3 %collective-permute-done.6 = bf16[512,256]{1,0:T(8,128)(2,1)S(1)} collective-permute-done((bf16[512,256]{1,0:T(8,128)(2,1)}, bf16[512,256]{1,0:T(8,128)(2,1)S(1)}, u32[]{:S(2)}, u32[]{:S(2)}) %collective-permute-start.6) | collective-permute-done | bytes 262176 | tf_op jit(solution)/shard_map/ppermute | solution.py:569
  149.4 1.0 add_convert_fusion.1
  150.4 1.3 collective-permute-start.7
  151.7 1.5 collective-permute-start.9
  153.2 0.0 collective-permute-done.5
  153.2 0.2 convert_add_fusion
  153.4 0.0 copy-start.4
  153.4 3.0 %collective-permute-done.7 = bf16[256,256]{1,0:T(8,128)(2,1)S(1)} collective-permute-done((bf16[256,256]{1,0:T(8,128)(2,1)S(1)}, bf16[256,256]{1,0:T(8,128)(2,1)S(1)}, u32[]{:S(2)}, u32[]{:S(2)}) %collective-permute-start.7) | collective-permute-done | bytes 131104 | tf_op jit(solution)/shard_map/ppermute | solution.py:574
  156.4 0.0 collective-permute-done.9
  156.4 0.1 fusion.3
  156.5 2.5 %collective-permute-start.10 = (bf16[512,256]{1,0:T(8,128)(2,1)S(1)}, bf16[512,256]{1,0:T(8,128)(2,1)S(1)}, u32[]{:S(2)}, u32[]{:S(2)}) collective-permute-start(bf16[512,256]{1,0:T(8,128)(2,1)S(1)} %get-tuple-element.40), channel_id=1, source_target_pairs={{0,6},{1,7},{2,0},{3,1},{4,2},{5,3},{6,4},{7,5},{8,14},{9,15},{10,... | collective-permute-start | bytes 786440 | tf_op jit(solution)/shard_map/ppermute | solution.py:574
  159.0 0.0 collective-permute-start.8
  159.0 4.2 %collective-permute-done.10 = bf16[512,256]{1,0:T(8,128)(2,1)S(1)} collective-permute-done((bf16[512,256]{1,0:T(8,128)(2,1)S(1)}, bf16[512,256]{1,0:T(8,128)(2,1)S(1)}, u32[]{:S(2)}, u32[]{:S(2)}) %collective-permute-start.10) | collective-permute-done | bytes 262176 | tf_op jit(solution)/shard_map/ppermute | solution.py:574
  163.3 3.0 %collective-permute-done.8 = bf16[512,256]{1,0:T(8,128)(2,1)S(1)} collective-permute-done((bf16[512,256]{1,0:T(8,128)(2,1)S(1)}, bf16[512,256]{1,0:T(8,128)(2,1)S(1)}, u32[]{:S(2)}, u32[]{:S(2)}) %collective-permute-start.8) | collective-permute-done | bytes 262176 | tf_op jit(solution)/shard_map/ppermute | solution.py:574
  166.3 0.8 fusion.7
  (17 shorter events, 0.0 us)
Async XLA Ops:
  6.5 8.8 %copy-start.8 = (f32[8]{0:T(128)S(1)}, f32[8]{0:T(128)}, u32[]{:S(2)}) copy-start(f32[8]{0:T(128)} %param.24) | copy-start | bytes 100
  6.5 128.2 %all-gather.3.cloned.1.call-start = ((), (), s32[]{:S(2)}) async-start(), calls=%async_computation.2 | async-start | bytes 9191424 | tf_op jit(solution)/shard_map/all_gather | solution.py:630
  8.5 30.5 %copy-start.7 = (bf16[512]{0:T(512)(128)(2,1)S(1)}, bf16[512]{0:T(512)(128)(2,1)}, u32[]{:S(2)}) copy-start(bf16[512]{0:T(512)(128)(2,1)} %param.30) | copy-start | bytes 3076
  10.1 6.4 %collective-permute-start = (bf16[16,896]{1,0:T(8,128)(2,1)}, bf16[16,896]{1,0:T(8,128)(2,1)S(1)}, u32[]{:S(2)}, u32[]{:S(2)}) collective-permute-start(bf16[16,896]{1,0:T(8,128)(2,1)} %pack_edge.1), channel_id=1, source_target_pairs={{0,8},{8,16},{16,24},{24,32},{32,40},{40,48},{48,56},{56,64},{64,7... | collective-permute-start | bytes 86024 | tf_op jit(solution)/shard_map/ppermute | solution.py:24
  16.5 0.6 copy-start.9
  22.1 6.7 %collective-permute-start.1 = (bf16[528,128]{1,0:T(8,128)(2,1)}, bf16[528,128]{1,0:T(8,128)(2,1)S(1)}, u32[]{:S(2)}, u32[]{:S(2)}) collective-permute-start(bf16[528,128]{1,0:T(8,128)(2,1)} %get-tuple-element.22.own_ref), channel_id=1, source_target_pairs={{0,8},{8,16},{16,24},{24,32},{32,40},{40,48},{48,56},{56,64},{64,7... | collective-permute-start | bytes 405512 | tf_op jit(solution)/shard_map/ppermute | solution.py:24
  28.9 0.7 copy-start.3
  31.2 12.9 %collective-permute-start.2 = (bf16[512,128]{1,0:T(8,128)(2,1)}, bf16[512,128]{1,0:T(8,128)(2,1)S(1)}, u32[]{:S(2)}, u32[]{:S(2)}) collective-permute-start(bf16[512,128]{1,0:T(8,128)(2,1)} %join_states.1), channel_id=1, source_target_pairs={{0,16},{8,24},{16,32},{24,40},{32,48},{40,56},{48,64},{56,72},{64,... | collective-permute-start | bytes 393224 | tf_op jit(solution)/shard_map/ppermute | solution.py:24
  44.0 0.7 copy-start.5
  51.2 20.9 %collective-permute-start.3 = (bf16[4,512,256]{2,1,0:T(8,128)(2,1)}, bf16[4,512,256]{2,1,0:T(8,128)(2,1)S(1)}, u32[]{:S(2)}, u32[]{:S(2)}) collective-permute-start(bf16[4,512,256]{2,1,0:T(8,128)(2,1)} %get-tuple-element.32), channel_id=1, source_target_pairs={{0,1},{1,0},{2,3},{3,2},{4,5},{5,4},{6,7},{7,6},{8,9},{9,8},{10,11... | collective-permute-start | bytes 3145736 | tf_op jit(solution)/shard_map/ppermute | solution.py:569
  94.1 19.7 %copy-start.6 = (bf16[2048]{0:T(1024)(128)(2,1)S(1)}, bf16[2048]{0:T(1024)(128)(2,1)}, u32[]{:S(2)}) copy-start(bf16[2048]{0:T(1024)(128)(2,1)} %param.32) | copy-start | bytes 12292
  111.7 4.4 %copy-start = (bf16[4,512,256]{2,1,0:T(8,128)(2,1)}, bf16[4,512,256]{2,1,0:T(8,128)(2,1)S(1)}, u32[]{:S(2)}) copy-start(bf16[4,512,256]{2,1,0:T(8,128)(2,1)S(1)} %all_to_all.11.mine_ref) | copy-start | bytes 3145732
  111.7 4.4 %collective-permute-start.4 = (bf16[4,512,256]{2,1,0:T(8,128)(2,1)S(1)}, bf16[4,512,256]{2,1,0:T(8,128)(2,1)S(1)}, u32[]{:S(2)}, u32[]{:S(2)}) collective-permute-start(bf16[4,512,256]{2,1,0:T(8,128)(2,1)S(1)} %all_to_all.11.mine_ref), channel_id=1, source_target_pairs={{0,1},{1,0},{2,3},{3,2},{4,5},{5,4},{6,7},{7,6},{8,9},{9,8},{10,11... | collective-permute-start | bytes 3145736 | tf_op jit(solution)/shard_map/ppermute | solution.py:569
  116.1 1.0 copy-start.1
  144.6 8.6 %copy-start.2 = (bf16[3,512,256]{2,1,0:T(8,128)(2,1)S(1)}, bf16[3,512,256]{2,1,0:T(8,128)(2,1)}, u32[]{:S(2)}) copy-start(bf16[3,512,256]{2,1,0:T(8,128)(2,1)} %get-tuple-element.35) | copy-start | bytes 2359300
  144.6 8.6 %collective-permute-start.5 = (bf16[3,512,256]{2,1,0:T(8,128)(2,1)}, bf16[3,512,256]{2,1,0:T(8,128)(2,1)S(1)}, u32[]{:S(2)}, u32[]{:S(2)}) collective-permute-start(bf16[3,512,256]{2,1,0:T(8,128)(2,1)} %get-tuple-element.36), channel_id=1, source_target_pairs={{0,1},{1,0},{2,3},{3,2},{4,5},{5,4},{6,7},{7,6},{8,9},{9,8},{10,11... | collective-permute-start | bytes 2359304 | tf_op jit(solution)/shard_map/ppermute | solution.py:569
  146.9 2.5 %collective-permute-start.6 = (bf16[512,256]{1,0:T(8,128)(2,1)}, bf16[512,256]{1,0:T(8,128)(2,1)S(1)}, u32[]{:S(2)}, u32[]{:S(2)}) collective-permute-start(bf16[512,256]{1,0:T(8,128)(2,1)} %get-tuple-element.38), channel_id=1, source_target_pairs={{0,1},{1,0},{2,3},{3,2},{4,5},{5,4},{6,7},{7,6},{8,9},{9,8},{10,11... | collective-permute-start | bytes 786440 | tf_op jit(solution)/shard_map/ppermute | solution.py:569
  150.4 6.0 %collective-permute-start.7 = (bf16[256,256]{1,0:T(8,128)(2,1)S(1)}, bf16[256,256]{1,0:T(8,128)(2,1)S(1)}, u32[]{:S(2)}, u32[]{:S(2)}) collective-permute-start(bf16[256,256]{1,0:T(8,128)(2,1)S(1)} %get-tuple-element.41), channel_id=1, source_target_pairs={{0,2},{1,3},{2,4},{3,5},{4,6},{5,7},{6,0},{7,1},{8,10},{9,11},{10,... | collective-permute-start | bytes 393224 | tf_op jit(solution)/shard_map/ppermute | solution.py:574
  151.7 4.7 %collective-permute-start.9 = (bf16[256,256]{1,0:T(8,128)(2,1)S(1)}, bf16[256,256]{1,0:T(8,128)(2,1)S(1)}, u32[]{:S(2)}, u32[]{:S(2)}) collective-permute-start(bf16[256,256]{1,0:T(8,128)(2,1)S(1)} %get-tuple-element.42), channel_id=1, source_target_pairs={{0,6},{1,7},{2,0},{3,1},{4,2},{5,3},{6,4},{7,5},{8,14},{9,15},{10,... | collective-permute-start | bytes 393224 | tf_op jit(solution)/shard_map/ppermute | solution.py:574
  153.4 12.9 %copy-start.4 = (bf16[512,256]{1,0:T(8,128)(2,1)S(1)}, bf16[512,256]{1,0:T(8,128)(2,1)}, u32[]{:S(2)}) copy-start(bf16[512,256]{1,0:T(8,128)(2,1)} %get-tuple-element.33) | copy-start | bytes 786436
  156.5 6.7 %collective-permute-start.10 = (bf16[512,256]{1,0:T(8,128)(2,1)S(1)}, bf16[512,256]{1,0:T(8,128)(2,1)S(1)}, u32[]{:S(2)}, u32[]{:S(2)}) collective-permute-start(bf16[512,256]{1,0:T(8,128)(2,1)S(1)} %get-tuple-element.40), channel_id=1, source_target_pairs={{0,6},{1,7},{2,0},{3,1},{4,2},{5,3},{6,4},{7,5},{8,14},{9,15},{10,... | collective-permute-start | bytes 786440 | tf_op jit(solution)/shard_map/ppermute | solution.py:574
  159.0 7.3 %collective-permute-start.8 = (bf16[512,256]{1,0:T(8,128)(2,1)S(1)}, bf16[512,256]{1,0:T(8,128)(2,1)S(1)}, u32[]{:S(2)}, u32[]{:S(2)}) collective-permute-start(bf16[512,256]{1,0:T(8,128)(2,1)S(1)} %get-tuple-element.39), channel_id=1, source_target_pairs={{0,2},{1,3},{2,4},{3,5},{4,6},{5,7},{6,0},{7,1},{8,10},{9,11},{10,... | collective-permute-start | bytes 786440 | tf_op jit(solution)/shard_map/ppermute | solution.py:574
Sparse Core Ops, SparseCore 0:
  9.1 125.5 all-gather.2

commit v7 on v6

--- a/solution.py
+++ b/solution.py
@@ -580,14 +580,21 @@
     other_near = to_partner(other_near)
     half = mine_far.shape[0] // 2
     far = mine_far.astype(F32) + other_far.astype(F32)
-    low = to_chip(far[:half].astype(BF16), 1)
-    high = to_chip(far[half:].astype(BF16), -1)
+    low = to_chip(far[:half].astype(BF16), 1).astype(F32)
+    high = to_chip(far[half:].astype(BF16), -1).astype(F32)
     near = mine_near.astype(F32) + other_near.astype(F32)
-    low = jnp.pad(low, ((0, half), (0, 0))).astype(F32)
-    high = jnp.pad(high, ((half, 0), (0, 0))).astype(F32)
-    right = to_chip((near[1] + low).astype(BF16), 1)
-    left = to_chip((near[2] + high).astype(BF16), -1)
-    down = near[0] + right.astype(F32) + left.astype(F32)
+    right_high = to_chip(near[1, half:].astype(BF16), 1)
+    left_low = to_chip(near[2, :half].astype(BF16), -1)
+    right_low = to_chip((near[1, :half] + low).astype(BF16), 1)
+    left_high = to_chip((near[2, half:] + high).astype(BF16), -1)
+    down = near[0]
+    for part, place in (
+        (right_low, (0, half)),
+        (left_low, (0, half)),
+        (right_high, (half, 0)),
+        (left_high, (half, 0)),
+    ):
+        down = down + jnp.pad(part, (place, (0, 0))).astype(F32)
     return (after.astype(F32) + down).astype(BF16)
 
 

time: 175 us -> 176 us (level)
    ppermute x4 -> x6, starting transfers between devices: 5.29 us -> 6.92 us  [to_chip(): lax.ppermute(value, 'tp', [(i, (i + 2 * by) % peers) for i in range(peers)])]
    ppermute x4 -> x6, waiting for transfers between devices: 10.3 us -> 8.95 us  [to_chip(): lax.ppermute(value, 'tp', [(i, (i + 2 * by) % peers) for i in range(peers)])]
  transfers between devices with their start and end apart: 12 -> 14, of which waited for: 10 -> 11; matrix products, arithmetic and copies ran while one was open for 3% -> 3% of each run, Pallas kernels for 15% -> 14%
where the time goes in v7:
time: 176 us; the launch traced here: 174 us
  starting transfers between devices  47.4 us (27%)
  blocking collectives  35.6 us (20%)
  Pallas kernels  35.1 us (20%)
  waiting for transfers between devices  32.2 us (18%)
  between operations  13.5 us (8%)
  other arithmetic  5.61 us (3%)
  local copies, waits for them, and re-layouts  4.88 us (3%)
    all_to_all x2, blocking collectives, exchange(): return lax.all_to_all(value, 'tp', 0, 0, axis_index_groups=rows, tiled=True)  35.6 us
    ppermute x4, starting transfers between devices, to_partner(): lax.ppermute(value, 'tp', [(i, i ^ 1) for i in range(lax.axis_size('tp'))])  22.9 us
    ppermute x3, starting transfers between devices, from_behind(): return lax.ppermute(value, axis, pairs)  17.5 us
    all_gather x1, waiting for transfers between devices, on_device(): weights = lax.all_gather(late, 'sp', axis=0)  13.6 us
    pallas_call x1, Pallas kernels, channel_mixer(): pl.pallas_call(functools.partial(mixer_kernel, tiles), in_specs=[smem(),...  9.82 us
    ppermute x6, waiting for transfers between devices, to_chip(): lax.ppermute(value, 'tp', [(i, (i + 2 * by) % peers) for i in range(peers)])  8.95 us
    ppermute x6, starting transfers between devices, to_chip(): lax.ppermute(value, 'tp', [(i, (i + 2 * by) % peers) for i in range(peers)])  6.92 us
    ppermute x4, waiting for transfers between devices, to_partner(): lax.ppermute(value, 'tp', [(i, i ^ 1) for i in range(lax.axis_size('tp'))])  6.53 us
  transfers between devices with their start and end apart: 14, of which 11 were waited for; matrix products, arithmetic and copies ran while one was open for 3% of the time, Pallas kernels for 14%

profile of v7, /device:TPU:33, one launch (start us, length us, event | category | flops | bytes accessed | tf_op | source)
XLA Modules:
  0.0 174.3 jit_solution(17920249825789433290)
XLA Ops:
  6.6 1.9 %pad_maximum_fusion = bf16[2112,128]{1,0:T(8,128)(2,1)} fusion(bf16[704,128]{1,0:T(8,128)(2,1)} %bitcast.38, bf16[704,128]{1,0:T(8,128)(2,1)} %bitcast.39, bf16[704,128]{1,0:T(8,128)(2,1)} %bitcast.40), kind=kLoop, calls=%fused_computation.2 | loop fusion | flops 1622016 | bytes 1081344 | tf_op jit(solution)/shard_map/concatenate | solution.py:636
  8.5 0.1 all-gather.3.cloned.1.call-update
  8.6 1.5 pack_edge.1
  10.1 5.2 %collective-permute-start = (bf16[16,896]{1,0:T(8,128)(2,1)}, bf16[16,896]{1,0:T(8,128)(2,1)S(1)}, u32[]{:S(2)}, u32[]{:S(2)}) collective-permute-start(bf16[16,896]{1,0:T(8,128)(2,1)} %pack_edge.1), channel_id=1, source_target_pairs={{0,8},{8,16},{16,24},{24,32},{32,40},{40,48},{48,56},{56,64},{64,7... | collective-permute-start | bytes 86024 | tf_op jit(solution)/shard_map/ppermute | solution.py:24
  15.3 0.7 copy.19.rate_ref
  16.0 0.5 collective-permute-done.before_ref
  16.5 0.6 copy-done.9
  17.1 5.0 %local_states.1 = (bf16[512,512]{1,0:T(8,128)(2,1)}, bf16[512,128]{1,0:T(8,128)(2,1)}, f32[8,512]{1,0:T(8,128)}, f32[8,512]{1,0:T(8,128)}, bf16[3,512,128]{2,1,0:T(8,128)(2,1)}, /*index=5*/bf16[528,128]{1,0:T(8,128)(2,1)}) custom-call(bf16[16,896]{1,0:T(8,128)(2,1)} %copy-done.9, bf16[512,512]{1,0:T(8,128)(2,1)} %values_ref.3, bf16[512,128]{1,0:T(8,128)(2,1)} %writes_ref.3, ...), custom_call_target="tpu_custom_call" | custom-call | flops 400000000 | bytes 4000000 | tf_op jit(solution)/shard_map/local_states/pallas_call | solution.py:211
  22.1 4.4 %collective-permute-start.1 = (bf16[528,128]{1,0:T(8,128)(2,1)}, bf16[528,128]{1,0:T(8,128)(2,1)S(1)}, u32[]{:S(2)}, u32[]{:S(2)}) collective-permute-start(bf16[528,128]{1,0:T(8,128)(2,1)} %get-tuple-element.22.own_ref), channel_id=1, source_target_pairs={{0,8},{8,16},{16,24},{24,32},{32,40},{40,48},{48,56},{56,64},{64,7... | collective-permute-start | bytes 405512 | tf_op jit(solution)/shard_map/ppermute | solution.py:24
  26.6 2.3 %collective-permute-done.1.near_ref = bf16[528,128]{1,0:T(8,128)(2,1)S(1)} collective-permute-done((bf16[528,128]{1,0:T(8,128)(2,1)}, bf16[528,128]{1,0:T(8,128)(2,1)S(1)}, u32[]{:S(2)}, u32[]{:S(2)}) %collective-permute-start.1) | collective-permute-done | bytes 135200 | tf_op jit(solution)/shard_map/ppermute | solution.py:24
  28.9 0.7 copy-done.3
  29.5 1.7 join_states.1
  31.2 7.8 %collective-permute-start.2 = (bf16[512,128]{1,0:T(8,128)(2,1)}, bf16[512,128]{1,0:T(8,128)(2,1)S(1)}, u32[]{:S(2)}, u32[]{:S(2)}) collective-permute-start(bf16[512,128]{1,0:T(8,128)(2,1)} %join_states.1), channel_id=1, source_target_pairs={{0,16},{8,24},{16,32},{24,40},{32,48},{40,56},{48,64},{56,72},{64,... | collective-permute-start | bytes 393224 | tf_op jit(solution)/shard_map/ppermute | solution.py:24
  39.1 0.6 reshape.24.gain_ref
  39.6 4.1 %local_mix.1 = (bf16[512,128]{1,0:T(8,128)(2,1)}, f32[512,512]{1,0:T(8,128)}, f32[8,512]{1,0:T(8,128)}) custom-call(bf16[16,896]{1,0:T(8,128)(2,1)} %copy-done.9, bf16[512,128]{1,0:T(8,128)(2,1)} %reads_ref.3, s32[4,128]{1,0:T(4,128)} %bitcast.43, bf16[4,128]{1,0:T(4,128)(2,1)} %taps_ref.1, bf16[512,512]{1,0:T(8,128)(2,1)} %get-tuple-element.23.sv_ref, ...), custom_call_target="tpu_custom_call" | custom-call | flops 800000000 | bytes 4000000 | tf_op jit(solution)/shard_map/local_mix/pallas_call | solution.py:331
  43.7 0.3 collective-permute-done.2.far_ref
  44.1 0.7 copy-done.5
  44.7 6.5 %project.1 = (bf16[4,512,256]{2,1,0:T(8,128)(2,1)}, bf16[4,512,256]{2,1,0:T(8,128)(2,1)}) custom-call(s32[1]{0:T(128)} %bitcast.1.core_ref, bf16[528,128]{1,0:T(8,128)(2,1)} %copy-done.3, bf16[512,128]{1,0:T(8,128)(2,1)} %copy-done.5, bf16[512,128]{1,0:T(8,128)(2,1)} %get-tuple-element.28.sr_ref, f32[512,512]{1,0:T(8,128)} %get-tuple-element.29.mixed_ref, ...), custom_call_target="tpu_custom_call" | custom-call | flops 1073741824 | bytes 6000000 | tf_op jit(solution)/shard_map/project/pallas_call | solution.py:405
  51.2 18.4 %collective-permute-start.3 = (bf16[4,512,256]{2,1,0:T(8,128)(2,1)}, bf16[4,512,256]{2,1,0:T(8,128)(2,1)S(1)}, u32[]{:S(2)}, u32[]{:S(2)}) collective-permute-start(bf16[4,512,256]{2,1,0:T(8,128)(2,1)} %get-tuple-element.32), channel_id=1, source_target_pairs={{0,1},{1,0},{2,3},{3,2},{4,5},{5,4},{6,7},{7,6},{8,9},{9,8},{10,11... | collective-permute-start | bytes 3145736 | tf_op jit(solution)/shard_map/ppermute | solution.py:569
  69.6 2.5 %collective-permute-done.3 = bf16[4,512,256]{2,1,0:T(8,128)(2,1)S(1)} collective-permute-done((bf16[4,512,256]{2,1,0:T(8,128)(2,1)}, bf16[4,512,256]{2,1,0:T(8,128)(2,1)S(1)}, u32[]{:S(2)}, u32[]{:S(2)}) %collective-permute-start.3) | collective-permute-done | bytes 1048608 | tf_op jit(solution)/shard_map/ppermute | solution.py:569
  72.1 1.5 add_convert_fusion
  73.6 18.0 %all_to_all.10.parts_ref = bf16[4,512,256]{2,1,0:T(8,128)(2,1)} all-to-all(bf16[4,512,256]{2,1,0:T(8,128)(2,1)S(1)} %add_convert_fusion), channel_id=1, replica_groups={{0,2,4,6},{1,3,5,7},{8,10,12,14},{9,11,13,15},{16,18,20,22},{17,19,21,2..., dimensions={0} | all-to-all | bytes 2097152 | tf_op jit(solution)/shard_map/all_to_all | solution.py:604
  91.7 2.5 %after_mix.1 = (bf16[512,256]{1,0:T(8,128)(2,1)}, bf16[4,512,256]{2,1,0:T(8,128)(2,1)}) custom-call(s32[1]{0:T(128)} %bitcast.at_ref, bf16[4,512,256]{2,1,0:T(8,128)(2,1)} %all_to_all.10.parts_ref, bf16[512,2048]{1,0:T(8,128)(2,1)} %residual_ref.1), custom_call_target="tpu_custom_call" | custom-call | tf_op jit(solution)/shard_map/after_mix/pallas_call | solution.py:429
  94.2 17.6 %all_to_all.11.mine_ref = bf16[4,512,256]{2,1,0:T(8,128)(2,1)S(1)} all-to-all(bf16[4,512,256]{2,1,0:T(8,128)(2,1)} %get-tuple-element.34), channel_id=1, replica_groups={{0,2,4,6},{1,3,5,7},{8,10,12,14},{9,11,13,15},{16,18,20,22},{17,19,21,2..., dimensions={0} | all-to-all | bytes 2097152 | tf_op jit(solution)/shard_map/all_to_all | solution.py:604
  111.8 2.1 %collective-permute-start.4 = (bf16[4,512,256]{2,1,0:T(8,128)(2,1)S(1)}, bf16[4,512,256]{2,1,0:T(8,128)(2,1)S(1)}, u32[]{:S(2)}, u32[]{:S(2)}) collective-permute-start(bf16[4,512,256]{2,1,0:T(8,128)(2,1)S(1)} %all_to_all.11.mine_ref), channel_id=1, source_target_pairs={{0,1},{1,0},{2,3},{3,2},{4,5},{5,4},{6,7},{7,6},{8,9},{9,8},{10,11... | collective-permute-start | bytes 3145736 | tf_op jit(solution)/shard_map/ppermute | solution.py:569
  113.9 0.6 reshape.25.gain_ref
  114.5 1.7 collective-permute-done.4.other_ref
  116.1 1.0 copy-done.1
  117.2 4.0 %normalised.1.normal_ref = bf16[512,2048]{1,0:T(8,128)(2,1)} custom-call(s32[1]{0:T(128)} %bitcast.at_ref, bf16[4,512,256]{2,1,0:T(8,128)(2,1)} %copy-done, bf16[4,512,256]{2,1,0:T(8,128)(2,1)} %copy-done.1, bf16[1,2048]{1,0:T(2,128)(2,1)} %reshape.25.gain_ref), custom_call_target="tpu_custom_call" | custom-call | tf_op jit(solution)/shard_map/normalised/pallas_call | solution.py:468
  121.2 13.6 %all-gather.3.cloned.1.call-done = bf16[33792,128]{1,0:T(8,128)(2,1)} async-done(((bf16[2112,128]{1,0:T(8,128)(2,1)}), bf16[33792,128]{1,0:T(8,128)(2,1)}) %all-gather.3.cloned.1.call-update) | async-done | bytes 8650768 | tf_op jit(solution)/shard_map/all_gather | solution.py:637
  134.8 9.8 %channel_mixer.1 = (bf16[512,256]{1,0:T(8,128)(2,1)}, bf16[512,256]{1,0:T(8,128)(2,1)}, bf16[3,512,256]{2,1,0:T(8,128)(2,1)}, bf16[3,512,256]{2,1,0:T(8,128)(2,1)}) custom-call(s32[1]{0:T(128)} %bitcast.at_ref, bf16[512,2048]{1,0:T(8,128)(2,1)} %normalised.1.normal_ref, bf16[16,2112,128]{2,1,0:T(8,128)(2,1)} %bitcast.45), custom_call_target="tpu_custom_call" | custom-call | flops 4429185024 | bytes 14000000 | tf_op jit(solution)/shard_map/channel_mixer/pallas_call | solution.py:545
  144.6 2.3 %collective-permute-start.5 = (bf16[3,512,256]{2,1,0:T(8,128)(2,1)}, bf16[3,512,256]{2,1,0:T(8,128)(2,1)S(1)}, u32[]{:S(2)}, u32[]{:S(2)}) collective-permute-start(bf16[3,512,256]{2,1,0:T(8,128)(2,1)} %get-tuple-element.36), channel_id=1, source_target_pairs={{0,1},{1,0},{2,3},{3,2},{4,5},{5,4},{6,7},{7,6},{8,9},{9,8},{10,11... | collective-permute-start | bytes 2359304 | tf_op jit(solution)/shard_map/ppermute | solution.py:569
  146.9 0.1 collective-permute-start.6
  147.0 2.3 %collective-permute-done.6 = bf16[512,256]{1,0:T(8,128)(2,1)S(1)} collective-permute-done((bf16[512,256]{1,0:T(8,128)(2,1)}, bf16[512,256]{1,0:T(8,128)(2,1)S(1)}, u32[]{:S(2)}, u32[]{:S(2)}) %collective-permute-start.6) | collective-permute-done | bytes 262176 | tf_op jit(solution)/shard_map/ppermute | solution.py:569
  149.4 1.0 add_convert_fusion.1
  150.4 2.6 %collective-permute-start.11 = (bf16[256,256]{1,0:T(8,128)(2,1)S(1)}, bf16[256,256]{1,0:T(8,128)(2,1)S(1)}, u32[]{:S(2)}, u32[]{:S(2)}) collective-permute-start(bf16[256,256]{1,0:T(8,128)(2,1)S(1)} %get-tuple-element.46), channel_id=1, source_target_pairs={{0,6},{1,7},{2,0},{3,1},{4,2},{5,3},{6,4},{7,5},{8,14},{9,15},{10,... | collective-permute-start | bytes 393224 | tf_op jit(solution)/shard_map/ppermute | solution.py:574
  153.0 0.2 fusion.10
  153.2 0.0 copy-start.4
  153.2 2.2 %collective-permute-done.11 = bf16[256,256]{1,0:T(8,128)(2,1)S(1)} collective-permute-done((bf16[256,256]{1,0:T(8,128)(2,1)S(1)}, bf16[256,256]{1,0:T(8,128)(2,1)S(1)}, u32[]{:S(2)}, u32[]{:S(2)}) %collective-permute-start.11) | collective-permute-done | bytes 131104 | tf_op jit(solution)/shard_map/ppermute | solution.py:574
  155.5 3.1 %collective-permute-done.7 = bf16[256,256]{1,0:T(8,128)(2,1)S(1)} collective-permute-done((bf16[256,256]{1,0:T(8,128)(2,1)S(1)}, bf16[256,256]{1,0:T(8,128)(2,1)S(1)}, u32[]{:S(2)}, u32[]{:S(2)}) %collective-permute-start.7) | collective-permute-done | bytes 131104 | tf_op jit(solution)/shard_map/ppermute | solution.py:574
  158.6 0.1 fusion.9
  158.6 0.4 collective-permute-start.12
  159.0 1.2 collective-permute-start.8
  160.2 0.1 collective-permute-start.10
  160.4 2.6 %collective-permute-start.9 = (bf16[256,256]{1,0:T(8,128)(2,1)S(1)}, bf16[256,256]{1,0:T(8,128)(2,1)S(1)}, u32[]{:S(2)}, u32[]{:S(2)}) collective-permute-start(bf16[256,256]{1,0:T(8,128)(2,1)S(1)} %get-tuple-element.43), channel_id=1, source_target_pairs={{0,6},{1,7},{2,0},{3,1},{4,2},{5,3},{6,4},{7,5},{8,14},{9,15},{10,... | collective-permute-start | bytes 393224 | tf_op jit(solution)/shard_map/ppermute | solution.py:574
  163.0 1.0 collective-permute-done.8
  164.1 2.5 %collective-permute-done.10 = bf16[256,256]{1,0:T(8,128)(2,1)S(1)} collective-permute-done((bf16[256,256]{1,0:T(8,128)(2,1)S(1)}, bf16[256,256]{1,0:T(8,128)(2,1)S(1)}, u32[]{:S(2)}, u32[]{:S(2)}) %collective-permute-start.10) | collective-permute-done | bytes 131104 | tf_op jit(solution)/shard_map/ppermute | solution.py:574
  166.6 0.8 fusion.5
  (22 shorter events, 0.1 us)
Async XLA Ops:
  6.5 8.8 %copy-start.8 = (f32[8]{0:T(128)S(1)}, f32[8]{0:T(128)}, u32[]{:S(2)}) copy-start(f32[8]{0:T(128)} %param.24) | copy-start | bytes 100
  6.5 128.2 %all-gather.3.cloned.1.call-start = ((), (), s32[]{:S(2)}) async-start(), calls=%async_computation.2 | async-start | bytes 9191424 | tf_op jit(solution)/shard_map/all_gather | solution.py:637
  8.5 30.6 %copy-start.7 = (bf16[512]{0:T(512)(128)(2,1)S(1)}, bf16[512]{0:T(512)(128)(2,1)}, u32[]{:S(2)}) copy-start(bf16[512]{0:T(512)(128)(2,1)} %param.30) | copy-start | bytes 3076
  10.1 6.4 %collective-permute-start = (bf16[16,896]{1,0:T(8,128)(2,1)}, bf16[16,896]{1,0:T(8,128)(2,1)S(1)}, u32[]{:S(2)}, u32[]{:S(2)}) collective-permute-start(bf16[16,896]{1,0:T(8,128)(2,1)} %pack_edge.1), channel_id=1, source_target_pairs={{0,8},{8,16},{16,24},{24,32},{32,40},{40,48},{48,56},{56,64},{64,7... | collective-permute-start | bytes 86024 | tf_op jit(solution)/shard_map/ppermute | solution.py:24
  16.5 0.6 copy-start.9
  22.1 6.7 %collective-permute-start.1 = (bf16[528,128]{1,0:T(8,128)(2,1)}, bf16[528,128]{1,0:T(8,128)(2,1)S(1)}, u32[]{:S(2)}, u32[]{:S(2)}) collective-permute-start(bf16[528,128]{1,0:T(8,128)(2,1)} %get-tuple-element.22.own_ref), channel_id=1, source_target_pairs={{0,8},{8,16},{16,24},{24,32},{32,40},{40,48},{48,56},{56,64},{64,7... | collective-permute-start | bytes 405512 | tf_op jit(solution)/shard_map/ppermute | solution.py:24
  28.9 0.7 copy-start.3
  31.2 12.9 %collective-permute-start.2 = (bf16[512,128]{1,0:T(8,128)(2,1)}, bf16[512,128]{1,0:T(8,128)(2,1)S(1)}, u32[]{:S(2)}, u32[]{:S(2)}) collective-permute-start(bf16[512,128]{1,0:T(8,128)(2,1)} %join_states.1), channel_id=1, source_target_pairs={{0,16},{8,24},{16,32},{24,40},{32,48},{40,56},{48,64},{56,72},{64,... | collective-permute-start | bytes 393224 | tf_op jit(solution)/shard_map/ppermute | solution.py:24
  44.1 0.7 copy-start.5
  51.2 20.9 %collective-permute-start.3 = (bf16[4,512,256]{2,1,0:T(8,128)(2,1)}, bf16[4,512,256]{2,1,0:T(8,128)(2,1)S(1)}, u32[]{:S(2)}, u32[]{:S(2)}) collective-permute-start(bf16[4,512,256]{2,1,0:T(8,128)(2,1)} %get-tuple-element.32), channel_id=1, source_target_pairs={{0,1},{1,0},{2,3},{3,2},{4,5},{5,4},{6,7},{7,6},{8,9},{9,8},{10,11... | collective-permute-start | bytes 3145736 | tf_op jit(solution)/shard_map/ppermute | solution.py:569
  94.2 19.7 %copy-start.6 = (bf16[2048]{0:T(1024)(128)(2,1)S(1)}, bf16[2048]{0:T(1024)(128)(2,1)}, u32[]{:S(2)}) copy-start(bf16[2048]{0:T(1024)(128)(2,1)} %param.32) | copy-start | bytes 12292
  111.8 4.4 %copy-start = (bf16[4,512,256]{2,1,0:T(8,128)(2,1)}, bf16[4,512,256]{2,1,0:T(8,128)(2,1)S(1)}, u32[]{:S(2)}) copy-start(bf16[4,512,256]{2,1,0:T(8,128)(2,1)S(1)} %all_to_all.11.mine_ref) | copy-start | bytes 3145732
  111.8 4.4 %collective-permute-start.4 = (bf16[4,512,256]{2,1,0:T(8,128)(2,1)S(1)}, bf16[4,512,256]{2,1,0:T(8,128)(2,1)S(1)}, u32[]{:S(2)}, u32[]{:S(2)}) collective-permute-start(bf16[4,512,256]{2,1,0:T(8,128)(2,1)S(1)} %all_to_all.11.mine_ref), channel_id=1, source_target_pairs={{0,1},{1,0},{2,3},{3,2},{4,5},{5,4},{6,7},{7,6},{8,9},{9,8},{10,11... | collective-permute-start | bytes 3145736 | tf_op jit(solution)/shard_map/ppermute | solution.py:569
  116.1 1.0 copy-start.1
  144.6 8.4 %copy-start.2 = (bf16[3,512,256]{2,1,0:T(8,128)(2,1)S(1)}, bf16[3,512,256]{2,1,0:T(8,128)(2,1)}, u32[]{:S(2)}) copy-start(bf16[3,512,256]{2,1,0:T(8,128)(2,1)} %get-tuple-element.35) | copy-start | bytes 2359300
  144.6 8.4 %collective-permute-start.5 = (bf16[3,512,256]{2,1,0:T(8,128)(2,1)}, bf16[3,512,256]{2,1,0:T(8,128)(2,1)S(1)}, u32[]{:S(2)}, u32[]{:S(2)}) collective-permute-start(bf16[3,512,256]{2,1,0:T(8,128)(2,1)} %get-tuple-element.36), channel_id=1, source_target_pairs={{0,1},{1,0},{2,3},{3,2},{4,5},{5,4},{6,7},{7,6},{8,9},{9,8},{10,11... | collective-permute-start | bytes 2359304 | tf_op jit(solution)/shard_map/ppermute | solution.py:569
  146.9 2.5 %collective-permute-start.6 = (bf16[512,256]{1,0:T(8,128)(2,1)}, bf16[512,256]{1,0:T(8,128)(2,1)S(1)}, u32[]{:S(2)}, u32[]{:S(2)}) collective-permute-start(bf16[512,256]{1,0:T(8,128)(2,1)} %get-tuple-element.38), channel_id=1, source_target_pairs={{0,1},{1,0},{2,3},{3,2},{4,5},{5,4},{6,7},{7,6},{8,9},{9,8},{10,11... | collective-permute-start | bytes 786440 | tf_op jit(solution)/shard_map/ppermute | solution.py:569
  150.4 5.0 %collective-permute-start.11 = (bf16[256,256]{1,0:T(8,128)(2,1)S(1)}, bf16[256,256]{1,0:T(8,128)(2,1)S(1)}, u32[]{:S(2)}, u32[]{:S(2)}) collective-permute-start(bf16[256,256]{1,0:T(8,128)(2,1)S(1)} %get-tuple-element.46), channel_id=1, source_target_pairs={{0,6},{1,7},{2,0},{3,1},{4,2},{5,3},{6,4},{7,5},{8,14},{9,15},{10,... | collective-permute-start | bytes 393224 | tf_op jit(solution)/shard_map/ppermute | solution.py:574
  153.0 5.6 %collective-permute-start.7 = (bf16[256,256]{1,0:T(8,128)(2,1)S(1)}, bf16[256,256]{1,0:T(8,128)(2,1)S(1)}, u32[]{:S(2)}, u32[]{:S(2)}) collective-permute-start(bf16[256,256]{1,0:T(8,128)(2,1)S(1)} %get-tuple-element.45), channel_id=1, source_target_pairs={{0,2},{1,3},{2,4},{3,5},{4,6},{5,7},{6,0},{7,1},{8,10},{9,11},{10,... | collective-permute-start | bytes 393224 | tf_op jit(solution)/shard_map/ppermute | solution.py:574
  153.2 13.4 %copy-start.4 = (bf16[512,256]{1,0:T(8,128)(2,1)S(1)}, bf16[512,256]{1,0:T(8,128)(2,1)}, u32[]{:S(2)}) copy-start(bf16[512,256]{1,0:T(8,128)(2,1)} %get-tuple-element.33) | copy-start | bytes 786436
  158.6 4.4 %collective-permute-start.12 = (bf16[256,256]{1,0:T(8,128)(2,1)S(1)}, bf16[256,256]{1,0:T(8,128)(2,1)S(1)}, u32[]{:S(2)}, u32[]{:S(2)}) collective-permute-start(bf16[256,256]{1,0:T(8,128)(2,1)S(1)} %get-tuple-element.40), channel_id=1, source_target_pairs={{0,6},{1,7},{2,0},{3,1},{4,2},{5,3},{6,4},{7,5},{8,14},{9,15},{10,... | collective-permute-start | bytes 393224 | tf_op jit(solution)/shard_map/ppermute | solution.py:574
  159.0 5.0 %collective-permute-start.8 = (bf16[256,256]{1,0:T(8,128)(2,1)S(1)}, bf16[256,256]{1,0:T(8,128)(2,1)S(1)}, u32[]{:S(2)}, u32[]{:S(2)}) collective-permute-start(bf16[256,256]{1,0:T(8,128)(2,1)S(1)} %get-tuple-element.39), channel_id=1, source_target_pairs={{0,2},{1,3},{2,4},{3,5},{4,6},{5,7},{6,0},{7,1},{8,10},{9,11},{10,... | collective-permute-start | bytes 393224 | tf_op jit(solution)/shard_map/ppermute | solution.py:574
  160.2 6.4 %collective-permute-start.10 = (bf16[256,256]{1,0:T(8,128)(2,1)S(1)}, bf16[256,256]{1,0:T(8,128)(2,1)S(1)}, u32[]{:S(2)}, u32[]{:S(2)}) collective-permute-start(bf16[256,256]{1,0:T(8,128)(2,1)S(1)} %get-tuple-element.44), channel_id=1, source_target_pairs={{0,2},{1,3},{2,4},{3,5},{4,6},{5,7},{6,0},{7,1},{8,10},{9,11},{10,... | collective-permute-start | bytes 393224 | tf_op jit(solution)/shard_map/ppermute | solution.py:574
  160.4 6.2 %collective-permute-start.9 = (bf16[256,256]{1,0:T(8,128)(2,1)S(1)}, bf16[256,256]{1,0:T(8,128)(2,1)S(1)}, u32[]{:S(2)}, u32[]{:S(2)}) collective-permute-start(bf16[256,256]{1,0:T(8,128)(2,1)S(1)} %get-tuple-element.43), channel_id=1, source_target_pairs={{0,6},{1,7},{2,0},{3,1},{4,2},{5,3},{6,4},{7,5},{8,14},{9,15},{10,... | collective-permute-start | bytes 393224 | tf_op jit(solution)/shard_map/ppermute | solution.py:574
Sparse Core Ops, SparseCore 0:
  9.1 125.5 all-gather.2

commit v8 on v7

--- a/solution.py
+++ b/solution.py
@@ -477,7 +477,7 @@
     mine_far, other_far, mine_near, other_near = refs[:4]
     late, downs, hidden_ref, far, near, late_sem, down_sem, far_sem, near_sem = refs[4:]
     peers, units, _ = downs.shape
-    _, turns, _, _ = near.shape
+    tokens = hidden_ref.shape[0]
     core, chip = lax.rem(at_ref[0], 2), lax.div(at_ref[0], 2)
 
     heavy = []
@@ -519,18 +519,23 @@
         copy.start()
         stores.append(copy)
 
-    for turn in (2, 0, 1, 3):
+    half = tokens // 2
+    low, high = slice(0, half), slice(half, tokens)
+    for turn in (2, 1, 3, 0):
         for flip in (1, 0):
-            c = 2 * lax.rem(chip + turn, turns + 1) + (core ^ flip)
+            c = 2 * lax.rem(chip + turn, 4) + (core ^ flip)
             part = jnp.concatenate([downs[2 * c], downs[2 * c + 1]], axis=1)
             product = jnp.dot(hidden, part, preferred_element_type=F32).astype(BF16)
             if turn == 2:
-                far[flip] = product
+                far[flip, 0, 0], far[flip, 1, 0] = product[low], product[high]
+            elif turn == 1:
+                far[flip, 0, 1], near[flip, 2] = product[high], product[low]
+            elif turn == 3:
+                far[flip, 1, 1], near[flip, 3] = product[low], product[high]
                 store(far.at[flip], (mine_far, other_far)[flip], far_sem.at[flip])
             else:
-                k = (0, 1, None, 2)[turn]
-                near[flip, k] = product
-                store(near.at[flip, k], (mine_near, other_near)[flip].at[k], near_sem.at[flip, k])
+                near[flip, 0], near[flip, 1] = product[low], product[high]
+                store(near.at[flip], (mine_near, other_near)[flip], near_sem.at[flip])
     for copy in stores:
         copy.wait()
 
@@ -538,10 +543,10 @@
 def channel_mixer(at, normal, weights, share):
     tokens = normal.shape[0]
     peers, units, depth = weights.shape[0], weights.shape[1] // 3, weights.shape[2]
-    turns = normal.shape[1] // (2 * share) - 1
     tiles = [(f, min(256, units - f)) for f in range(0, units, 256)]
     anywhere = pl.BlockSpec(memory_space=pl.ANY)
-    far, near = shape((tokens, share), BF16), shape((turns, tokens, share), BF16)
+    far = shape((2, 2, tokens // 2, share), BF16)
+    near = shape((4, tokens // 2, share), BF16)
     return pl.pallas_call(
         functools.partial(mixer_kernel, tiles),
         in_specs=[smem(), vmem(), anywhere],
@@ -551,12 +556,12 @@
             pltpu.VMEM((peers, 2 * units, depth), BF16),
             pltpu.VMEM((peers, units, depth), BF16),
             pltpu.VMEM((tokens, units), BF16),
-            pltpu.VMEM((2, tokens, share), BF16),
-            pltpu.VMEM((2, turns, tokens, share), BF16),
+            pltpu.VMEM((2, *far.shape), BF16),
+            pltpu.VMEM((2, *near.shape), BF16),
             pltpu.SemaphoreType.DMA((len(tiles), 2)),
             pltpu.SemaphoreType.DMA,
             pltpu.SemaphoreType.DMA((2,)),
-            pltpu.SemaphoreType.DMA((2, turns)),
+            pltpu.SemaphoreType.DMA((2,)),
         ],
         cost_estimate=pl.CostEstimate(
             flops=6 * tokens * normal.shape[1] * units, transcendentals=0, bytes_accessed=14_000_000
@@ -578,16 +583,14 @@
     mine_far, other_far, mine_near, other_near = parts
     other_far = to_partner(other_far)
     other_near = to_partner(other_near)
-    half = mine_far.shape[0] // 2
-    far = mine_far.astype(F32) + other_far.astype(F32)
-    low = to_chip(far[:half].astype(BF16), 1).astype(F32)
-    high = to_chip(far[half:].astype(BF16), -1).astype(F32)
+    first = (mine_far.astype(F32) + other_far.astype(F32)).astype(BF16)
+    low, right_high = to_chip(first[0], 1)
+    high, left_low = to_chip(first[1], -1)
     near = mine_near.astype(F32) + other_near.astype(F32)
-    right_high = to_chip(near[1, half:].astype(BF16), 1)
-    left_low = to_chip(near[2, :half].astype(BF16), -1)
-    right_low = to_chip((near[1, :half] + low).astype(BF16), 1)
-    left_high = to_chip((near[2, half:] + high).astype(BF16), -1)
-    down = near[0]
+    right_low = to_chip((near[2] + low.astype(F32)).astype(BF16), 1)
+    left_high = to_chip((near[3] + high.astype(F32)).astype(BF16), -1)
+    down = near[:2].reshape(after.shape)
+    half = near.shape[1]
     for part, place in (
         (right_low, (0, half)),
         (left_low, (0, half)),

time: 176 us -> 175 us (level)
    ppermute x6 -> x4, waiting for transfers between devices: 8.95 us -> 10.9 us  [to_chip(): lax.ppermute(value, 'tp', [(i, (i + 2 * by) % peers) for i in range(peers)])]
    ppermute x6 -> x4, starting transfers between devices: 6.92 us -> 5.29 us  [to_chip(): lax.ppermute(value, 'tp', [(i, (i + 2 * by) % peers) for i in range(peers)])]
  transfers between devices with their start and end apart: 14 -> 12, of which waited for: 11 -> 10; matrix products, arithmetic and copies ran while one was open for 3% -> 3% of each run, Pallas kernels for 14% -> 15%
where the time goes in v8:
time: 175 us; the launch traced here: 174 us
  starting transfers between devices  45.7 us (26%)
  blocking collectives  35.5 us (20%)
  Pallas kernels  35.2 us (20%)
  waiting for transfers between devices  33.5 us (19%)
  between operations  13.6 us (8%)
  other arithmetic  5.64 us (3%)
  local copies, waits for them, and re-layouts  4.9 us (3%)
    all_to_all x2, blocking collectives, exchange(): return lax.all_to_all(value, 'tp', 0, 0, axis_index_groups=rows, tiled=True)  35.5 us
    ppermute x4, starting transfers between devices, to_partner(): lax.ppermute(value, 'tp', [(i, i ^ 1) for i in range(lax.axis_size('tp'))])  22.9 us
    ppermute x3, starting transfers between devices, from_behind(): return lax.ppermute(value, axis, pairs)  17.5 us
    all_gather x1, waiting for transfers between devices, on_device(): weights = lax.all_gather(late, 'sp', axis=0)  13.8 us
    ppermute x4, waiting for transfers between devices, to_chip(): lax.ppermute(value, 'tp', [(i, (i + 2 * by) % peers) for i in range(peers)])  10.9 us
    pallas_call x1, Pallas kernels, channel_mixer(): pl.pallas_call(functools.partial(mixer_kernel, tiles), in_specs=[smem(),...  9.92 us
    pallas_call x1, Pallas kernels, project(): pl.pallas_call(project_kernel, in_specs=[smem()] + [vmem()] * 8, out_shap...  6.47 us
    ppermute x4, waiting for transfers between devices, to_partner(): lax.ppermute(value, 'tp', [(i, i ^ 1) for i in range(lax.axis_size('tp'))])  5.78 us
  transfers between devices with their start and end apart: 12, of which 10 were waited for; matrix products, arithmetic and copies ran while one was open for 3% of the time, Pallas kernels for 15%

profile of v8, /device:TPU:33, one launch (start us, length us, event | category | flops | bytes accessed | tf_op | source)
XLA Modules:
  0.0 174.0 jit_solution(7773615418864517291)
XLA Ops:
  6.6 2.0 %pad_maximum_fusion = bf16[2112,128]{1,0:T(8,128)(2,1)} fusion(bf16[704,128]{1,0:T(8,128)(2,1)} %bitcast.32, bf16[704,128]{1,0:T(8,128)(2,1)} %bitcast.33, bf16[704,128]{1,0:T(8,128)(2,1)} %bitcast.34), kind=kLoop, calls=%fused_computation.3 | loop fusion | flops 1622016 | bytes 1081344 | tf_op jit(solution)/shard_map/concatenate | solution.py:639
  8.5 0.1 all-gather.3.cloned.1.call-update
  8.6 1.5 pack_edge.1
  10.1 5.2 %collective-permute-start = (bf16[16,896]{1,0:T(8,128)(2,1)}, bf16[16,896]{1,0:T(8,128)(2,1)S(1)}, u32[]{:S(2)}, u32[]{:S(2)}) collective-permute-start(bf16[16,896]{1,0:T(8,128)(2,1)} %pack_edge.1), channel_id=1, source_target_pairs={{0,8},{8,16},{16,24},{24,32},{32,40},{40,48},{48,56},{56,64},{64,7... | collective-permute-start | bytes 86024 | tf_op jit(solution)/shard_map/ppermute | solution.py:24
  15.4 0.7 copy.19.rate_ref
  16.0 0.5 collective-permute-done.before_ref
  16.5 0.6 copy-done.9
  17.1 5.0 %local_states.1 = (bf16[512,512]{1,0:T(8,128)(2,1)}, bf16[512,128]{1,0:T(8,128)(2,1)}, f32[8,512]{1,0:T(8,128)}, f32[8,512]{1,0:T(8,128)}, bf16[3,512,128]{2,1,0:T(8,128)(2,1)}, /*index=5*/bf16[528,128]{1,0:T(8,128)(2,1)}) custom-call(bf16[16,896]{1,0:T(8,128)(2,1)} %copy-done.9, bf16[512,512]{1,0:T(8,128)(2,1)} %values_ref.3, bf16[512,128]{1,0:T(8,128)(2,1)} %writes_ref.3, ...), custom_call_target="tpu_custom_call" | custom-call | flops 400000000 | bytes 4000000 | tf_op jit(solution)/shard_map/local_states/pallas_call | solution.py:211
  22.2 4.4 %collective-permute-start.1 = (bf16[528,128]{1,0:T(8,128)(2,1)}, bf16[528,128]{1,0:T(8,128)(2,1)S(1)}, u32[]{:S(2)}, u32[]{:S(2)}) collective-permute-start(bf16[528,128]{1,0:T(8,128)(2,1)} %get-tuple-element.22.own_ref), channel_id=1, source_target_pairs={{0,8},{8,16},{16,24},{24,32},{32,40},{40,48},{48,56},{56,64},{64,7... | collective-permute-start | bytes 405512 | tf_op jit(solution)/shard_map/ppermute | solution.py:24
  26.6 2.3 %collective-permute-done.1.near_ref = bf16[528,128]{1,0:T(8,128)(2,1)S(1)} collective-permute-done((bf16[528,128]{1,0:T(8,128)(2,1)}, bf16[528,128]{1,0:T(8,128)(2,1)S(1)}, u32[]{:S(2)}, u32[]{:S(2)}) %collective-permute-start.1) | collective-permute-done | bytes 135200 | tf_op jit(solution)/shard_map/ppermute | solution.py:24
  28.9 0.6 copy-done.2
  29.5 1.7 join_states.1
  31.2 7.9 %collective-permute-start.2 = (bf16[512,128]{1,0:T(8,128)(2,1)}, bf16[512,128]{1,0:T(8,128)(2,1)S(1)}, u32[]{:S(2)}, u32[]{:S(2)}) collective-permute-start(bf16[512,128]{1,0:T(8,128)(2,1)} %join_states.1), channel_id=1, source_target_pairs={{0,16},{8,24},{16,32},{24,40},{32,48},{40,56},{48,64},{56,72},{64,... | collective-permute-start | bytes 393224 | tf_op jit(solution)/shard_map/ppermute | solution.py:24
  39.0 0.0 copy-done.7
  39.0 0.6 reshape.31.gain_ref
  39.6 4.1 %local_mix.1 = (bf16[512,128]{1,0:T(8,128)(2,1)}, f32[512,512]{1,0:T(8,128)}, f32[8,512]{1,0:T(8,128)}) custom-call(bf16[16,896]{1,0:T(8,128)(2,1)} %copy-done.9, bf16[512,128]{1,0:T(8,128)(2,1)} %reads_ref.3, s32[4,128]{1,0:T(4,128)} %bitcast.37, bf16[4,128]{1,0:T(4,128)(2,1)} %taps_ref.1, bf16[512,512]{1,0:T(8,128)(2,1)} %get-tuple-element.23.sv_ref, ...), custom_call_target="tpu_custom_call" | custom-call | flops 800000000 | bytes 4000000 | tf_op jit(solution)/shard_map/local_mix/pallas_call | solution.py:331
  43.7 0.3 collective-permute-done.2.far_ref
  44.1 0.7 copy-done.5
  44.7 6.5 %project.1 = (bf16[4,512,256]{2,1,0:T(8,128)(2,1)}, bf16[4,512,256]{2,1,0:T(8,128)(2,1)}) custom-call(s32[1]{0:T(128)} %bitcast.1.core_ref, bf16[528,128]{1,0:T(8,128)(2,1)} %copy-done.2, bf16[512,128]{1,0:T(8,128)(2,1)} %copy-done.5, bf16[512,128]{1,0:T(8,128)(2,1)} %get-tuple-element.28.sr_ref, f32[512,512]{1,0:T(8,128)} %get-tuple-element.29.mixed_ref, ...), custom_call_target="tpu_custom_call" | custom-call | flops 1073741824 | bytes 6000000 | tf_op jit(solution)/shard_map/project/pallas_call | solution.py:405
  51.2 18.4 %collective-permute-start.3 = (bf16[4,512,256]{2,1,0:T(8,128)(2,1)}, bf16[4,512,256]{2,1,0:T(8,128)(2,1)S(1)}, u32[]{:S(2)}, u32[]{:S(2)}) collective-permute-start(bf16[4,512,256]{2,1,0:T(8,128)(2,1)} %get-tuple-element.32), channel_id=1, source_target_pairs={{0,1},{1,0},{2,3},{3,2},{4,5},{5,4},{6,7},{7,6},{8,9},{9,8},{10,11... | collective-permute-start | bytes 3145736 | tf_op jit(solution)/shard_map/ppermute | solution.py:574
  69.6 2.5 %collective-permute-done.3 = bf16[4,512,256]{2,1,0:T(8,128)(2,1)S(1)} collective-permute-done((bf16[4,512,256]{2,1,0:T(8,128)(2,1)}, bf16[4,512,256]{2,1,0:T(8,128)(2,1)S(1)}, u32[]{:S(2)}, u32[]{:S(2)}) %collective-permute-start.3) | collective-permute-done | bytes 1048608 | tf_op jit(solution)/shard_map/ppermute | solution.py:574
  72.1 1.5 add_convert_fusion
  73.6 18.0 %all_to_all.10.parts_ref = bf16[4,512,256]{2,1,0:T(8,128)(2,1)} all-to-all(bf16[4,512,256]{2,1,0:T(8,128)(2,1)S(1)} %add_convert_fusion), channel_id=1, replica_groups={{0,2,4,6},{1,3,5,7},{8,10,12,14},{9,11,13,15},{16,18,20,22},{17,19,21,2..., dimensions={0} | all-to-all | bytes 2097152 | tf_op jit(solution)/shard_map/all_to_all | solution.py:607
  91.6 2.5 %after_mix.1 = (bf16[512,256]{1,0:T(8,128)(2,1)}, bf16[4,512,256]{2,1,0:T(8,128)(2,1)}) custom-call(s32[1]{0:T(128)} %bitcast.at_ref, bf16[4,512,256]{2,1,0:T(8,128)(2,1)} %all_to_all.10.parts_ref, bf16[512,2048]{1,0:T(8,128)(2,1)} %residual_ref.1), custom_call_target="tpu_custom_call" | custom-call | tf_op jit(solution)/shard_map/after_mix/pallas_call | solution.py:429
  94.1 17.5 %all_to_all.11.mine_ref = bf16[4,512,256]{2,1,0:T(8,128)(2,1)S(1)} all-to-all(bf16[4,512,256]{2,1,0:T(8,128)(2,1)} %get-tuple-element.34), channel_id=1, replica_groups={{0,2,4,6},{1,3,5,7},{8,10,12,14},{9,11,13,15},{16,18,20,22},{17,19,21,2..., dimensions={0} | all-to-all | bytes 2097152 | tf_op jit(solution)/shard_map/all_to_all | solution.py:607
  111.6 2.1 %collective-permute-start.4 = (bf16[4,512,256]{2,1,0:T(8,128)(2,1)S(1)}, bf16[4,512,256]{2,1,0:T(8,128)(2,1)S(1)}, u32[]{:S(2)}, u32[]{:S(2)}) collective-permute-start(bf16[4,512,256]{2,1,0:T(8,128)(2,1)S(1)} %all_to_all.11.mine_ref), channel_id=1, source_target_pairs={{0,1},{1,0},{2,3},{3,2},{4,5},{5,4},{6,7},{7,6},{8,9},{9,8},{10,11... | collective-permute-start | bytes 3145736 | tf_op jit(solution)/shard_map/ppermute | solution.py:574
  113.7 0.6 reshape.32.gain_ref
  114.3 1.7 collective-permute-done.4.other_ref
  116.0 1.0 copy-done.1
  117.0 4.0 %normalised.1.normal_ref = bf16[512,2048]{1,0:T(8,128)(2,1)} custom-call(s32[1]{0:T(128)} %bitcast.at_ref, bf16[4,512,256]{2,1,0:T(8,128)(2,1)} %copy-done, bf16[4,512,256]{2,1,0:T(8,128)(2,1)} %copy-done.1, bf16[1,2048]{1,0:T(2,128)(2,1)} %reshape.32.gain_ref), custom_call_target="tpu_custom_call" | custom-call | tf_op jit(solution)/shard_map/normalised/pallas_call | solution.py:468
  121.0 13.8 %all-gather.3.cloned.1.call-done = bf16[33792,128]{1,0:T(8,128)(2,1)} async-done(((bf16[2112,128]{1,0:T(8,128)(2,1)}), bf16[33792,128]{1,0:T(8,128)(2,1)}) %all-gather.3.cloned.1.call-update) | async-done | bytes 8650768 | tf_op jit(solution)/shard_map/all_gather | solution.py:640
  134.8 9.9 %channel_mixer.1 = (bf16[2,2,256,256]{3,2,1,0:T(8,128)(2,1)}, bf16[2,2,256,256]{3,2,1,0:T(8,128)(2,1)}, bf16[4,256,256]{2,1,0:T(8,128)(2,1)}, bf16[4,256,256]{2,1,0:T(8,128)(2,1)}) custom-call(s32[1]{0:T(128)} %bitcast.at_ref, bf16[512,2048]{1,0:T(8,128)(2,1)} %normalised.1.normal_ref, bf16[16,2112,128]{2,1,0:T(8,128)(2,1)} %bitcast.39), custom_call_target="tpu_custom_call" | custom-call | flops 4429185024 | bytes 14000000 | tf_op jit(solution)/shard_map/channel_mixer/pallas_call | solution.py:550
  144.7 2.3 %collective-permute-start.6 = (bf16[2,2,256,256]{3,2,1,0:T(8,128)(2,1)}, bf16[2,2,256,256]{3,2,1,0:T(8,128)(2,1)S(1)}, u32[]{:S(2)}, u32[]{:S(2)}) collective-permute-start(bf16[2,2,256,256]{3,2,1,0:T(8,128)(2,1)} %get-tuple-element.38), channel_id=1, source_target_pairs={{0,1},{1,0},{2,3},{3,2},{4,5},{5,4},{6,7},{7,6},{8,9},{9,8},{10,11... | collective-permute-start | bytes 1572872 | tf_op jit(solution)/shard_map/ppermute | solution.py:574
  147.0 0.1 collective-permute-start.5
  147.1 1.6 collective-permute-done.6
  148.7 1.2 add_convert_fusion.1
  149.9 1.3 collective-permute-start.7
  151.2 1.5 collective-permute-start.9
  152.7 0.0 collective-permute-done.5
  152.7 0.1 convert_add_fusion
  152.9 5.9 %collective-permute-done.7 = bf16[2,256,256]{2,1,0:T(8,128)(2,1)S(1)} collective-permute-done((bf16[2,256,256]{2,1,0:T(8,128)(2,1)S(1)}, bf16[2,256,256]{2,1,0:T(8,128)(2,1)S(1)}, u32[]{:S(2)}, u32[]{:S(2)}) %collective-permute-start.7) | collective-permute-done | bytes 262176 | tf_op jit(solution)/shard_map/ppermute | solution.py:579
  158.7 0.0 collective-permute-done.9
  158.7 0.1 fusion.7
  158.8 2.5 %collective-permute-start.10 = (bf16[256,256]{1,0:T(8,128)(2,1)S(1)}, bf16[256,256]{1,0:T(8,128)(2,1)S(1)}, u32[]{:S(2)}, u32[]{:S(2)}) collective-permute-start(bf16[256,256]{1,0:T(8,128)(2,1)S(1)} %get-tuple-element.40), channel_id=1, source_target_pairs={{0,6},{1,7},{2,0},{3,1},{4,2},{5,3},{6,4},{7,5},{8,14},{9,15},{10,... | collective-permute-start | bytes 393224 | tf_op jit(solution)/shard_map/ppermute | solution.py:579
  161.3 0.0 collective-permute-start.8
  161.3 1.9 %collective-permute-done.10 = bf16[256,256]{1,0:T(8,128)(2,1)S(1)} collective-permute-done((bf16[256,256]{1,0:T(8,128)(2,1)S(1)}, bf16[256,256]{1,0:T(8,128)(2,1)S(1)}, u32[]{:S(2)}, u32[]{:S(2)}) %collective-permute-start.10) | collective-permute-done | bytes 131104 | tf_op jit(solution)/shard_map/ppermute | solution.py:579
  163.2 3.1 %collective-permute-done.8 = bf16[256,256]{1,0:T(8,128)(2,1)S(1)} collective-permute-done((bf16[256,256]{1,0:T(8,128)(2,1)S(1)}, bf16[256,256]{1,0:T(8,128)(2,1)S(1)}, u32[]{:S(2)}, u32[]{:S(2)}) %collective-permute-start.8) | collective-permute-done | bytes 131104 | tf_op jit(solution)/shard_map/ppermute | solution.py:579
  166.3 0.8 fusion.4
  (20 shorter events, 0.1 us)
Async XLA Ops:
  6.5 8.8 %copy-start.8 = (f32[8]{0:T(128)S(1)}, f32[8]{0:T(128)}, u32[]{:S(2)}) copy-start(f32[8]{0:T(128)} %param.24) | copy-start | bytes 100
  6.5 128.2 %all-gather.3.cloned.1.call-start = ((), (), s32[]{:S(2)}) async-start(), calls=%async_computation.2 | async-start | bytes 9191424 | tf_op jit(solution)/shard_map/all_gather | solution.py:640
  6.6 32.5 %copy-start.7 = (bf16[512]{0:T(512)(128)(2,1)S(1)}, bf16[512]{0:T(512)(128)(2,1)}, u32[]{:S(2)}) copy-start(bf16[512]{0:T(512)(128)(2,1)} %param.30) | copy-start | bytes 3076
  10.1 6.4 %collective-permute-start = (bf16[16,896]{1,0:T(8,128)(2,1)}, bf16[16,896]{1,0:T(8,128)(2,1)S(1)}, u32[]{:S(2)}, u32[]{:S(2)}) collective-permute-start(bf16[16,896]{1,0:T(8,128)(2,1)} %pack_edge.1), channel_id=1, source_target_pairs={{0,8},{8,16},{16,24},{24,32},{32,40},{40,48},{48,56},{56,64},{64,7... | collective-permute-start | bytes 86024 | tf_op jit(solution)/shard_map/ppermute | solution.py:24
  16.5 0.6 copy-start.9
  22.2 6.7 %collective-permute-start.1 = (bf16[528,128]{1,0:T(8,128)(2,1)}, bf16[528,128]{1,0:T(8,128)(2,1)S(1)}, u32[]{:S(2)}, u32[]{:S(2)}) collective-permute-start(bf16[528,128]{1,0:T(8,128)(2,1)} %get-tuple-element.22.own_ref), channel_id=1, source_target_pairs={{0,8},{8,16},{16,24},{24,32},{32,40},{40,48},{48,56},{56,64},{64,7... | collective-permute-start | bytes 405512 | tf_op jit(solution)/shard_map/ppermute | solution.py:24
  28.9 0.7 copy-start.2
  31.2 12.9 %collective-permute-start.2 = (bf16[512,128]{1,0:T(8,128)(2,1)}, bf16[512,128]{1,0:T(8,128)(2,1)S(1)}, u32[]{:S(2)}, u32[]{:S(2)}) collective-permute-start(bf16[512,128]{1,0:T(8,128)(2,1)} %join_states.1), channel_id=1, source_target_pairs={{0,16},{8,24},{16,32},{24,40},{32,48},{40,56},{48,64},{56,72},{64,... | collective-permute-start | bytes 393224 | tf_op jit(solution)/shard_map/ppermute | solution.py:24
  44.1 0.7 copy-start.5
  51.2 20.9 %collective-permute-start.3 = (bf16[4,512,256]{2,1,0:T(8,128)(2,1)}, bf16[4,512,256]{2,1,0:T(8,128)(2,1)S(1)}, u32[]{:S(2)}, u32[]{:S(2)}) collective-permute-start(bf16[4,512,256]{2,1,0:T(8,128)(2,1)} %get-tuple-element.32), channel_id=1, source_target_pairs={{0,1},{1,0},{2,3},{3,2},{4,5},{5,4},{6,7},{7,6},{8,9},{9,8},{10,11... | collective-permute-start | bytes 3145736 | tf_op jit(solution)/shard_map/ppermute | solution.py:574
  91.6 22.1 %copy-start.6 = (bf16[2048]{0:T(1024)(128)(2,1)S(1)}, bf16[2048]{0:T(1024)(128)(2,1)}, u32[]{:S(2)}) copy-start(bf16[2048]{0:T(1024)(128)(2,1)} %param.32) | copy-start | bytes 12292
  111.6 4.4 %copy-start = (bf16[4,512,256]{2,1,0:T(8,128)(2,1)}, bf16[4,512,256]{2,1,0:T(8,128)(2,1)S(1)}, u32[]{:S(2)}) copy-start(bf16[4,512,256]{2,1,0:T(8,128)(2,1)S(1)} %all_to_all.11.mine_ref) | copy-start | bytes 3145732
  111.6 4.4 %collective-permute-start.4 = (bf16[4,512,256]{2,1,0:T(8,128)(2,1)S(1)}, bf16[4,512,256]{2,1,0:T(8,128)(2,1)S(1)}, u32[]{:S(2)}, u32[]{:S(2)}) collective-permute-start(bf16[4,512,256]{2,1,0:T(8,128)(2,1)S(1)} %all_to_all.11.mine_ref), channel_id=1, source_target_pairs={{0,1},{1,0},{2,3},{3,2},{4,5},{5,4},{6,7},{7,6},{8,9},{9,8},{10,11... | collective-permute-start | bytes 3145736 | tf_op jit(solution)/shard_map/ppermute | solution.py:574
  116.0 1.0 copy-start.1
  144.7 8.0 %copy-start.3 = (bf16[4,256,256]{2,1,0:T(8,128)(2,1)S(1)}, bf16[4,256,256]{2,1,0:T(8,128)(2,1)}, u32[]{:S(2)}) copy-start(bf16[4,256,256]{2,1,0:T(8,128)(2,1)} %get-tuple-element.35) | copy-start | bytes 1572868
  144.7 4.0 %collective-permute-start.6 = (bf16[2,2,256,256]{3,2,1,0:T(8,128)(2,1)}, bf16[2,2,256,256]{3,2,1,0:T(8,128)(2,1)S(1)}, u32[]{:S(2)}, u32[]{:S(2)}) collective-permute-start(bf16[2,2,256,256]{3,2,1,0:T(8,128)(2,1)} %get-tuple-element.38), channel_id=1, source_target_pairs={{0,1},{1,0},{2,3},{3,2},{4,5},{5,4},{6,7},{7,6},{8,9},{9,8},{10,11... | collective-permute-start | bytes 1572872 | tf_op jit(solution)/shard_map/ppermute | solution.py:574
  147.0 5.8 %collective-permute-start.5 = (bf16[4,256,256]{2,1,0:T(8,128)(2,1)}, bf16[4,256,256]{2,1,0:T(8,128)(2,1)S(1)}, u32[]{:S(2)}, u32[]{:S(2)}) collective-permute-start(bf16[4,256,256]{2,1,0:T(8,128)(2,1)} %get-tuple-element.36), channel_id=1, source_target_pairs={{0,1},{1,0},{2,3},{3,2},{4,5},{5,4},{6,7},{7,6},{8,9},{9,8},{10,11... | collective-permute-start | bytes 1572872 | tf_op jit(solution)/shard_map/ppermute | solution.py:574
  149.9 8.8 %collective-permute-start.7 = (bf16[2,256,256]{2,1,0:T(8,128)(2,1)S(1)}, bf16[2,256,256]{2,1,0:T(8,128)(2,1)S(1)}, u32[]{:S(2)}, u32[]{:S(2)}) collective-permute-start(bf16[2,256,256]{2,1,0:T(8,128)(2,1)S(1)} %get-tuple-element.41), channel_id=1, source_target_pairs={{0,2},{1,3},{2,4},{3,5},{4,6},{5,7},{6,0},{7,1},{8,10},{9,11},{10,... | collective-permute-start | bytes 786440 | tf_op jit(solution)/shard_map/ppermute | solution.py:579
  151.2 7.5 %collective-permute-start.9 = (bf16[2,256,256]{2,1,0:T(8,128)(2,1)S(1)}, bf16[2,256,256]{2,1,0:T(8,128)(2,1)S(1)}, u32[]{:S(2)}, u32[]{:S(2)}) collective-permute-start(bf16[2,256,256]{2,1,0:T(8,128)(2,1)S(1)} %get-tuple-element.42), channel_id=1, source_target_pairs={{0,6},{1,7},{2,0},{3,1},{4,2},{5,3},{6,4},{7,5},{8,14},{9,15},{10,... | collective-permute-start | bytes 786440 | tf_op jit(solution)/shard_map/ppermute | solution.py:579
  152.7 13.6 %copy-start.4 = (bf16[512,256]{1,0:T(8,128)(2,1)S(1)}, bf16[512,256]{1,0:T(8,128)(2,1)}, u32[]{:S(2)}) copy-start(bf16[512,256]{1,0:T(8,128)(2,1)} %get-tuple-element.33) | copy-start | bytes 786436
  158.8 4.4 %collective-permute-start.10 = (bf16[256,256]{1,0:T(8,128)(2,1)S(1)}, bf16[256,256]{1,0:T(8,128)(2,1)S(1)}, u32[]{:S(2)}, u32[]{:S(2)}) collective-permute-start(bf16[256,256]{1,0:T(8,128)(2,1)S(1)} %get-tuple-element.40), channel_id=1, source_target_pairs={{0,6},{1,7},{2,0},{3,1},{4,2},{5,3},{6,4},{7,5},{8,14},{9,15},{10,... | collective-permute-start | bytes 393224 | tf_op jit(solution)/shard_map/ppermute | solution.py:579
  161.3 5.0 %collective-permute-start.8 = (bf16[256,256]{1,0:T(8,128)(2,1)S(1)}, bf16[256,256]{1,0:T(8,128)(2,1)S(1)}, u32[]{:S(2)}, u32[]{:S(2)}) collective-permute-start(bf16[256,256]{1,0:T(8,128)(2,1)S(1)} %get-tuple-element.39), channel_id=1, source_target_pairs={{0,2},{1,3},{2,4},{3,5},{4,6},{5,7},{6,0},{7,1},{8,10},{9,11},{10,... | collective-permute-start | bytes 393224 | tf_op jit(solution)/shard_map/ppermute | solution.py:579
Sparse Core Ops, SparseCore 0:
  9.1 125.5 all-gather.2
